TPU v7x, 512 devices: a whole 4x8x8 slice. The times are simulated.
512 devices in a mesh: sp: 64 (over z, y), tp: 8 (over x, core).
Axes of the slice: x: 4, y: 8, z: 8, core: 2. Of those that a mesh axis runs over, the one named last changes fastest.
Arguments:
- queries: bfloat16 [1, 24576, 2048], P(None, 'sp', 'tp'), may hold values from -5 to 5
- keys: bfloat16 [1, 24576, 2048], P(None, 'sp', 'tp'), may hold values from -5 to 5
- values: bfloat16 [1, 24576, 2048], P(None, 'sp', 'tp'), may hold values from -6 to 6
- rel_bias: float32 [16, 192], P('tp'), may hold values from -3 to 3
- out_grad: bfloat16 [1, 24576, 2048], P(None, 'sp', 'tp'), may hold values from -48 to 48
Outputs:
- query_grad: bfloat16 [1, 24576, 2048], P(None, 'sp', 'tp')
- key_grad: bfloat16 [1, 24576, 2048], P(None, 'sp', 'tp')
- value_grad: bfloat16 [1, 24576, 2048], P(None, 'sp', 'tp')
- bias_grad: float32 [16, 192], replicated
All inputs are finite; a program needn't handle non-finite values.
Results may differ from a plain program's by a relative error of at most 0.0049.
Values may be sent and summed in bfloat16 or wider, within the bound.
No kernel may reach another device: no remote copies, remote signals or barrier semaphores. Data moves between devices by JAX's collectives and lax.ppermute only.
A program may use at most 64 MiB of HBM per device.

v0:
```python
import jax
import jax.numpy as jnp
from jax import lax
from jax.sharding import PartitionSpec as P

HEAD_DIM = 128
SEG = 64
LEFT = 4
CLIP = 128
BAND = 320
BUCKETS = 192


def from_behind(value, axis, steps):
    count = lax.axis_size(axis)
    leading, last = (max(0, -steps), min(count, count - steps))
    return lax.ppermute(value, axis, [(source, source + steps) for source in range(leading, last)])


def copy_for_each(shard, axis):
    copies = jnp.broadcast_to(shard, (lax.axis_size(axis), *shard.shape))
    return lax.all_to_all(copies, axis, split_axis=0, concat_axis=0, tiled=True)


def taken_together(shard, axis):
    everything = copy_for_each(shard, axis)
    return jnp.sum(everything, axis=0)


def joined_along(pieces, dim):
    shape = list(pieces.shape[1:])
    shape[dim] *= pieces.shape[0]
    return jnp.moveaxis(pieces, 0, dim).reshape(shape)


def collect(shard, axis, dim):
    return joined_along(copy_for_each(shard, axis), dim)


def diagonal_onehot():
    span = SEG + BAND - 1
    diag = jnp.arange(span, dtype=jnp.int32)
    bucket = jnp.clip(SEG - 1 - diag + LEFT * SEG, 1 - SEG, CLIP) + SEG - 1
    return (bucket[None, :] == jnp.arange(BUCKETS, dtype=jnp.int32)[:, None]).astype(jnp.float32)


def on_diagonals(rel_bias, onehot):
    return jnp.dot(
        rel_bias, onehot, preferred_element_type=jnp.float32, precision=lax.Precision.HIGHEST
    )


def fill_toeplitz(diag_vals):
    head_count, span = diag_vals.shape
    tiled = jnp.tile(diag_vals, (1, SEG))[:, SEG - 1 :]
    tiled = tiled[:, : SEG * (span - 1)].reshape(head_count, SEG, span - 1)
    return tiled[:, :, :BAND]


def sum_diagonals(terms):
    head_count = terms.shape[0]
    span = SEG + BAND - 1
    padded = jnp.concatenate(
        [
            jnp.zeros((head_count, SEG, SEG - 1), jnp.float32),
            terms,
            jnp.zeros((head_count, SEG, SEG), jnp.float32),
        ],
        axis=2,
    )
    width = padded.shape[2]
    flat = jnp.concatenate(
        [padded.reshape(head_count, SEG * width), jnp.zeros((head_count, SEG), jnp.float32)], axis=1
    )
    skewed = flat.reshape(head_count, SEG, width + 1)[:, :, :span]
    return jnp.sum(skewed, axis=1)


def band_core(q_segs, k_band, v_band, g_segs, table, key_valid):
    seg_count = q_segs.shape[1]
    score_scale = HEAD_DIM ** (-0.5)
    score_parts = []
    prob_parts = []
    for offset in range(LEFT + 1):
        score_parts.append(
            jnp.einsum(
                "sncha,snkha->snhck",
                q_segs,
                k_band[:, offset : offset + seg_count],
                preferred_element_type=jnp.float32,
            )
        )
        prob_parts.append(
            jnp.einsum(
                "sncha,snkha->snhck",
                g_segs,
                v_band[:, offset : offset + seg_count],
                preferred_element_type=jnp.float32,
            )
        )
    score = jnp.concatenate(score_parts, axis=-1) * score_scale + table[None, None]
    score = jnp.where(key_valid[None, :, None, None, :], score, -jnp.inf)
    row_max = jnp.max(score, axis=-1, keepdims=True)
    expo = jnp.exp(score - row_max)
    row_sum = jnp.sum(expo, axis=-1, keepdims=True)
    prob = expo / row_sum
    log_norm = (row_max + jnp.log(row_sum))[..., 0]
    prob_grad = jnp.concatenate(prob_parts, axis=-1)
    row_delta = jnp.sum(prob * prob_grad, axis=-1)
    score_grad = prob * (prob_grad - row_delta[..., None])
    bias_terms = jnp.sum(score_grad, axis=(0, 1))
    prob_low = prob.astype(jnp.bfloat16)
    grad_low = (score_grad * score_scale).astype(jnp.bfloat16)
    query_acc = jnp.zeros(q_segs.shape, jnp.float32)
    key_acc = jnp.zeros(k_band.shape, jnp.float32)
    value_acc = jnp.zeros(k_band.shape, jnp.float32)
    for offset in range(LEFT + 1):
        grad_part = grad_low[..., offset * SEG : (offset + 1) * SEG]
        prob_part = prob_low[..., offset * SEG : (offset + 1) * SEG]
        query_acc = query_acc + jnp.einsum(
            "snhck,snkha->sncha",
            grad_part,
            k_band[:, offset : offset + seg_count],
            preferred_element_type=jnp.float32,
        )
        first_seg = 0
        key_acc = key_acc.at[:, offset + first_seg : offset + seg_count].add(
            jnp.einsum("snhck,sncha->snkha", grad_part, q_segs, preferred_element_type=jnp.float32)
        )
        value_acc = value_acc.at[:, offset + first_seg : offset + seg_count].add(
            jnp.einsum("snhck,sncha->snkha", prob_part, g_segs, preferred_element_type=jnp.float32)
        )
    return (query_acc, key_acc, value_acc, bias_terms, log_norm, row_delta)


def local(queries, keys, values, rel_bias, out_grad):
    seq_count, tok_rows, row_width = queries.shape
    head_count = row_width // HEAD_DIM
    seg_count = tok_rows // SEG
    reach = LEFT * SEG
    seq_index = lax.axis_index("sp")
    seg_shape = (seq_count, seg_count, SEG, head_count, HEAD_DIM)
    band_shape = (seq_count, seg_count + LEFT, SEG, head_count, HEAD_DIM)
    onehot = diagonal_onehot()
    table = fill_toeplitz(on_diagonals(rel_bias, onehot))
    prior_k, prior_v = from_behind(
        (keys[:, tok_rows - reach :], values[:, tok_rows - reach :]), "sp", 1
    )
    k_band = jnp.concatenate([prior_k, keys], axis=1).reshape(band_shape)
    v_band = jnp.concatenate([prior_v, values], axis=1).reshape(band_shape)
    q_segs = queries.reshape(seg_shape)
    g_segs = out_grad.reshape(seg_shape)
    positions = (
        seq_index * tok_rows
        + jnp.arange(seg_count, dtype=jnp.int32)[:, None] * SEG
        - reach
        + jnp.arange(BAND, dtype=jnp.int32)[None, :]
    )
    key_valid = positions >= 0
    flat = (seq_count, reach + tok_rows, row_width)
    query_acc, key_acc, value_acc, bias_terms, log_norm, row_delta = band_core(
        q_segs, k_band, v_band, g_segs, table, key_valid
    )
    key_flat = key_acc.reshape(flat)
    value_flat = value_acc.reshape(flat)
    back_k, back_v = from_behind((key_flat[:, :reach], value_flat[:, :reach]), "sp", -1)
    key_own = key_flat[:, reach:].at[:, tok_rows - reach :].add(back_k)
    value_own = value_flat[:, reach:].at[:, tok_rows - reach :].add(back_v)
    query_grad = query_acc.astype(jnp.bfloat16).reshape(seq_count, tok_rows, row_width)
    key_grad = key_own.astype(jnp.bfloat16)
    value_grad = value_own.astype(jnp.bfloat16)
    local_bias = jnp.dot(
        sum_diagonals(bias_terms),
        onehot.T,
        preferred_element_type=jnp.float32,
        precision=lax.Precision.HIGHEST,
    )
    summed = taken_together(local_bias, "sp")
    bias_grad = collect(summed, "tp", 0)
    return (query_grad, key_grad, value_grad, bias_grad)


def solution(mesh):
    return jax.shard_map(
        local,
        mesh=mesh,
        in_specs=(
            P(None, "sp", "tp"),
            P(None, "sp", "tp"),
            P(None, "sp", "tp"),
            P("tp", None),
            P(None, "sp", "tp"),
        ),
        out_specs=(P(None, "sp", "tp"), P(None, "sp", "tp"), P(None, "sp", "tp"), P()),
        check_vma=False,
    )
```

profile of v0, /device:TPU:1, one launch (start us, length us, event | category | flops | bytes accessed | tf_op | source)
XLA Modules:
  0.0 84.2 jit_solution(5421645292207113864)
XLA Ops:
  0.6 0.9 %slice.478 = bf16[1,256,256]{2,1,0:T(8,128)(2,1)S(1)} slice(bf16[1,384,256]{2,1,0:T(8,128)(2,1)} %param.30), slice={[0:1], [128:384], [0:256]} | slice | bytes 262144 | tf_op jit(solution)/shard_map/slice | solution.py:147
  1.6 4.0 %collective-permute-start = (bf16[1,256,256]{2,1,0:T(8,128)(2,1)S(1)}, bf16[1,256,256]{2,1,0:T(8,128)(2,1)S(1)}, u32[]{:S(2)}, u32[]{:S(2)}) collective-permute-start(bf16[1,256,256]{2,1,0:T(8,128)(2,1)S(1)} %slice.478), channel_id=1, source_target_pairs={{0,8},{8,16},{16,24},{24,32},{32,40},{40,48},{48,56},{56,64},{64,7... | collective-permute-start | bytes 393224 | tf_op jit(solution)/shard_map/ppermute | solution.py:17
  5.6 0.9 %slice.486 = bf16[1,256,256]{2,1,0:T(8,128)(2,1)S(1)} slice(bf16[1,384,256]{2,1,0:T(8,128)(2,1)} %param.31), slice={[0:1], [128:384], [0:256]} | slice | bytes 262144 | tf_op jit(solution)/shard_map/slice | solution.py:147
  6.5 3.3 %collective-permute-start.1 = (bf16[1,256,256]{2,1,0:T(8,128)(2,1)S(1)}, bf16[1,256,256]{2,1,0:T(8,128)(2,1)S(1)}, u32[]{:S(2)}, u32[]{:S(2)}) collective-permute-start(bf16[1,256,256]{2,1,0:T(8,128)(2,1)S(1)} %slice.486), channel_id=1, source_target_pairs={{0,8},{8,16},{16,24},{24,32},{32,40},{40,48},{48,56},{56,64},{64,7... | collective-permute-start | bytes 393224 | tf_op jit(solution)/shard_map/ppermute | solution.py:17
  9.9 1.0 %reshape.1130 = bf16[6,64,2,128]{3,2,1,0:T(2,128)(2,1)S(1)} reshape(bf16[1,384,256]{2,1,0:T(8,128)(2,1)} %param.33) | data formatting | bytes 393216 | tf_op jit(solution)/shard_map/reshape.447
  10.9 1.0 %reshape.1122 = bf16[6,64,2,128]{3,2,1,0:T(2,128)(2,1)S(1)} reshape(bf16[1,384,256]{2,1,0:T(8,128)(2,1)} %param.29) | data formatting | bytes 393216 | tf_op jit(solution)/shard_map/reshape.428
  13.0 0.7 pad.29.clone
  14.5 0.9 %fusion.49 = (bf16[1,6,64,2,128]{4,3,2,1,0:T(2,128)(2,1)S(1)}, bf16[1,6,64,2,128]{4,3,2,1,0:T(2,128)(2,1)S(1)}, bf16[1,6,64,2,128]{4,3,2,1,0:T(2,128)(2,1)S(1)},...) fusion(bf16[1,10,64,2,128]{4,3,2,1,0:T(2,128)(2,1)S(1)} %reshape.1120), kind=kLoop, calls=%fused_computation.109 | loop fusion | bytes 1966080 | tf_op jit(solution)/shard_map/slice | solution.py:89
  15.6 0.9 %fusion.50 = (bf16[1,6,64,2,128]{4,3,2,1,0:T(2,128)(2,1)S(1)}, bf16[1,6,64,2,128]{4,3,2,1,0:T(2,128)(2,1)S(1)}, bf16[1,6,64,2,128]{4,3,2,1,0:T(2,128)(2,1)S(1)},...) fusion(bf16[1,10,64,2,128]{4,3,2,1,0:T(2,128)(2,1)S(1)} %reshape.1128), kind=kLoop, calls=%fused_computation.110 | loop fusion | bytes 1966080 | tf_op jit(solution)/shard_map/slice | solution.py:97
  16.7 1.0 %convolution_bitcast_fusion.13 = f32[1,6,2,64,64]{4,3,2,1,0:T(8,128)} fusion(bf16[1,6,64,2,128]{4,3,2,1,0:T(2,128)(2,1)S(1)} %get-tuple-element.171, bf16[6,64,2,128]{3,2,1,0:T(2,128)(2,1)S(1)} %reshape.1130), kind=kOutput, calls=%fused_computation.17 | convolution fusion | flops 12582912 | bytes 589824 | tf_op jit(solution)/shard_map/sncha,snkha->snhck/dot_general | solution.py:94
  17.7 1.0 %convolution_bitcast_fusion.12 = f32[1,6,2,64,64]{4,3,2,1,0:T(8,128)} fusion(bf16[1,6,64,2,128]{4,3,2,1,0:T(2,128)(2,1)S(1)} %get-tuple-element.170, bf16[6,64,2,128]{3,2,1,0:T(2,128)(2,1)S(1)} %reshape.1130), kind=kOutput, calls=%fused_computation.16 | convolution fusion | flops 12582912 | bytes 589824 | tf_op jit(solution)/shard_map/sncha,snkha->snhck/dot_general | solution.py:94
  18.7 1.0 %convolution_bitcast_fusion.11 = f32[1,6,2,64,64]{4,3,2,1,0:T(8,128)} fusion(bf16[1,6,64,2,128]{4,3,2,1,0:T(2,128)(2,1)S(1)} %get-tuple-element.169, bf16[6,64,2,128]{3,2,1,0:T(2,128)(2,1)S(1)} %reshape.1130), kind=kOutput, calls=%fused_computation.15 | convolution fusion | flops 12582912 | bytes 589824 | tf_op jit(solution)/shard_map/sncha,snkha->snhck/dot_general | solution.py:94
  19.6 1.0 %convolution_bitcast_fusion.10 = f32[1,6,2,64,64]{4,3,2,1,0:T(8,128)} fusion(bf16[1,6,64,2,128]{4,3,2,1,0:T(2,128)(2,1)S(1)} %get-tuple-element.168, bf16[6,64,2,128]{3,2,1,0:T(2,128)(2,1)S(1)} %reshape.1130), kind=kOutput, calls=%fused_computation.14 | convolution fusion | flops 12582912 | bytes 589824 | tf_op jit(solution)/shard_map/sncha,snkha->snhck/dot_general | solution.py:94
  21.3 1.0 %convolution_bitcast_fusion.16 = f32[1,6,2,64,64]{4,3,2,1,0:T(8,128)} fusion(bf16[1,6,64,2,128]{4,3,2,1,0:T(2,128)(2,1)S(1)} %get-tuple-element.164, bf16[6,64,2,128]{3,2,1,0:T(2,128)(2,1)S(1)} %reshape.1122), kind=kOutput, calls=%fused_computation.20 | convolution fusion | flops 12582912 | bytes 589824 | tf_op jit(solution)/shard_map/sncha,snkha->snhck/dot_general | solution.py:86
  22.3 1.0 %convolution_bitcast_fusion.15 = f32[1,6,2,64,64]{4,3,2,1,0:T(8,128)} fusion(bf16[1,6,64,2,128]{4,3,2,1,0:T(2,128)(2,1)S(1)} %get-tuple-element.163, bf16[6,64,2,128]{3,2,1,0:T(2,128)(2,1)S(1)} %reshape.1122), kind=kOutput, calls=%fused_computation.19 | convolution fusion | flops 12582912 | bytes 589824 | tf_op jit(solution)/shard_map/sncha,snkha->snhck/dot_general | solution.py:86
  23.3 1.5 %concatenate.116 = f32[1,6,2,64,320]{4,3,2,1,0:T(8,128)S(1)} concatenate(f32[1,6,2,64,64]{4,3,2,1,0:T(8,128)S(1)} %convolution_bitcast_fusion.19, f32[1,6,2,64,64]{4,3,2,1,0:T(8,128)S(1)} %convolution_bitcast_fusion.18, f32[1,6,2,64,64]{4,3,2,1,0:T(8,128)S(1)} %convolution_bitcast_fusion.17, f32[1,6,2,64,64]{4,3,2,1,0:T(8,128)} %convolution_bitcast_fusion.16, ...), dimensions={4} | concatenate | bytes 1966080 | tf_op jit(solution)/shard_map/concatenate | solution.py:101
  25.6 1.7 %concatenate.123 = f32[1,6,2,64,320]{4,3,2,1,0:T(8,128)S(1)} concatenate(f32[1,6,2,64,64]{4,3,2,1,0:T(8,128)S(1)} %convolution_bitcast_fusion.14, f32[1,6,2,64,64]{4,3,2,1,0:T(8,128)} %convolution_bitcast_fusion.13, f32[1,6,2,64,64]{4,3,2,1,0:T(8,128)} %convolution_bitcast_fusion.12, f32[1,6,2,64,64]{4,3,2,1,0:T(8,128)} %convolution_bitcast_fusion.11, ...), dimensions={4} | concatenate | bytes 1966080 | tf_op jit(solution)/shard_map/concatenate | solution.py:108
  27.9 1.4 %fusion.21 = (f32[2,64,320]{2,1,0:T(8,128)S(1)}, bf16[1,6,2,64,320]{4,3,2,1,0:T(8,128)(2,1)S(1)}, bf16[1,6,2,64,320]{4,3,2,1,0:T(8,128)(2,1)S(1)}) fusion(f32[1,6,2,64,320]{4,3,2,1,0:T(8,128)S(1)} %concatenate.123, f32[6,2,64]{2,1,0:T(2,128)S(1)} %multiply_reduce_fusion, f32[6,2,64]{2,1,0:T(2,128)} %copy-done.14, f32[6,2,64]{2,1,0:T(2,128)S(1)} %fusion.20, ...), kind=kLoop, calls=%fused_computation.51 | loop fusion | flops 2662400 | bytes 3287936 | tf_op jit(solution)/shard_map/reduce_sum | solution.py:111
  33.5 0.9 %slice.539 = f32[1,256,256]{2,0,1:T(1,128)} slice(f32[1,640,256]{2,0,1:T(1,128)S(1)} %bitcast.217), slice={[0:1], [0:256], [0:256]} | slice | bytes 524288 | tf_op jit(solution)/shard_map/slice | solution.py:166
  34.4 1.3 %collective-permute-start.2 = (f32[1,256,256]{2,0,1:T(1,128)}, f32[1,256,256]{2,0,1:T(1,128)}, u32[]{:S(2)}, u32[]{:S(2)}) collective-permute-start(f32[1,256,256]{2,0,1:T(1,128)} %slice.539), channel_id=1, source_target_pairs={{8,0},{16,8},{24,16},{32,24},{40,32},{48,40},{56,48},{64,56},{72,6... | collective-permute-start | bytes 786440 | tf_op jit(solution)/shard_map/ppermute | solution.py:17
  38.2 0.7 broadcast_in_dim.38
  38.9 17.6 %all-to-all-start = ((f32[64,2,192]{2,1,0:T(2,128)}), f32[64,2,192]{2,1,0:T(2,128)S(1)}, u32[]{:S(2)}, u32[]{:S(2)}) async-start(f32[64,2,192]{2,1,0:T(2,128)} %broadcast_in_dim.38), calls=%async_computation | async-start | bytes 262144 | tf_op jit(solution)/shard_map/all_to_all | solution.py:22
  56.5 1.2 %fusion.15 = f32[1,10,64,2,128]{4,2,3,1,0:T(8,128)S(1)} fusion(f32[1,10,64,2,128]{4,2,3,1,0:T(8,128)S(1)} %fusion.13, bf16[1,6,2,64,320]{4,3,2,1,0:T(8,128)(2,1)} %copy-done.1, bf16[6,64,2,128]{3,2,1,0:T(2,128)(2,1)S(1)} %reshape.1130), kind=kOutput, calls=%fused_computation.39 | convolution fusion | flops 12681216 | bytes 1179648 | tf_op jit(solution)/shard_map/snhck,sncha->snkha/dot_general | solution.py:131
  58.3 0.9 %slice.550 = f32[1,256,256]{2,0,1:T(1,128)} slice(f32[1,640,256]{2,0,1:T(1,128)S(1)} %bitcast.220), slice={[0:1], [0:256], [0:256]} | slice | bytes 524288 | tf_op jit(solution)/shard_map/slice | solution.py:166
  59.2 1.3 %collective-permute-start.3 = (f32[1,256,256]{2,0,1:T(1,128)}, f32[1,256,256]{2,0,1:T(1,128)S(1)}, u32[]{:S(2)}, u32[]{:S(2)}) collective-permute-start(f32[1,256,256]{2,0,1:T(1,128)} %slice.550), channel_id=1, source_target_pairs={{8,0},{16,8},{24,16},{32,24},{40,32},{48,40},{56,48},{64,56},{72,6... | collective-permute-start | bytes 786440 | tf_op jit(solution)/shard_map/ppermute | solution.py:17
  60.4 7.5 %all-to-all-done = f32[64,2,192]{2,1,0:T(2,128)S(1)} async-done(((f32[64,2,192]{2,1,0:T(2,128)}), f32[64,2,192]{2,1,0:T(2,128)S(1)}, u32[]{:S(2)}, u32[]{:S(2)}) %all-to-all-start) | async-done | bytes 98336 | tf_op jit(solution)/shard_map/all_to_all | solution.py:22
  68.6 7.3 %all-to-all-start.1 = ((f32[8,2,192]{2,1,0:T(2,128)}), f32[8,2,192]{2,1,0:T(2,128)S(1)}, u32[]{:S(2)}, u32[]{:S(2)}) async-start(f32[8,2,192]{2,1,0:T(2,128)} %broadcast_in_dim.39), calls=%async_computation.1 | async-start | bytes 32768 | tf_op jit(solution)/shard_map/all_to_all | solution.py:22
  76.8 0.8 reshape.1140
  77.7 2.9 %all-to-all-done.1 = f32[8,2,192]{2,1,0:T(2,128)S(1)} async-done(((f32[8,2,192]{2,1,0:T(2,128)}), f32[8,2,192]{2,1,0:T(2,128)S(1)}, u32[]{:S(2)}, u32[]{:S(2)}) %all-to-all-start.1) | async-done | bytes 12320 | tf_op jit(solution)/shard_map/all_to_all | solution.py:22
  81.2 1.3 %fusion.24 = bf16[1,384,256]{2,0,1:T(2,128)(2,1)S(1)} fusion(bf16[1,384,256]{2,0,1:T(2,128)(2,1)S(1)} %slice.537, f32[1,256,256]{2,0,1:T(1,128)} %collective-permute-done.2, f32[1,640,256]{2,0,1:T(1,128)S(1)} %bitcast.219), kind=kLoop, calls=%fused_computation.59 | loop fusion | flops 65536 | bytes 786432 | tf_op jit(solution)/shard_map/scatter-add | solution.py:167
  82.5 0.7 copy.173
  83.5 0.7 copy.174
  (95 shorter events, 13.9 us)
Async XLA Ops:
  0.6 11.2 %copy-start = (f32[2,192]{1,0:T(2,128)S(1)}, f32[2,192]{1,0:T(2,128)}, u32[]{:S(2)}) copy-start(f32[2,192]{1,0:T(2,128)} %param.32) | copy-start | bytes 4612
  1.6 12.8 %collective-permute-start = (bf16[1,256,256]{2,1,0:T(8,128)(2,1)S(1)}, bf16[1,256,256]{2,1,0:T(8,128)(2,1)S(1)}, u32[]{:S(2)}, u32[]{:S(2)}) collective-permute-start(bf16[1,256,256]{2,1,0:T(8,128)(2,1)S(1)} %slice.478), channel_id=1, source_target_pairs={{0,8},{8,16},{16,24},{24,32},{32,40},{40,48},{48,56},{56,64},{64,7... | collective-permute-start | bytes 393224 | tf_op jit(solution)/shard_map/ppermute | solution.py:17
  6.5 7.9 %copy-start.12 = (bf16[1,384,256]{2,1,0:T(8,128)(2,1)S(1)}, bf16[1,384,256]{2,1,0:T(8,128)(2,1)}, u32[]{:S(2)}) copy-start(bf16[1,384,256]{2,1,0:T(8,128)(2,1)} %param.30) | copy-start | bytes 589828
  6.5 8.9 %collective-permute-start.1 = (bf16[1,256,256]{2,1,0:T(8,128)(2,1)S(1)}, bf16[1,256,256]{2,1,0:T(8,128)(2,1)S(1)}, u32[]{:S(2)}, u32[]{:S(2)}) collective-permute-start(bf16[1,256,256]{2,1,0:T(8,128)(2,1)S(1)} %slice.486), channel_id=1, source_target_pairs={{0,8},{8,16},{16,24},{24,32},{32,40},{40,48},{48,56},{56,64},{64,7... | collective-permute-start | bytes 393224 | tf_op jit(solution)/shard_map/ppermute | solution.py:17
  9.9 4.5 %copy-start.17 = (s32[383]{0:T(512)}, s32[383]{0:T(512)S(1)}, u32[]{:S(2)}) copy-start(s32[383]{0:T(512)S(1)} %clamp_add_fusion) | copy-start | bytes 4600
  14.4 1.0 %copy-start.13 = (bf16[1,384,256]{2,1,0:T(8,128)(2,1)S(1)}, bf16[1,384,256]{2,1,0:T(8,128)(2,1)}, u32[]{:S(2)}) copy-start(bf16[1,384,256]{2,1,0:T(8,128)(2,1)} %param.31) | copy-start | bytes 589828
  15.4 5.2 %copy-start.8 = (bf16[1,6,64,2,128]{4,3,2,1,0:T(2,128)(2,1)}, bf16[1,6,64,2,128]{4,3,2,1,0:T(2,128)(2,1)S(1)}, u32[]{:S(2)}) copy-start(bf16[1,6,64,2,128]{4,3,2,1,0:T(2,128)(2,1)S(1)} %get-tuple-element.167) | copy-start | bytes 589828
  15.4 5.5 %copy-start.6 = (bf16[1,6,64,2,128]{4,3,2,1,0:T(2,128)(2,1)}, bf16[1,6,64,2,128]{4,3,2,1,0:T(2,128)(2,1)S(1)}, u32[]{:S(2)}) copy-start(bf16[1,6,64,2,128]{4,3,2,1,0:T(2,128)(2,1)S(1)} %get-tuple-element.166) | copy-start | bytes 589828
  15.4 5.7 %copy-start.4 = (bf16[1,6,64,2,128]{4,3,2,1,0:T(2,128)(2,1)}, bf16[1,6,64,2,128]{4,3,2,1,0:T(2,128)(2,1)S(1)}, u32[]{:S(2)}) copy-start(bf16[1,6,64,2,128]{4,3,2,1,0:T(2,128)(2,1)S(1)} %get-tuple-element.165) | copy-start | bytes 589828
  15.4 5.9 %copy-start.2 = (bf16[1,6,64,2,128]{4,3,2,1,0:T(2,128)(2,1)}, bf16[1,6,64,2,128]{4,3,2,1,0:T(2,128)(2,1)S(1)}, u32[]{:S(2)}) copy-start(bf16[1,6,64,2,128]{4,3,2,1,0:T(2,128)(2,1)S(1)} %get-tuple-element.164) | copy-start | bytes 589828
  15.4 6.9 %copy-start.10 = (bf16[1,6,64,2,128]{4,3,2,1,0:T(2,128)(2,1)}, bf16[1,6,64,2,128]{4,3,2,1,0:T(2,128)(2,1)S(1)}, u32[]{:S(2)}) copy-start(bf16[1,6,64,2,128]{4,3,2,1,0:T(2,128)(2,1)S(1)} %get-tuple-element.163) | copy-start | bytes 589828
  25.5 1.7 %copy-start.14 = (f32[6,2,64]{2,1,0:T(2,128)}, f32[6,2,64]{2,1,0:T(2,128)S(1)}, u32[]{:S(2)}) copy-start(f32[6,2,64]{2,1,0:T(2,128)S(1)} %fusion.19) | copy-start | bytes 9220
  27.9 1.4 %copy-start.9 = (bf16[1,6,64,2,128]{4,3,2,1,0:T(2,128)(2,1)S(1)}, bf16[1,6,64,2,128]{4,3,2,1,0:T(2,128)(2,1)}, u32[]{:S(2)}) copy-start(bf16[1,6,64,2,128]{4,3,2,1,0:T(2,128)(2,1)} %copy-done.8) | copy-start | bytes 589828
  29.3 7.4 %copy-start.1 = (bf16[1,6,2,64,320]{4,3,2,1,0:T(8,128)(2,1)}, bf16[1,6,2,64,320]{4,3,2,1,0:T(8,128)(2,1)S(1)}, u32[]{:S(2)}) copy-start(bf16[1,6,2,64,320]{4,3,2,1,0:T(8,128)(2,1)S(1)} %get-tuple-element.162) | copy-start | bytes 1474564
  29.3 1.1 %copy-start.7 = (bf16[1,6,64,2,128]{4,3,2,1,0:T(2,128)(2,1)S(1)}, bf16[1,6,64,2,128]{4,3,2,1,0:T(2,128)(2,1)}, u32[]{:S(2)}) copy-start(bf16[1,6,64,2,128]{4,3,2,1,0:T(2,128)(2,1)} %copy-done.6) | copy-start | bytes 589828
  29.5 1.2 %copy-start.5 = (bf16[1,6,64,2,128]{4,3,2,1,0:T(2,128)(2,1)S(1)}, bf16[1,6,64,2,128]{4,3,2,1,0:T(2,128)(2,1)}, u32[]{:S(2)}) copy-start(bf16[1,6,64,2,128]{4,3,2,1,0:T(2,128)(2,1)} %copy-done.4) | copy-start | bytes 589828
  30.4 0.9 %copy-start.3 = (bf16[1,6,64,2,128]{4,3,2,1,0:T(2,128)(2,1)S(1)}, bf16[1,6,64,2,128]{4,3,2,1,0:T(2,128)(2,1)}, u32[]{:S(2)}) copy-start(bf16[1,6,64,2,128]{4,3,2,1,0:T(2,128)(2,1)} %copy-done.2) | copy-start | bytes 589828
  34.4 46.7 %collective-permute-start.2 = (f32[1,256,256]{2,0,1:T(1,128)}, f32[1,256,256]{2,0,1:T(1,128)}, u32[]{:S(2)}, u32[]{:S(2)}) collective-permute-start(f32[1,256,256]{2,0,1:T(1,128)} %slice.539), channel_id=1, source_target_pairs={{8,0},{16,8},{24,16},{32,24},{40,32},{48,40},{56,48},{64,56},{72,6... | collective-permute-start | bytes 786440 | tf_op jit(solution)/shard_map/ppermute | solution.py:17
  36.4 0.7 copy-start.15
  36.4 0.7 copy-start.16
  37.1 0.9 %copy-start.18 = (s32[383]{0:T(512)S(1)}, s32[383]{0:T(512)}, u32[]{:S(2)}) copy-start(s32[383]{0:T(512)} %copy-done.17) | copy-start | bytes 4600
  38.9 29.0 %all-to-all-start = ((f32[64,2,192]{2,1,0:T(2,128)}), f32[64,2,192]{2,1,0:T(2,128)S(1)}, u32[]{:S(2)}, u32[]{:S(2)}) async-start(f32[64,2,192]{2,1,0:T(2,128)} %broadcast_in_dim.38), calls=%async_computation | async-start | bytes 262144 | tf_op jit(solution)/shard_map/all_to_all | solution.py:22
  57.7 18.1 %copy-start.11 = (bf16[1,6,64,2,128]{4,3,2,1,0:T(2,128)(2,1)S(1)}, bf16[1,6,64,2,128]{4,3,2,1,0:T(2,128)(2,1)}, u32[]{:S(2)}) copy-start(bf16[1,6,64,2,128]{4,3,2,1,0:T(2,128)(2,1)} %copy-done.10) | copy-start | bytes 589828
  59.2 24.0 %collective-permute-start.3 = (f32[1,256,256]{2,0,1:T(1,128)}, f32[1,256,256]{2,0,1:T(1,128)S(1)}, u32[]{:S(2)}, u32[]{:S(2)}) collective-permute-start(f32[1,256,256]{2,0,1:T(1,128)} %slice.550), channel_id=1, source_target_pairs={{8,0},{16,8},{24,16},{32,24},{40,32},{48,40},{56,48},{64,56},{72,6... | collective-permute-start | bytes 786440 | tf_op jit(solution)/shard_map/ppermute | solution.py:17
  68.6 11.9 %all-to-all-start.1 = ((f32[8,2,192]{2,1,0:T(2,128)}), f32[8,2,192]{2,1,0:T(2,128)S(1)}, u32[]{:S(2)}, u32[]{:S(2)}) async-start(f32[8,2,192]{2,1,0:T(2,128)} %broadcast_in_dim.39), calls=%async_computation.1 | async-start | bytes 32768 | tf_op jit(solution)/shard_map/all_to_all | solution.py:22
where the time goes:
time: 84.8 us; the launch traced here: 84.2 us
  starting transfers between devices  34.8 us (41%)
  local copies, waits for them, and re-layouts  20.8 us (25%)
  matrix products  12.3 us (15%)
  waiting for transfers between devices  10.3 us (12%)
  other arithmetic  4.67 us (6%)
  between operations  1.29 us (2%)
    all_to_all x2, starting transfers between devices, copy_for_each(): return lax.all_to_all(copies, axis, split_axis=0, concat_axis=0, tiled=True)  24.8 us
    all_to_all x2, waiting for transfers between devices, copy_for_each(): return lax.all_to_all(copies, axis, split_axis=0, concat_axis=0, tiled=True)  10.3 us
    ppermute x4, starting transfers between devices, from_behind(): lax.ppermute(value, axis, [(source, source + steps) for source in range(l...  9.92 us
    dot_general x5, matrix products, band_core(): jnp.einsum('sncha,snkha->snhck', g_segs, v_band[:, offset:offset + seg_co...  4.16 us
    unnamed x40, local copies, waits for them, and re-layouts  2.63 us
    dot_general x5, matrix products, band_core(): jnp.einsum('sncha,snkha->snhck', q_segs, k_band[:, offset:offset + seg_co...  2.6 us
    dot_general x5, matrix products, band_core(): jnp.einsum('snhck,sncha->snkha', prob_part, g_segs, preferred_element_typ...  2.47 us
    another operation x2, local copies, waits for them, and re-layouts  1.96 us
  transfers between devices with their start and end apart: 6, of which 2 were waited for; matrix products, arithmetic and copies ran while one was open for 20% of the time, Pallas kernels for 0%

commit v1 on v0

v1 whole, which is shorter than its diff:
```python
import jax
import jax.numpy as jnp
from jax import lax
from jax.experimental import pallas as pl
from jax.experimental.pallas import tpu as pltpu
from jax.sharding import PartitionSpec as P

HEAD_DIM = 128
SEG = 64
LEFT = 4
CLIP = 128
BUCKETS = 192
HEADS = 2
BLK = 128
SCALE = HEAD_DIM**-0.5
LOG2E = 1.4426950408889634
NEG = -1e30
F32 = jnp.float32
BF16 = jnp.bfloat16
VMEM = pl.BlockSpec(memory_space=pltpu.VMEM)
ANY = pl.BlockSpec(memory_space=pl.ANY)


def params(mib):
    return pltpu.CompilerParams(vmem_limit_bytes=mib << 20)


def dot(a, b, ca, cb):
    return lax.dot_general(a, b, (((ca,), (cb,)), ((), ())), preferred_element_type=F32)


def iotas():
    c = lax.broadcasted_iota(jnp.int32, (BLK, BLK), 0)
    r = lax.broadcasted_iota(jnp.int32, (BLK, BLK), 1)
    return c, r


def bias_blocks(row):
    c, r = iotas()
    row = row * LOG2E
    wide = jnp.broadcast_to(row, (8, 2 * BLK))
    mid = pltpu.roll(wide, 2 * BLK - (SEG - 1), 1)[:1, :BLK]
    low = pltpu.roll(wide, SEG + 1, 1)[:1, :BLK]
    top = wide[:1, BUCKETS - 1 : BUCKETS]
    mid = pltpu.roll(jnp.broadcast_to(mid, (BLK, BLK)), 0, 1, stride=1, stride_axis=0)
    low = pltpu.roll(jnp.broadcast_to(low, (BLK, BLK)), 0, 1, stride=1, stride_axis=0)
    t0 = jnp.where((c < SEG) & (r >= SEG), NEG, top)
    t1 = jnp.where(r >= c, top, mid)
    t2 = jnp.where(r >= c, mid, jnp.where((c >= SEG) & (r < SEG), NEG, low))
    return t0, t1, t2


def along_diagonals(x):
    acc = x[:8]
    for a in range(8, BLK, 8):
        acc = acc + pltpu.roll(x[a : a + 8], BLK - a, 1)
    row = lax.broadcasted_iota(jnp.int32, acc.shape, 0)
    for bit in (1, 2, 4):
        acc = jnp.where((row & bit) != 0, pltpu.roll(acc, BLK - bit, 1), acc)
    return jnp.sum(acc, axis=0, keepdims=True)


def skew_sum(d0, d1, d2):
    c, r = iotas()
    upper = r >= c
    mid = along_diagonals(jnp.where(upper, d2, d1))
    low = along_diagonals(jnp.where(upper, 0.0, d2))
    top = jnp.sum(jnp.where(upper, d1, 0.0) + d0, axis=0, keepdims=True)
    top = top + pltpu.roll(jnp.broadcast_to(top, (8, BLK)), SEG, 1)[:1]
    low = jnp.where(r[:1] < SEG, top, low)
    return jnp.concatenate([low, mid], axis=0)


def softmax_grad(scores, prob_grads):
    peak = scores[0].max(axis=0, keepdims=True)
    for s in scores[1:]:
        peak = jnp.maximum(peak, s.max(axis=0, keepdims=True))
    expo = [jnp.exp2(s - peak) for s in scores]
    total = sum(e.sum(axis=0, keepdims=True) for e in expo)
    mixed = sum((e * g).sum(axis=0, keepdims=True) for e, g in zip(expo, prob_grads))
    inv = 1.0 / total
    delta = mixed * inv
    prob = [e * inv for e in expo]
    grad = [p * (g - delta) for p, g in zip(prob, prob_grads)]
    return [p.astype(BF16) for p in prob], [(g * SCALE).astype(BF16) for g in grad], grad


def tails_body(k_ref, v_ref, o_ref, sem):
    rows = o_ref.shape[1]
    first = k_ref.shape[0] - rows
    copies = [
        pltpu.make_async_copy(ref.at[pl.ds(first, rows)], o_ref.at[i], sem.at[i])
        for i, ref in enumerate((k_ref, v_ref))
    ]
    for copy in copies:
        copy.start()
    for copy in copies:
        copy.wait()


def own_body(q_ref, k_ref, v_ref, g_ref, rb_ref, dq_ref, part_ref, pay_ref, tab_ref, rb_pad):
    rb_pad[...] = jnp.zeros_like(rb_pad)
    rb_pad[0:HEADS, 0:BUCKETS] = rb_ref[...]
    for h in range(HEADS):
        hs = slice(h * HEAD_DIM, (h + 1) * HEAD_DIM)
        table = bias_blocks(rb_pad[h : h + 1, :])
        for m in range(3):
            tab_ref[3 * h + m] = table[m]
        k = k_ref[:, hs]
        q = q_ref[2 * BLK :, hs]
        g = g_ref[2 * BLK :, hs]
        raw = dot(k, q, 1, 1)
        dp = dot(v_ref[:, hs], g, 1, 1)
        cut = [slice(m * BLK, (m + 1) * BLK) for m in range(3)]
        scores = [raw[cut[m]] * (SCALE * LOG2E) + table[m] for m in range(3)]
        prob, low, grad = softmax_grad(scores, [dp[cut[m]] for m in range(3)])
        low = jnp.concatenate(low, axis=0)
        dq_ref[:, hs] = dot(low, k, 0, 0).astype(BF16)
        part_ref[0, :, hs] = dot(low, q, 1, 0)
        part_ref[1, :, hs] = dot(jnp.concatenate(prob, axis=0), g, 1, 0)
        pay_ref[2 * h : 2 * h + 2, :] = skew_sum(*grad)


def rest_body(
    q_ref, k_ref, v_ref, g_ref, halo_ref, tab_ref, dq2_ref, part_in, pay_in,
    dq_ref, part_ref, back_ref, pay_ref,
):
    hidden = jnp.where(lax.axis_index("sp") == 0, NEG, 0.0).astype(F32)
    dq_ref[2 * BLK :, :] = dq2_ref[...]
    pay = []
    for h in range(HEADS):
        hs = slice(h * HEAD_DIM, (h + 1) * HEAD_DIM)
        table = [tab_ref[3 * h + m] for m in range(3)]
        ks = [halo_ref[0, :BLK, hs], halo_ref[0, BLK:, hs], k_ref[:BLK, hs], k_ref[BLK : 2 * BLK, hs]]
        vs = [halo_ref[1, :BLK, hs], halo_ref[1, BLK:, hs], v_ref[:BLK, hs], v_ref[BLK : 2 * BLK, hs]]
        q = q_ref[: 2 * BLK, hs]
        g = g_ref[: 2 * BLK, hs]
        lows, probs, sums = [], [], [None] * 3
        for p in range(2):
            rows = slice(p * BLK, (p + 1) * BLK)
            raw = dot(jnp.concatenate(ks[p : p + 3], axis=0), q[rows], 1, 1)
            dp = dot(jnp.concatenate(vs[p : p + 3], axis=0), g[rows], 1, 1)
            cut = [slice(m * BLK, (m + 1) * BLK) for m in range(3)]
            shift = [table[m] + hidden if p + m < 2 else table[m] for m in range(3)]
            scores = [raw[cut[m]] * (SCALE * LOG2E) + shift[m] for m in range(3)]
            prob, low, grad = softmax_grad(scores, [dp[cut[m]] for m in range(3)])
            dq_ref[rows, hs] = dot(
                jnp.concatenate(low, axis=0), jnp.concatenate(ks[p : p + 3], axis=0), 0, 0
            ).astype(BF16)
            lows.append(low)
            probs.append(prob)
            sums = [d if s is None else s + d for s, d in zip(sums, grad)]
        pay.append(skew_sum(*sums))
        for i, (w, x) in enumerate(((lows, q), (probs, g))):
            out = [
                dot(w[0][0], x[:BLK], 1, 0),
                dot(jnp.concatenate([w[0][1], w[1][0]], axis=1), x, 1, 0),
                dot(jnp.concatenate([w[0][2], w[1][1]], axis=1), x, 1, 0),
                dot(w[1][2], x[BLK:], 1, 0),
            ]
            back_ref[i, :BLK, hs] = out[0].astype(BF16)
            back_ref[i, BLK:, hs] = out[1].astype(BF16)
            part_ref[i, :BLK, hs] = part_in[i, :BLK, hs] + out[2]
            part_ref[i, BLK : 2 * BLK, hs] = part_in[i, BLK : 2 * BLK, hs] + out[3]
            part_ref[i, 2 * BLK :, hs] = part_in[i, 2 * BLK :, hs]
    total = jnp.concatenate(pay, axis=0) + pay_in[...]
    pay_ref[...] = jnp.broadcast_to(total[None], pay_ref.shape)


def join_body(part_ref, back_ref, dk_ref, dv_ref):
    for i, out in enumerate((dk_ref, dv_ref)):
        out[:BLK, :] = part_ref[i, :BLK, :].astype(BF16)
        out[BLK:, :] = (part_ref[i, BLK:, :] + back_ref[i].astype(F32)).astype(BF16)


def table_body(x_ref, o_ref):
    heads = o_ref.shape[0]
    low = x_ref[pl.ds(0, heads, stride=2), :]
    mid = x_ref[pl.ds(1, heads, stride=2), :]
    lane = lax.broadcasted_iota(jnp.int32, low.shape, 1)
    top = jnp.sum(jnp.where(lane < SEG, low, 0.0), axis=1, keepdims=True)
    mid = pltpu.roll(mid, SEG - 1, 1)
    first = jnp.where(lane < SEG - 1, pltpu.roll(low, SEG - 1, 1), mid)
    last = jnp.where(lane < SEG - 1, mid, top)
    o_ref[:, :BLK] = first
    o_ref[:, BLK:] = last[:, : BUCKETS - BLK]


def local(queries, keys, values, rel_bias, out_grad):
    _, rows, width = queries.shape
    reach = LEFT * SEG
    q, k, v, g = (a.reshape(rows, width) for a in (queries, keys, values, out_grad))
    count = lax.axis_size("sp")
    heads = lax.axis_size("tp")
    tails = pl.pallas_call(
        tails_body,
        out_shape=jax.ShapeDtypeStruct((2, reach, width), BF16),
        in_specs=[ANY, ANY],
        out_specs=VMEM,
        scratch_shapes=[pltpu.SemaphoreType.DMA((2,))],
        compiler_params=params(4),
        name="tails",
    )(k, v)
    halo = lax.ppermute(tails, "sp", [(s, s + 1) for s in range(count - 1)])
    dq2, part, pay, table = pl.pallas_call(
        own_body,
        out_shape=(
            jax.ShapeDtypeStruct((BLK, width), BF16),
            jax.ShapeDtypeStruct((2, rows, width), F32),
            jax.ShapeDtypeStruct((2 * HEADS, BLK), F32),
            jax.ShapeDtypeStruct((3 * HEADS, BLK, BLK), F32),
        ),
        in_specs=[VMEM] * 5,
        out_specs=(VMEM,) * 4,
        scratch_shapes=[pltpu.VMEM((8, 2 * BLK), F32)],
        compiler_params=params(8),
        name="own",
    )(q, k, v, g, rel_bias)
    dq, part, back, pay = pl.pallas_call(
        rest_body,
        out_shape=(
            jax.ShapeDtypeStruct((rows, width), BF16),
            jax.ShapeDtypeStruct((2, rows, width), F32),
            jax.ShapeDtypeStruct((2, reach, width), BF16),
            jax.ShapeDtypeStruct((count, 2 * HEADS, BLK), F32),
        ),
        in_specs=[VMEM] * 9,
        out_specs=(VMEM,) * 4,
        compiler_params=params(8),
        name="rest",
    )(q, k, v, g, halo, table, dq2, part, pay)
    pay = lax.all_to_all(pay, "sp", split_axis=0, concat_axis=0, tiled=True)
    back = lax.ppermute(back, "sp", [(s + 1, s) for s in range(count - 1)])
    pay = jnp.broadcast_to(jnp.sum(pay, axis=0), (heads, 2 * HEADS, BLK))
    pay = lax.all_to_all(pay, "tp", split_axis=0, concat_axis=0, tiled=True)
    dk, dv = pl.pallas_call(
        join_body,
        out_shape=(jax.ShapeDtypeStruct((rows, width), BF16),) * 2,
        in_specs=[VMEM] * 2,
        out_specs=(VMEM,) * 2,
        compiler_params=params(6),
        name="join",
    )(part, back)
    bias = pl.pallas_call(
        table_body,
        out_shape=jax.ShapeDtypeStruct((heads * HEADS, BUCKETS), F32),
        in_specs=[VMEM],
        out_specs=VMEM,
        compiler_params=params(4),
        name="table",
    )(pay.reshape(heads * 2 * HEADS, BLK))
    return tuple(a.reshape(queries.shape) for a in (dq, dk, dv)) + (bias,)


def solution(mesh):
    return jax.shard_map(
        local,
        mesh=mesh,
        in_specs=(
            P(None, "sp", "tp"),
            P(None, "sp", "tp"),
            P(None, "sp", "tp"),
            P("tp", None),
            P(None, "sp", "tp"),
        ),
        out_specs=(P(None, "sp", "tp"), P(None, "sp", "tp"), P(None, "sp", "tp"), P()),
        check_vma=False,
    )
```

time: 84.8 us -> 58 us (0.68)
  local copies, waits for them, and re-layouts: 20.8 us -> 3.4 us
  matrix products: 12.3 us -> 0 us
  Pallas kernels: 0 us -> 5.47 us
  waiting for transfers between devices: 10.3 us -> 15.3 us
  other arithmetic: 4.67 us -> 0.08 us
  starting transfers between devices: 34.8 us -> 32.7 us
    dot_general x27 -> x0, matrix products: 12.3 us -> none  [the longest x5 4.16 us: band_core(): jnp.einsum('sncha,snkha->snhck', g_segs, v_band[:, offset:offset + seg_co...]
    slice x9 -> x0, local copies, waits for them, and re-layouts: 6.16 us -> none  [the longest x1 0.92 us: local(): keys[:, tok_rows - reach:]]
    pallas_call x0 -> x5, Pallas kernels: none -> 5.47 us  [the longest x1 2.54 us: local(): pl.pallas_call(rest_body, out_shape=(jax.ShapeDtypeStruct((rows, width),...]
    ppermute x4 -> x2, starting transfers between devices: 9.92 us -> 5.33 us  [the longest x1 4.03 us: local(): halo = lax.ppermute(tails, 'sp', [(s, s + 1) for s in range(count - 1)])]
    concatenate x5 -> x0, local copies, waits for them, and re-layouts: 4.58 us -> none  [the longest x1 1.71 us: band_core(): prob_grad = jnp.concatenate(prob_parts, axis=-1)]
    all_to_all x2, waiting for transfers between devices: 10.3 us -> 14.1 us  [the longest x1 10.3 us: local(): pay = lax.all_to_all(pay, 'sp', split_axis=0, concat_axis=0, tiled=True)]
    all_to_all x2, starting transfers between devices: 24.8 us -> 27.4 us  [the longest x1 20.1 us: local(): pay = lax.all_to_all(pay, 'sp', split_axis=0, concat_axis=0, tiled=True)]
    reshape x7 -> x0, local copies, waits for them, and re-layouts: 2.47 us -> none  [the longest x1 0.81 us: local(): query_acc.astype(jnp.bfloat16).reshape(seq_count, tok_rows, row_width)]
  transfers between devices with their start and end apart: 6 -> 4, of which waited for: 2 -> 3; matrix products, arithmetic and copies ran while one was open for 20% -> 1% of each run, Pallas kernels for 0% -> 3%
where the time goes in v1:
time: 58 us; the launch traced here: 57.7 us
  starting transfers between devices  32.7 us (56%)
  waiting for transfers between devices  15.3 us (26%)
  Pallas kernels  5.47 us (9%)
  local copies, waits for them, and re-layouts  3.4 us (6%)
  between operations  0.73 us (1%)
    all_to_all x1, starting transfers between devices, local(): pay = lax.all_to_all(pay, 'sp', split_axis=0, concat_axis=0, tiled=True)  20.1 us
    all_to_all x1, waiting for transfers between devices, local(): pay = lax.all_to_all(pay, 'sp', split_axis=0, concat_axis=0, tiled=True)  10.3 us
    all_to_all x1, starting transfers between devices, local(): pay = lax.all_to_all(pay, 'tp', split_axis=0, concat_axis=0, tiled=True)  7.26 us
    ppermute x1, starting transfers between devices, local(): halo = lax.ppermute(tails, 'sp', [(s, s + 1) for s in range(count - 1)])  4.03 us
    all_to_all x1, waiting for transfers between devices, local(): pay = lax.all_to_all(pay, 'tp', split_axis=0, concat_axis=0, tiled=True)  3.86 us
    unnamed x16, local copies, waits for them, and re-layouts  2.79 us
    pallas_call x1, Pallas kernels, local(): pl.pallas_call(rest_body, out_shape=(jax.ShapeDtypeStruct((rows, width),...  2.54 us
    ppermute x1, starting transfers between devices, local(): back = lax.ppermute(back, 'sp', [(s + 1, s) for s in range(count - 1)])  1.29 us
  transfers between devices with their start and end apart: 4, of which 3 were waited for; matrix products, arithmetic and copies ran while one was open for 1% of the time, Pallas kernels for 3%

profile of v1, /device:TPU:1, one launch (start us, length us, event | category | flops | bytes accessed | tf_op | source)
XLA Modules:
  0.0 57.7 jit_solution(4834832841319415898)
XLA Ops:
  0.6 0.0 copy-start
  0.6 0.9 %copy-done = bf16[1,384,256]{2,1,0:T(8,128)(2,1)S(1)} copy-done((bf16[1,384,256]{2,1,0:T(8,128)(2,1)S(1)}, bf16[1,384,256]{2,1,0:T(8,128)(2,1)}, u32[]{:S(2)}) %copy-start) | copy-done | bytes 196632
  1.6 0.0 copy-start.2
  1.6 0.9 %copy-done.2 = bf16[1,384,256]{2,1,0:T(8,128)(2,1)S(1)} copy-done((bf16[1,384,256]{2,1,0:T(8,128)(2,1)S(1)}, bf16[1,384,256]{2,1,0:T(8,128)(2,1)}, u32[]{:S(2)}) %copy-start.2) | copy-done | bytes 196632
  2.5 0.0 copy-start.1
  2.5 0.0 copy-start.3
  2.5 0.0 copy-start.4
  2.5 0.3 tails.1
  2.9 0.0 copy-start.7
  2.9 4.0 %collective-permute-start = (bf16[2,256,256]{2,1,0:T(8,128)(2,1)S(1)}, bf16[2,256,256]{2,1,0:T(8,128)(2,1)S(1)}, u32[]{:S(2)}, u32[]{:S(2)}) collective-permute-start(bf16[2,256,256]{2,1,0:T(8,128)(2,1)S(1)} %tails.1), channel_id=1, source_target_pairs={{0,8},{8,16},{16,24},{24,32},{32,40},{40,48},{48,56},{56,64},{64,7... | collective-permute-start | bytes 786440 | tf_op jit(solution)/shard_map/ppermute | solution.py:204
  6.9 0.0 copy-done.1
  6.9 0.0 copy-done.3
  6.9 0.0 copy-done.4
  6.9 0.0 copy-done.7
  6.9 0.0 copy-start.5
  7.0 0.9 %copy-done.5 = bf16[1,384,256]{2,1,0:T(8,128)(2,1)S(1)} copy-done((bf16[1,384,256]{2,1,0:T(8,128)(2,1)S(1)}, bf16[1,384,256]{2,1,0:T(8,128)(2,1)}, u32[]{:S(2)}) %copy-start.5) | copy-done | bytes 196632
  7.9 0.0 copy-start.6
  7.9 1.1 %own.1 = (bf16[128,256]{1,0:T(8,128)(2,1)S(1)}, f32[2,384,256]{2,1,0:T(8,128)S(1)}, f32[4,128]{1,0:T(4,128)S(1)}, f32[6,128,128]{2,1,0:T(8,128)S(1)}) custom-call(bf16[384,256]{1,0:T(8,128)(2,1)S(1)} %bitcast.14, bf16[384,256]{1,0:T(8,128)(2,1)S(1)} %bitcast.9, bf16[384,256]{1,0:T(8,128)(2,1)S(1)} %bitcast.12, bf16[384,256]{1,0:T(8,128)(2,1)S(1)} %bitcast.16, ...), custom_call_target="tpu_custom_call" | custom-call | tf_op jit(solution)/shard_map/own/pallas_call | solution.py:205
  9.0 1.2 %collective-permute-done.halo_ref = bf16[2,256,256]{2,1,0:T(8,128)(2,1)S(1)} collective-permute-done((bf16[2,256,256]{2,1,0:T(8,128)(2,1)S(1)}, bf16[2,256,256]{2,1,0:T(8,128)(2,1)S(1)}, u32[]{:S(2)}, u32[]{:S(2)}) %collective-permute-start) | collective-permute-done | bytes 262176 | tf_op jit(solution)/shard_map/ppermute | solution.py:204
  10.2 0.0 copy-done.6
  10.2 2.5 %rest.1 = (bf16[384,256]{1,0:T(8,128)(2,1)}, f32[2,384,256]{2,1,0:T(8,128)S(1)}, bf16[2,256,256]{2,1,0:T(8,128)(2,1)S(1)}, f32[64,4,128]{2,1,0:T(4,128)}) custom-call(bf16[384,256]{1,0:T(8,128)(2,1)S(1)} %bitcast.15, bf16[384,256]{1,0:T(8,128)(2,1)S(1)} %bitcast.10, bf16[384,256]{1,0:T(8,128)(2,1)S(1)} %bitcast.13, bf16[384,256]{1,0:T(8,128)(2,1)S(1)} %bitcast.17, ...), custom_call_target="tpu_custom_call" | custom-call | tf_op jit(solution)/shard_map/rest/pallas_call | solution.py:219
  12.7 20.1 %all-to-all-start = ((f32[64,4,128]{2,1,0:T(4,128)}), f32[64,4,128]{2,1,0:T(4,128)S(1)}, u32[]{:S(2)}, u32[]{:S(2)}) async-start(f32[64,4,128]{2,1,0:T(4,128)} %get-tuple-element.23), calls=%async_computation | async-start | bytes 262144 | tf_op jit(solution)/shard_map/all_to_all | solution.py:232
  32.8 1.3 %collective-permute-start.1 = (bf16[2,256,256]{2,1,0:T(8,128)(2,1)S(1)}, bf16[2,256,256]{2,1,0:T(8,128)(2,1)S(1)}, u32[]{:S(2)}, u32[]{:S(2)}) collective-permute-start(bf16[2,256,256]{2,1,0:T(8,128)(2,1)S(1)} %get-tuple-element.20), channel_id=1, source_target_pairs={{8,0},{16,8},{24,16},{32,24},{40,32},{48,40},{56,48},{64,56},{72,6... | collective-permute-start | bytes 786440 | tf_op jit(solution)/shard_map/ppermute | solution.py:233
  34.1 10.3 %all-to-all-done = f32[64,4,128]{2,1,0:T(4,128)S(1)} async-done(((f32[64,4,128]{2,1,0:T(4,128)}), f32[64,4,128]{2,1,0:T(4,128)S(1)}, u32[]{:S(2)}, u32[]{:S(2)}) %all-to-all-start) | async-done | bytes 131104 | tf_op jit(solution)/shard_map/all_to_all | solution.py:232
  44.4 0.1 reduce_sum.9
  44.5 0.6 %broadcast_in_dim.3 = f32[8,4,128]{2,1,0:T(4,128)} broadcast(f32[4,128]{1,0:T(4,128)S(1)} %reduce_sum.9), dimensions={1,2} | broadcast | bytes 18432 | tf_op jit(solution)/shard_map/broadcast_in_dim | solution.py:234
  45.1 7.3 %all-to-all-start.1 = ((f32[8,4,128]{2,1,0:T(4,128)}), f32[8,4,128]{2,1,0:T(4,128)S(1)}, u32[]{:S(2)}, u32[]{:S(2)}) async-start(f32[8,4,128]{2,1,0:T(4,128)} %broadcast_in_dim.3), calls=%async_computation.1 | async-start | bytes 32768 | tf_op jit(solution)/shard_map/all_to_all | solution.py:235
  52.4 0.0 collective-permute-done.1.back_ref
  52.4 0.8 %join.1 = (bf16[384,256]{1,0:T(8,128)(2,1)}, bf16[384,256]{1,0:T(8,128)(2,1)}) custom-call(f32[2,384,256]{2,1,0:T(8,128)S(1)} %get-tuple-element.19.part_ref, bf16[2,256,256]{2,1,0:T(8,128)(2,1)S(1)} %collective-permute-done.1.back_ref), custom_call_target="tpu_custom_call" | custom-call | tf_op jit(solution)/shard_map/join/pallas_call | solution.py:236
  53.1 3.9 %all-to-all-done.1 = f32[8,4,128]{2,1,0:T(4,128)S(1)} async-done(((f32[8,4,128]{2,1,0:T(4,128)}), f32[8,4,128]{2,1,0:T(4,128)S(1)}, u32[]{:S(2)}, u32[]{:S(2)}) %all-to-all-start.1) | async-done | bytes 16416 | tf_op jit(solution)/shard_map/all_to_all | solution.py:235
  57.0 0.7 %table.1 = f32[16,192]{1,0:T(8,128)} custom-call(f32[32,128]{1,0:T(8,128)S(1)} %bitcast.18), custom_call_target="tpu_custom_call" | custom-call | tf_op jit(solution)/shard_map/table/pallas_call | solution.py:244
Async XLA Ops:
  0.6 0.9 %copy-start = (bf16[1,384,256]{2,1,0:T(8,128)(2,1)S(1)}, bf16[1,384,256]{2,1,0:T(8,128)(2,1)}, u32[]{:S(2)}) copy-start(bf16[1,384,256]{2,1,0:T(8,128)(2,1)} %param.6) | copy-start | bytes 589828
  1.6 0.9 %copy-start.2 = (bf16[1,384,256]{2,1,0:T(8,128)(2,1)S(1)}, bf16[1,384,256]{2,1,0:T(8,128)(2,1)}, u32[]{:S(2)}) copy-start(bf16[1,384,256]{2,1,0:T(8,128)(2,1)} %param.7) | copy-start | bytes 589828
  2.5 4.4 %copy-start.1 = (bf16[1,384,256]{2,1,0:T(8,128)(2,1)S(1)}, bf16[1,384,256]{2,1,0:T(8,128)(2,1)}, u32[]{:S(2)}) copy-start(bf16[1,384,256]{2,1,0:T(8,128)(2,1)} %param.6) | copy-start | bytes 589828
  2.5 4.4 %copy-start.3 = (bf16[1,384,256]{2,1,0:T(8,128)(2,1)S(1)}, bf16[1,384,256]{2,1,0:T(8,128)(2,1)}, u32[]{:S(2)}) copy-start(bf16[1,384,256]{2,1,0:T(8,128)(2,1)} %param.7) | copy-start | bytes 589828
  2.5 4.4 %copy-start.4 = (bf16[1,384,256]{2,1,0:T(8,128)(2,1)S(1)}, bf16[1,384,256]{2,1,0:T(8,128)(2,1)}, u32[]{:S(2)}) copy-start(bf16[1,384,256]{2,1,0:T(8,128)(2,1)} %param.5) | copy-start | bytes 589828
  2.9 4.1 %copy-start.7 = (f32[2,192]{1,0:T(2,128)S(1)}, f32[2,192]{1,0:T(2,128)}, u32[]{:S(2)}) copy-start(f32[2,192]{1,0:T(2,128)} %rb_ref.1) | copy-start | bytes 4612
  2.9 7.3 %collective-permute-start = (bf16[2,256,256]{2,1,0:T(8,128)(2,1)S(1)}, bf16[2,256,256]{2,1,0:T(8,128)(2,1)S(1)}, u32[]{:S(2)}, u32[]{:S(2)}) collective-permute-start(bf16[2,256,256]{2,1,0:T(8,128)(2,1)S(1)} %tails.1), channel_id=1, source_target_pairs={{0,8},{8,16},{16,24},{24,32},{32,40},{40,48},{48,56},{56,64},{64,7... | collective-permute-start | bytes 786440 | tf_op jit(solution)/shard_map/ppermute | solution.py:204
  6.9 0.9 %copy-start.5 = (bf16[1,384,256]{2,1,0:T(8,128)(2,1)S(1)}, bf16[1,384,256]{2,1,0:T(8,128)(2,1)}, u32[]{:S(2)}) copy-start(bf16[1,384,256]{2,1,0:T(8,128)(2,1)} %param.9) | copy-start | bytes 589828
  7.9 2.3 %copy-start.6 = (bf16[1,384,256]{2,1,0:T(8,128)(2,1)S(1)}, bf16[1,384,256]{2,1,0:T(8,128)(2,1)}, u32[]{:S(2)}) copy-start(bf16[1,384,256]{2,1,0:T(8,128)(2,1)} %param.9) | copy-start | bytes 589828
  12.7 31.7 %all-to-all-start = ((f32[64,4,128]{2,1,0:T(4,128)}), f32[64,4,128]{2,1,0:T(4,128)S(1)}, u32[]{:S(2)}, u32[]{:S(2)}) async-start(f32[64,4,128]{2,1,0:T(4,128)} %get-tuple-element.23), calls=%async_computation | async-start | bytes 262144 | tf_op jit(solution)/shard_map/all_to_all | solution.py:232
  32.8 19.5 %collective-permute-start.1 = (bf16[2,256,256]{2,1,0:T(8,128)(2,1)S(1)}, bf16[2,256,256]{2,1,0:T(8,128)(2,1)S(1)}, u32[]{:S(2)}, u32[]{:S(2)}) collective-permute-start(bf16[2,256,256]{2,1,0:T(8,128)(2,1)S(1)} %get-tuple-element.20), channel_id=1, source_target_pairs={{8,0},{16,8},{24,16},{32,24},{40,32},{48,40},{56,48},{64,56},{72,6... | collective-permute-start | bytes 786440 | tf_op jit(solution)/shard_map/ppermute | solution.py:233
  45.1 11.9 %all-to-all-start.1 = ((f32[8,4,128]{2,1,0:T(4,128)}), f32[8,4,128]{2,1,0:T(4,128)S(1)}, u32[]{:S(2)}, u32[]{:S(2)}) async-start(f32[8,4,128]{2,1,0:T(4,128)} %broadcast_in_dim.3), calls=%async_computation.1 | async-start | bytes 32768 | tf_op jit(solution)/shard_map/all_to_all | solution.py:235

commit v2 on v1

v2 whole, which is shorter than its diff:
```python
import functools

import jax
import jax.numpy as jnp
from jax import lax
from jax.experimental import pallas as pl
from jax.experimental.pallas import tpu as pltpu
from jax.sharding import Mesh, PartitionSpec as P

HEAD_DIM = 128
SEG = 64
LEFT = 4
CLIP = 128
BUCKETS = 192
HEADS = 2
BLK = 128
SCALE = HEAD_DIM**-0.5
LOG2E = 1.4426950408889634
NEG = -1e30
F32 = jnp.float32
BF16 = jnp.bfloat16
VMEM = pl.BlockSpec(memory_space=pltpu.VMEM)
HBM = pl.BlockSpec(memory_space=pltpu.HBM)
AXES = ("z", "y", "x", "c")


def dot(a, b, ca, cb):
    return lax.dot_general(a, b, (((ca,), (cb,)), ((), ())), preferred_element_type=F32)


def iotas():
    c = lax.broadcasted_iota(jnp.int32, (BLK, BLK), 0)
    r = lax.broadcasted_iota(jnp.int32, (BLK, BLK), 1)
    return c, r


def bias_blocks(row):
    c, r = iotas()
    row = row * LOG2E
    wide = jnp.broadcast_to(row, (8, 2 * BLK))
    mid = pltpu.roll(wide, 2 * BLK - (SEG - 1), 1)[:1, :BLK]
    low = pltpu.roll(wide, SEG + 1, 1)[:1, :BLK]
    top = wide[:1, BUCKETS - 1 : BUCKETS]
    mid = pltpu.roll(jnp.broadcast_to(mid, (BLK, BLK)), 0, 1, stride=1, stride_axis=0)
    low = pltpu.roll(jnp.broadcast_to(low, (BLK, BLK)), 0, 1, stride=1, stride_axis=0)
    t0 = jnp.where((c < SEG) & (r >= SEG), NEG, top)
    t1 = jnp.where(r >= c, top, mid)
    t2 = jnp.where(r >= c, mid, jnp.where((c >= SEG) & (r < SEG), NEG, low))
    return t0, t1, t2


def along_diagonals(x):
    acc = x[:8]
    for a in range(8, BLK, 8):
        acc = acc + pltpu.roll(x[a : a + 8], BLK - a, 1)
    row = lax.broadcasted_iota(jnp.int32, acc.shape, 0)
    for bit in (1, 2, 4):
        acc = jnp.where((row & bit) != 0, pltpu.roll(acc, BLK - bit, 1), acc)
    return jnp.sum(acc, axis=0, keepdims=True)


def skew_sum(d0, d1, d2):
    c, r = iotas()
    upper = r >= c
    mid = along_diagonals(jnp.where(upper, d2, d1))
    low = along_diagonals(jnp.where(upper, 0.0, d2))
    top = jnp.sum(jnp.where(upper, d1, 0.0) + d0, axis=0, keepdims=True)
    top = top + pltpu.roll(jnp.broadcast_to(top, (8, BLK)), SEG, 1)[:1]
    low = jnp.where(r[:1] < SEG, top, low)
    return jnp.concatenate([low, mid], axis=0)


def softmax_grad(expo, prob_grads, inv, delta):
    prob = [e * i for e, i in zip(expo, inv)]
    grad = [p * (g - delta) for p, g in zip(prob, prob_grads)]
    return [p.astype(BF16) for p in prob], [(g * SCALE).astype(BF16) for g in grad], grad


def peak_of(scores):
    return functools.reduce(jnp.maximum, scores).max(axis=0, keepdims=True)


def sum_of(blocks):
    return functools.reduce(jnp.add, blocks).sum(axis=0, keepdims=True)


def weights(scores, prob_grads):
    peak = peak_of(scores)
    expo = [jnp.exp2(s - peak) for s in scores]
    return expo, peak, sum_of(expo), sum_of([e * g for e, g in zip(expo, prob_grads)])


def cut(x):
    return [x[at : at + BLK] for at in range(0, x.shape[0], BLK)]


def stack(blocks):
    return jnp.concatenate(blocks, axis=0)


def head(h):
    return slice(h * HEAD_DIM, (h + 1) * HEAD_DIM)


def hidden_keys():
    first = (lax.axis_index("z") == 0) & (lax.axis_index("y") == 0)
    return jnp.where(first, NEG, 0.0).astype(F32)


def tails_body(k_ref, v_ref, near_ref, far_ref, sem):
    first = k_ref.shape[0] - 2 * BLK
    copies = [
        pltpu.make_async_copy(ref.at[pl.ds(first + at, BLK)], out.at[i], sem.at[2 * i + j])
        for i, ref in enumerate((k_ref, v_ref))
        for j, (out, at) in enumerate(((near_ref, BLK), (far_ref, 0)))
    ]
    for copy in copies:
        copy.start()
    for copy in copies:
        copy.wait()


def own_body(q_ref, k_ref, v_ref, g_ref, rb_ref, dq_ref, mid_ref, end_ref, pay_ref, tab_ref, rb_pad):
    rb_pad[...] = jnp.zeros_like(rb_pad)
    rb_pad[0:HEADS, 0:BUCKETS] = rb_ref[...]
    for h in range(HEADS):
        hs = head(h)
        table = bias_blocks(rb_pad[h : h + 1, :])
        for m in range(3):
            tab_ref[3 * h + m] = table[m]
        k = k_ref[:, hs]
        q = q_ref[2 * BLK :, hs]
        g = g_ref[2 * BLK :, hs]
        scores = [s * (SCALE * LOG2E) + t for s, t in zip(cut(dot(k, q, 1, 1)), table)]
        dp = cut(dot(v_ref[:, hs], g, 1, 1))
        expo, _, total, mixed = weights(scores, dp)
        inv = 1.0 / total
        prob, low, grad = softmax_grad(expo, dp, [inv] * 3, mixed * inv)
        low = stack(low)
        dq_ref[:, hs] = dot(low, k, 0, 0).astype(BF16)
        for i, out in enumerate((dot(low, q, 1, 0), dot(stack(prob), g, 1, 0))):
            mid_ref[i, :, hs] = out[: 2 * BLK]
            end_ref[i, :, hs] = out[2 * BLK :]
        pay_ref[2 * h : 2 * h + 2, :] = skew_sum(*grad)


def near_body(
    q_ref, k_ref, v_ref, g_ref, near_ref, tab_ref, mid_in, pay_in,
    dq_ref, part_ref, pay_ref, expo_ref, dp_ref, stat_ref,
):
    hidden = hidden_keys()
    for h in range(HEADS):
        hs = head(h)
        table = [tab_ref[3 * h + m] for m in range(3)]
        veiled = [table[0] + hidden, table[1] + hidden]
        k = stack([near_ref[0, :, hs], k_ref[: 2 * BLK, hs]])
        v = stack([near_ref[1, :, hs], v_ref[: 2 * BLK, hs]])
        q = q_ref[: 2 * BLK, hs]
        g = g_ref[: 2 * BLK, hs]
        raw = dot(k, q, 1, 1)
        dps = dot(v, g, 1, 1)
        scores = [s * (SCALE * LOG2E) + t for s, t in zip(cut(raw[:, BLK:]), [veiled[0]] + table[1:])]
        dp = cut(dps[:, BLK:])
        expo, _, total, mixed = weights(scores, dp)
        inv = 1.0 / total
        prob, low, grad = softmax_grad(expo, dp, [inv] * 3, mixed * inv)
        low = stack(low)
        dq_ref[:, hs] = dot(low, k, 0, 0).astype(BF16)
        for i, out in enumerate((dot(low, q[BLK:], 1, 0), dot(stack(prob), g[BLK:], 1, 0))):
            part_ref[i, :BLK, hs] = out[:BLK]
            part_ref[i, BLK:, hs] = out[BLK:] + mid_in[i, :, hs]
        pay_ref[2 * h : 2 * h + 2, :] = skew_sum(*grad) + pay_in[2 * h : 2 * h + 2, :]
        scores = [s * (SCALE * LOG2E) + t for s, t in zip(cut(raw[: 2 * BLK, :BLK]), [veiled[1], table[2]])]
        dp = cut(dps[: 2 * BLK, :BLK])
        expo, peak, total, mixed = weights(scores, dp)
        for i in range(2):
            expo_ref[2 * h + i] = expo[i]
            dp_ref[2 * h + i] = dp[i]
        for i, x in enumerate((peak, total, mixed)):
            stat_ref[3 * h + i : 3 * h + i + 1, :] = x


def far_body(
    q_ref, g_ref, far_ref, tab_ref, pay_in, expo_ref, dp_ref, stat_ref, pay_ref, prob_ref, low_ref
):
    hidden = hidden_keys()
    pay = []
    for h in range(HEADS):
        hs = head(h)
        score = dot(far_ref[0, :, hs], q_ref[:BLK, hs], 1, 1) * (SCALE * LOG2E) + (tab_ref[3 * h] + hidden)
        dp = dot(far_ref[1, :, hs], g_ref[:BLK, hs], 1, 1)
        peak, total, mixed = (stat_ref[3 * h + i : 3 * h + i + 1, :] for i in range(3))
        top = jnp.maximum(peak, score.max(axis=0, keepdims=True))
        expo = jnp.exp2(score - top)
        fade = jnp.exp2(peak - top)
        inv = 1.0 / (total * fade + sum_of([expo]))
        delta = (mixed * fade + sum_of([expo * dp])) * inv
        fade = fade * inv
        expos = [expo, expo_ref[2 * h], expo_ref[2 * h + 1]]
        dps = [dp, dp_ref[2 * h], dp_ref[2 * h + 1]]
        prob, low, grad = softmax_grad(expos, dps, [inv, fade, fade], delta)
        pay.append(skew_sum(*grad))
        for m in range(3):
            prob_ref[h, m * BLK : (m + 1) * BLK, :] = prob[m]
            low_ref[h, m * BLK : (m + 1) * BLK, :] = low[m]
    total = jnp.concatenate(pay, axis=0) + pay_in[...]
    pay_ref[...] = jnp.broadcast_to(total[None], pay_ref.shape)


def first_body(
    q_ref, k_ref, g_ref, near_ref, far_ref, part_ref, prob_ref, low_ref, dq1_ref, dq2_ref,
    dq_ref, back_ref, done_ref,
):
    dq_ref[BLK : 2 * BLK, :] = dq1_ref[...]
    dq_ref[2 * BLK :, :] = dq2_ref[...]
    for h in range(HEADS):
        hs = head(h)
        low = low_ref[h]
        keys = stack([far_ref[0, :, hs], near_ref[0, :, hs], k_ref[:BLK, hs]])
        dq_ref[:BLK, hs] = dot(low, keys, 0, 0).astype(BF16)
        outs = (dot(low, q_ref[:BLK, hs], 1, 0), dot(prob_ref[h], g_ref[:BLK, hs], 1, 0))
        for i, out in enumerate(outs):
            back_ref[i, :BLK, hs] = out[:BLK].astype(BF16)
            back_ref[i, BLK:, hs] = (out[BLK : 2 * BLK] + part_ref[i, :BLK, hs]).astype(BF16)
            done_ref[i, :, hs] = (out[2 * BLK :] + part_ref[i, BLK : 2 * BLK, hs]).astype(BF16)


def join_body(part_ref, end_ref, done_ref, back_ref, dk_ref, dv_ref):
    for i, out in enumerate((dk_ref, dv_ref)):
        out[:BLK, :] = done_ref[i]
        out[BLK : 2 * BLK, :] = (part_ref[i, 2 * BLK :, :] + back_ref[i, :BLK, :].astype(F32)).astype(BF16)
        out[2 * BLK :, :] = (end_ref[i] + back_ref[i, BLK:, :].astype(F32)).astype(BF16)


def table_body(x_ref, o_ref, sum_ref):
    heads = o_ref.shape[0]
    sum_ref[...] = jnp.sum(x_ref[...], axis=0)
    low = sum_ref[pl.ds(0, heads, stride=2), :]
    mid = sum_ref[pl.ds(1, heads, stride=2), :]
    lane = lax.broadcasted_iota(jnp.int32, low.shape, 1)
    top = jnp.sum(jnp.where(lane < SEG, low, 0.0), axis=1, keepdims=True)
    mid = pltpu.roll(mid, SEG - 1, 1)
    first = jnp.where(lane < SEG - 1, pltpu.roll(low, SEG - 1, 1), mid)
    last = jnp.where(lane < SEG - 1, mid, top)
    o_ref[:, :BLK] = first
    o_ref[:, BLK:] = last[:, : BUCKETS - BLK]


def call(body, name, outs, args, spaces=None, scratch=(), mib=8):
    return pl.pallas_call(
        body,
        out_shape=tuple(jax.ShapeDtypeStruct(*o) for o in outs),
        in_specs=spaces or [VMEM] * len(args),
        out_specs=(VMEM,) * len(outs),
        scratch_shapes=scratch,
        compiler_params=pltpu.CompilerParams(vmem_limit_bytes=mib << 20),
        name=name,
    )(*args)


def exchange(x, axes):
    return lax.all_to_all(x, axes, split_axis=0, concat_axis=0, tiled=True)


def local(queries, keys, values, rel_bias, out_grad):
    _, rows, width = queries.shape
    q, k, v, g = (a.reshape(rows, width) for a in (queries, keys, values, out_grad))
    size = {a: lax.axis_size(a) for a in AXES}
    count = size["z"] * size["y"]
    pair = (2, BLK, width)
    near, far = call(
        tails_body, "tails", [(pair, BF16)] * 2, (k, v), [HBM] * 2, [pltpu.SemaphoreType.DMA((4,))], 4
    )
    ahead = [(s, s + 1) for s in range(count - 1)]
    near = lax.ppermute(near, ("z", "y"), ahead)
    far = lax.ppermute(far, ("z", "y"), ahead)
    dq2, mid, end, pay, table = call(
        own_body,
        "own",
        [
            ((BLK, width), BF16),
            ((2, 2 * BLK, width), F32),
            (pair, F32),
            ((2 * HEADS, BLK), F32),
            ((3 * HEADS, BLK, BLK), F32),
        ],
        (q, k, v, g, rel_bias),
        scratch=[pltpu.VMEM((8, 2 * BLK), F32)],
    )
    dq1, part, pay, expo, dp, stat = call(
        near_body,
        "near",
        [
            ((BLK, width), BF16),
            ((2, 3 * BLK, width), F32),
            ((2 * HEADS, BLK), F32),
            ((2 * HEADS, BLK, BLK), F32),
            ((2 * HEADS, BLK, BLK), F32),
            ((8, BLK), F32),
        ],
        (q, k, v, g, near, table, mid, pay),
    )
    group = size["y"] * size["c"]
    pay, prob, low = call(
        far_body,
        "far",
        [
            ((group, 2 * HEADS, BLK), F32),
            ((HEADS, 3 * BLK, BLK), BF16),
            ((HEADS, 3 * BLK, BLK), BF16),
        ],
        (q, g, far, table, pay, expo, dp, stat),
    )
    pay = exchange(pay, ("y", "c"))
    dq, back, done = call(
        first_body,
        "first",
        [((rows, width), BF16), ((2, 2 * BLK, width), BF16), (pair, BF16)],
        (q, k, g, near, far, part, prob, low, dq1, dq2),
    )
    back = lax.ppermute(back, ("z", "y"), [(s + 1, s) for s in range(count - 1)])
    pay = pay.reshape(size["y"], size["c"] * 2 * HEADS, BLK).sum(axis=0)
    pay = jnp.broadcast_to(pay, (size["z"] * size["x"], *pay.shape))
    pay = exchange(pay, ("z", "x"))
    dk, dv = call(join_body, "join", [((rows, width), BF16)] * 2, (part, end, done, back), mib=6)
    shape = (size["x"] * size["c"] * 2 * HEADS, BLK)
    (bias,) = call(
        table_body,
        "table",
        [((shape[0] // 2, BUCKETS), F32)],
        (pay.reshape(size["z"], *shape),),
        scratch=[pltpu.VMEM(shape, F32)],
        mib=4,
    )
    return tuple(a.reshape(queries.shape) for a in (dq, dk, dv)) + (bias,)


def solution(mesh):
    sp, tp = mesh.devices.shape
    split = Mesh(mesh.devices.reshape(8, sp // 8, tp // 2, 2), AXES)
    rows = P(None, ("z", "y"), ("x", "c"))
    return jax.shard_map(
        local,
        mesh=split,
        in_specs=(rows, rows, rows, P(("x", "c"), None), rows),
        out_specs=(rows, rows, rows, P()),
        check_vma=False,
    )
```

time: 58 us -> 55.3 us (0.953)
  starting transfers between devices: 32.7 us -> 29.7 us
  waiting for transfers between devices: 15.3 us -> 13.7 us
  local copies, waits for them, and re-layouts: 3.4 us -> 4.4 us
  Pallas kernels: 5.47 us -> 6.44 us
    all_to_all x2, starting transfers between devices: 27.4 us -> 21.1 us  [exchange(): return lax.all_to_all(x, axes, split_axis=0, concat_axis=0, tiled=True)]
    ppermute x2 -> x3, starting transfers between devices: 5.33 us -> 8.51 us  [the longest x1 4.03 us: local(): near = lax.ppermute(near, ('z', 'y'), ahead)]
    ppermute x2 -> x3, waiting for transfers between devices: 1.21 us -> 0.01 us  [the longest x1 0.01 us: local(): near = lax.ppermute(near, ('z', 'y'), ahead)]
    pallas_call x5 -> x7, Pallas kernels: 5.47 us -> 6.44 us  [call(): pl.pallas_call(body, out_shape=tuple((jax.ShapeDtypeStruct(*o) for o in o...]
    unnamed x16, local copies, waits for them, and re-layouts: 2.79 us -> 3.71 us
  transfers between devices with their start and end apart: 4 -> 5, of which waited for: 3 -> 2; matrix products, arithmetic and copies ran while one was open for 1% -> 1% of each run, Pallas kernels for 3% -> 7%
where the time goes in v2:
time: 55.3 us; the launch traced here: 54.9 us
  starting transfers between devices  29.7 us (54%)
  waiting for transfers between devices  13.7 us (25%)
  Pallas kernels  6.44 us (12%)
  local copies, waits for them, and re-layouts  4.4 us (8%)
  between operations  0.76 us (1%)
    all_to_all x2, starting transfers between devices, exchange(): return lax.all_to_all(x, axes, split_axis=0, concat_axis=0, tiled=True)  21.1 us
    all_to_all x2, waiting for transfers between devices, exchange(): return lax.all_to_all(x, axes, split_axis=0, concat_axis=0, tiled=True)  13.7 us
    pallas_call x7, Pallas kernels, call(): pl.pallas_call(body, out_shape=tuple((jax.ShapeDtypeStruct(*o) for o in o...  6.44 us
    ppermute x1, starting transfers between devices, local(): near = lax.ppermute(near, ('z', 'y'), ahead)  4.03 us
    unnamed x16, local copies, waits for them, and re-layouts  3.71 us
    ppermute x1, starting transfers between devices, local(): far = lax.ppermute(far, ('z', 'y'), ahead)  3.2 us
    ppermute x1, starting transfers between devices, local(): lax.ppermute(back, ('z', 'y'), [(s + 1, s) for s in range(count - 1)])  1.28 us
  transfers between devices with their start and end apart: 5, of which 2 were waited for; matrix products, arithmetic and copies ran while one was open for 1% of the time, Pallas kernels for 7%

profile of v2, /device:TPU:1, one launch (start us, length us, event | category | flops | bytes accessed | tf_op | source)
XLA Modules:
  0.0 54.9 jit_solution(1983886045079898998)
XLA Ops:
  0.6 0.0 copy-start
  0.6 0.9 %copy-done = bf16[1,384,256]{2,1,0:T(8,128)(2,1)S(1)} copy-done((bf16[1,384,256]{2,1,0:T(8,128)(2,1)S(1)}, bf16[1,384,256]{2,1,0:T(8,128)(2,1)}, u32[]{:S(2)}) %copy-start) | copy-done | bytes 196632
  1.6 0.0 copy-start.5
  1.6 0.9 %copy-done.5 = bf16[1,384,256]{2,1,0:T(8,128)(2,1)S(1)} copy-done((bf16[1,384,256]{2,1,0:T(8,128)(2,1)S(1)}, bf16[1,384,256]{2,1,0:T(8,128)(2,1)}, u32[]{:S(2)}) %copy-start.5) | copy-done | bytes 196632
  2.5 0.0 copy-start.1
  2.5 0.4 tails.1
  2.9 4.0 %collective-permute-start = (bf16[2,128,256]{2,1,0:T(8,128)(2,1)S(1)}, bf16[2,128,256]{2,1,0:T(8,128)(2,1)S(1)}, u32[]{:S(2)}, u32[]{:S(2)}) collective-permute-start(bf16[2,128,256]{2,1,0:T(8,128)(2,1)S(1)} %get-tuple-element.25), channel_id=1, source_target_pairs={{0,8},{8,16},{16,24},{24,32},{32,40},{40,48},{48,56},{56,64},{64,7... | collective-permute-start | bytes 393224 | tf_op jit(solution)/shard_map/ppermute | solution.py:275
  6.9 0.0 copy-start.7
  6.9 3.2 %collective-permute-start.1 = (bf16[2,128,256]{2,1,0:T(8,128)(2,1)S(1)}, bf16[2,128,256]{2,1,0:T(8,128)(2,1)S(1)}, u32[]{:S(2)}, u32[]{:S(2)}) collective-permute-start(bf16[2,128,256]{2,1,0:T(8,128)(2,1)S(1)} %get-tuple-element.26), channel_id=1, source_target_pairs={{0,8},{8,16},{16,24},{24,32},{32,40},{40,48},{48,56},{56,64},{64,7... | collective-permute-start | bytes 393224 | tf_op jit(solution)/shard_map/ppermute | solution.py:276
  10.1 0.0 copy-done.1
  10.1 0.0 copy-done.2
  10.1 0.0 copy-done.7
  10.1 0.0 copy-start.3
  10.2 0.9 %copy-done.3 = bf16[1,384,256]{2,1,0:T(8,128)(2,1)S(1)} copy-done((bf16[1,384,256]{2,1,0:T(8,128)(2,1)S(1)}, bf16[1,384,256]{2,1,0:T(8,128)(2,1)}, u32[]{:S(2)}) %copy-start.3) | copy-done | bytes 196632
  11.1 0.9 %copy-done.6 = bf16[1,384,256]{2,1,0:T(8,128)(2,1)S(1)} copy-done((bf16[1,384,256]{2,1,0:T(8,128)(2,1)S(1)}, bf16[1,384,256]{2,1,0:T(8,128)(2,1)}, u32[]{:S(2)}) %copy-start.6) | copy-done | bytes 196632
  12.0 1.1 %own.1 = (bf16[128,256]{1,0:T(8,128)(2,1)S(1)}, f32[2,256,256]{2,1,0:T(8,128)S(1)}, f32[2,128,256]{2,1,0:T(8,128)S(1)}, f32[4,128]{1,0:T(4,128)S(1)}, f32[6,128,128]{2,1,0:T(8,128)S(1)}) custom-call(bf16[384,256]{1,0:T(8,128)(2,1)S(1)} %bitcast.15, bf16[384,256]{1,0:T(8,128)(2,1)S(1)} %bitcast.12, bf16[384,256]{1,0:T(8,128)(2,1)S(1)} %bitcast.24, ...), custom_call_target="tpu_custom_call" | custom-call | tf_op jit(solution)/shard_map/own/pallas_call | solution.py:250
  13.1 0.0 collective-permute-done.near_ref
  13.1 1.2 %near.1 = (bf16[128,256]{1,0:T(8,128)(2,1)S(1)}, f32[2,384,256]{2,1,0:T(8,128)S(1)}, f32[4,128]{1,0:T(4,128)S(1)}, f32[4,128,128]{2,1,0:T(8,128)S(1)}, f32[4,128,128]{2,1,0:T(8,128)S(1)}, /*index=5*/f32[8,128]{1,0:T(8,128)S(1)}) custom-call(bf16[384,256]{1,0:T(8,128)(2,1)S(1)} %bitcast.16, bf16[384,256]{1,0:T(8,128)(2,1)S(1)} %bitcast.13, ...), custom_call_target="tpu_custom_call" | custom-call | tf_op jit(solution)/shard_map/near/pallas_call | solution.py:250
  14.3 0.0 collective-permute-done.1.far_ref
  14.3 0.0 copy-start.4
  14.4 1.3 %far.1 = (f32[16,4,128]{2,1,0:T(4,128)}, bf16[2,384,128]{2,1,0:T(8,128)(2,1)S(1)}, bf16[2,384,128]{2,1,0:T(8,128)(2,1)S(1)}) custom-call(bf16[384,256]{1,0:T(8,128)(2,1)S(1)} %bitcast.17, bf16[384,256]{1,0:T(8,128)(2,1)S(1)} %bitcast.21, bf16[2,128,256]{2,1,0:T(8,128)(2,1)S(1)} %collective-permute-done.1.far_ref, ...), custom_call_target="tpu_custom_call" | custom-call | tf_op jit(solution)/shard_map/far/pallas_call | solution.py:250
  15.7 8.3 %all-to-all-start = ((f32[16,4,128]{2,1,0:T(4,128)}), f32[16,4,128]{2,1,0:T(4,128)S(1)}, u32[]{:S(2)}, u32[]{:S(2)}) async-start(f32[16,4,128]{2,1,0:T(4,128)} %get-tuple-element.45), calls=%async_computation | async-start | bytes 65536 | tf_op jit(solution)/shard_map/all_to_all | solution.py:262
  23.9 0.0 copy-done.4
  23.9 1.0 %first.1 = (bf16[384,256]{1,0:T(8,128)(2,1)}, bf16[2,256,256]{2,1,0:T(8,128)(2,1)S(1)}, bf16[2,128,256]{2,1,0:T(8,128)(2,1)S(1)}) custom-call(bf16[384,256]{1,0:T(8,128)(2,1)S(1)} %bitcast.18, bf16[384,256]{1,0:T(8,128)(2,1)S(1)} %bitcast.14, bf16[384,256]{1,0:T(8,128)(2,1)S(1)} %bitcast.22, bf16[2,128,256]{2,1,0:T(8,128)(2,1)S(1)} %collective-permute-done.near_ref, ...), custom_call_target="tpu_custom_call" | custom-call | tf_op jit(solution)/shard_map/first/pallas_call | solution.py:250
  24.9 1.3 %collective-permute-start.2 = (bf16[2,256,256]{2,1,0:T(8,128)(2,1)S(1)}, bf16[2,256,256]{2,1,0:T(8,128)(2,1)S(1)}, u32[]{:S(2)}, u32[]{:S(2)}) collective-permute-start(bf16[2,256,256]{2,1,0:T(8,128)(2,1)S(1)} %get-tuple-element.42), channel_id=1, source_target_pairs={{8,0},{16,8},{24,16},{32,24},{40,32},{48,40},{56,48},{64,56},{72,6... | collective-permute-start | bytes 786440 | tf_op jit(solution)/shard_map/ppermute | solution.py:321
  26.2 5.1 %all-to-all-done = f32[16,4,128]{2,1,0:T(4,128)S(1)} async-done(((f32[16,4,128]{2,1,0:T(4,128)}), f32[16,4,128]{2,1,0:T(4,128)S(1)}, u32[]{:S(2)}, u32[]{:S(2)}) %all-to-all-start) | async-done | bytes 32800 | tf_op jit(solution)/shard_map/all_to_all | solution.py:262
  31.3 0.7 %broadcast_in_dim.3 = f32[32,8,128]{2,1,0:T(8,128)} broadcast(f32[8,128]{1,0:T(8,128)S(1)} %bitcast_reduce_fusion), dimensions={1,2} | broadcast | bytes 135168 | tf_op jit(solution)/shard_map/broadcast_in_dim | solution.py:323
  32.0 12.9 %all-to-all-start.1 = ((f32[32,8,128]{2,1,0:T(8,128)}), f32[32,8,128]{2,1,0:T(8,128)S(1)}, u32[]{:S(2)}, u32[]{:S(2)}) async-start(f32[32,8,128]{2,1,0:T(8,128)} %broadcast_in_dim.3), calls=%async_computation.1 | async-start | bytes 262144 | tf_op jit(solution)/shard_map/all_to_all | solution.py:262
  44.9 0.0 collective-permute-done.2.back_ref
  44.9 0.8 %join.1 = (bf16[384,256]{1,0:T(8,128)(2,1)}, bf16[384,256]{1,0:T(8,128)(2,1)}) custom-call(f32[2,384,256]{2,1,0:T(8,128)S(1)} %get-tuple-element.30.part_ref, f32[2,128,256]{2,1,0:T(8,128)S(1)} %get-tuple-element.40.end_ref, bf16[2,128,256]{2,1,0:T(8,128)(2,1)S(1)} %get-tuple-element.41.done_ref, bf16[2,256,256]{2,1,0:T(8,128)(2,1)S(1)} %collective-permute-done.2.back_ref), custom_call_target="tpu_custom_call" | custom-call | tf_op jit(solution)/shard_map/join/pallas_call | solution.py:250
  45.7 8.6 %all-to-all-done.1 = f32[32,8,128]{2,1,0:T(8,128)S(1)} async-done(((f32[32,8,128]{2,1,0:T(8,128)}), f32[32,8,128]{2,1,0:T(8,128)S(1)}, u32[]{:S(2)}, u32[]{:S(2)}) %all-to-all-start.1) | async-done | bytes 131104 | tf_op jit(solution)/shard_map/all_to_all | solution.py:262
  54.2 0.7 %table.1 = f32[16,192]{1,0:T(8,128)} custom-call(f32[8,32,128]{2,1,0:T(8,128)S(1)} %bitcast.26), custom_call_target="tpu_custom_call" | custom-call | tf_op jit(solution)/shard_map/table/pallas_call | solution.py:250
  (3 shorter events, 0.0 us)
Async XLA Ops:
  0.6 0.9 %copy-start = (bf16[1,384,256]{2,1,0:T(8,128)(2,1)S(1)}, bf16[1,384,256]{2,1,0:T(8,128)(2,1)}, u32[]{:S(2)}) copy-start(bf16[1,384,256]{2,1,0:T(8,128)(2,1)} %param.6) | copy-start | bytes 589828
  1.6 0.9 %copy-start.5 = (bf16[1,384,256]{2,1,0:T(8,128)(2,1)S(1)}, bf16[1,384,256]{2,1,0:T(8,128)(2,1)}, u32[]{:S(2)}) copy-start(bf16[1,384,256]{2,1,0:T(8,128)(2,1)} %param.7) | copy-start | bytes 589828
  2.5 7.6 %copy-start.1 = (bf16[1,384,256]{2,1,0:T(8,128)(2,1)S(1)}, bf16[1,384,256]{2,1,0:T(8,128)(2,1)}, u32[]{:S(2)}) copy-start(bf16[1,384,256]{2,1,0:T(8,128)(2,1)} %param.6) | copy-start | bytes 589828
  2.5 7.6 %copy-start.2 = (bf16[1,384,256]{2,1,0:T(8,128)(2,1)S(1)}, bf16[1,384,256]{2,1,0:T(8,128)(2,1)}, u32[]{:S(2)}) copy-start(bf16[1,384,256]{2,1,0:T(8,128)(2,1)} %param.5) | copy-start | bytes 589828
  2.9 10.3 %collective-permute-start = (bf16[2,128,256]{2,1,0:T(8,128)(2,1)S(1)}, bf16[2,128,256]{2,1,0:T(8,128)(2,1)S(1)}, u32[]{:S(2)}, u32[]{:S(2)}) collective-permute-start(bf16[2,128,256]{2,1,0:T(8,128)(2,1)S(1)} %get-tuple-element.25), channel_id=1, source_target_pairs={{0,8},{8,16},{16,24},{24,32},{32,40},{40,48},{48,56},{56,64},{64,7... | collective-permute-start | bytes 393224 | tf_op jit(solution)/shard_map/ppermute | solution.py:275
  6.9 3.2 %copy-start.7 = (f32[2,192]{1,0:T(2,128)S(1)}, f32[2,192]{1,0:T(2,128)}, u32[]{:S(2)}) copy-start(f32[2,192]{1,0:T(2,128)} %rb_ref.1) | copy-start | bytes 4612
  6.9 7.4 %collective-permute-start.1 = (bf16[2,128,256]{2,1,0:T(8,128)(2,1)S(1)}, bf16[2,128,256]{2,1,0:T(8,128)(2,1)S(1)}, u32[]{:S(2)}, u32[]{:S(2)}) collective-permute-start(bf16[2,128,256]{2,1,0:T(8,128)(2,1)S(1)} %get-tuple-element.26), channel_id=1, source_target_pairs={{0,8},{8,16},{16,24},{24,32},{32,40},{40,48},{48,56},{56,64},{64,7... | collective-permute-start | bytes 393224 | tf_op jit(solution)/shard_map/ppermute | solution.py:276
  10.1 0.9 %copy-start.3 = (bf16[1,384,256]{2,1,0:T(8,128)(2,1)S(1)}, bf16[1,384,256]{2,1,0:T(8,128)(2,1)}, u32[]{:S(2)}) copy-start(bf16[1,384,256]{2,1,0:T(8,128)(2,1)} %param.9) | copy-start | bytes 589828
  11.1 0.9 %copy-start.6 = (bf16[1,384,256]{2,1,0:T(8,128)(2,1)S(1)}, bf16[1,384,256]{2,1,0:T(8,128)(2,1)}, u32[]{:S(2)}) copy-start(bf16[1,384,256]{2,1,0:T(8,128)(2,1)} %param.7) | copy-start | bytes 589828
  14.3 9.6 %copy-start.4 = (bf16[1,384,256]{2,1,0:T(8,128)(2,1)S(1)}, bf16[1,384,256]{2,1,0:T(8,128)(2,1)}, u32[]{:S(2)}) copy-start(bf16[1,384,256]{2,1,0:T(8,128)(2,1)} %param.9) | copy-start | bytes 589828
  15.7 15.7 %all-to-all-start = ((f32[16,4,128]{2,1,0:T(4,128)}), f32[16,4,128]{2,1,0:T(4,128)S(1)}, u32[]{:S(2)}, u32[]{:S(2)}) async-start(f32[16,4,128]{2,1,0:T(4,128)} %get-tuple-element.45), calls=%async_computation | async-start | bytes 65536 | tf_op jit(solution)/shard_map/all_to_all | solution.py:262
  24.9 20.0 %collective-permute-start.2 = (bf16[2,256,256]{2,1,0:T(8,128)(2,1)S(1)}, bf16[2,256,256]{2,1,0:T(8,128)(2,1)S(1)}, u32[]{:S(2)}, u32[]{:S(2)}) collective-permute-start(bf16[2,256,256]{2,1,0:T(8,128)(2,1)S(1)} %get-tuple-element.42), channel_id=1, source_target_pairs={{8,0},{16,8},{24,16},{32,24},{40,32},{48,40},{56,48},{64,56},{72,6... | collective-permute-start | bytes 786440 | tf_op jit(solution)/shard_map/ppermute | solution.py:321
  32.0 22.2 %all-to-all-start.1 = ((f32[32,8,128]{2,1,0:T(8,128)}), f32[32,8,128]{2,1,0:T(8,128)S(1)}, u32[]{:S(2)}, u32[]{:S(2)}) async-start(f32[32,8,128]{2,1,0:T(8,128)} %broadcast_in_dim.3), calls=%async_computation.1 | async-start | bytes 262144 | tf_op jit(solution)/shard_map/all_to_all | solution.py:262

commit v3 on v2

--- a/solution.py
+++ b/solution.py
@@ -268,8 +268,9 @@
     size = {a: lax.axis_size(a) for a in AXES}
     count = size["z"] * size["y"]
     pair = (2, BLK, width)
+    kept = tuple(pltpu.with_memory_space_constraint(a, pltpu.HBM) for a in (k, v))
     near, far = call(
-        tails_body, "tails", [(pair, BF16)] * 2, (k, v), [HBM] * 2, [pltpu.SemaphoreType.DMA((4,))], 4
+        tails_body, "tails", [(pair, BF16)] * 2, kept, [HBM] * 2, [pltpu.SemaphoreType.DMA((4,))], 4
     )
     ahead = [(s, s + 1) for s in range(count - 1)]
     near = lax.ppermute(near, ("z", "y"), ahead)

time: 55.3 us -> 54.1 us (0.978)
  local copies, waits for them, and re-layouts: 4.4 us -> 2.54 us
  Pallas kernels: 6.44 us -> 7.09 us
    unnamed x16 -> x12, local copies, waits for them, and re-layouts: 3.71 us -> 1.87 us
    pallas_call x7, Pallas kernels: 6.44 us -> 7.09 us  [call(): pl.pallas_call(body, out_shape=tuple((jax.ShapeDtypeStruct(*o) for o in o...]
  transfers between devices with their start and end apart: 5 -> 5, of which waited for: 2 -> 2; matrix products, arithmetic and copies ran while one was open for 1% -> 1% of each run, Pallas kernels for 7% -> 8%
where the time goes in v3:
time: 54.1 us; the launch traced here: 53.7 us
  starting transfers between devices  29.7 us (55%)
  waiting for transfers between devices  13.7 us (25%)
  Pallas kernels  7.09 us (13%)
  local copies, waits for them, and re-layouts  2.54 us (5%)
  between operations  0.77 us (1%)
    all_to_all x2, starting transfers between devices, exchange(): return lax.all_to_all(x, axes, split_axis=0, concat_axis=0, tiled=True)  21.1 us
    all_to_all x2, waiting for transfers between devices, exchange(): return lax.all_to_all(x, axes, split_axis=0, concat_axis=0, tiled=True)  13.7 us
    pallas_call x7, Pallas kernels, call(): pl.pallas_call(body, out_shape=tuple((jax.ShapeDtypeStruct(*o) for o in o...  7.09 us
    ppermute x1, starting transfers between devices, local(): near = lax.ppermute(near, ('z', 'y'), ahead)  4.03 us
    ppermute x1, starting transfers between devices, local(): far = lax.ppermute(far, ('z', 'y'), ahead)  3.2 us
    unnamed x12, local copies, waits for them, and re-layouts  1.87 us
    ppermute x1, starting transfers between devices, local(): lax.ppermute(back, ('z', 'y'), [(s + 1, s) for s in range(count - 1)])  1.28 us
  transfers between devices with their start and end apart: 5, of which 2 were waited for; matrix products, arithmetic and copies ran while one was open for 1% of the time, Pallas kernels for 8%

profile of v3, /device:TPU:1, one launch (start us, length us, event | category | flops | bytes accessed | tf_op | source)
XLA Modules:
  0.0 53.7 jit_solution(2988534136844006250)
XLA Ops:
  0.6 0.0 copy-start
  0.6 0.0 copy-start.1
  0.7 1.0 %tails.1 = (bf16[2,128,256]{2,1,0:T(8,128)(2,1)S(1)}, bf16[2,128,256]{2,1,0:T(8,128)(2,1)S(1)}) custom-call(bf16[384,256]{1,0:T(8,128)(2,1)} %bitcast.11, bf16[384,256]{1,0:T(8,128)(2,1)} %bitcast.23), custom_call_target="tpu_custom_call" | custom-call | tf_op jit(solution)/shard_map/tails/pallas_call | solution.py:250
  1.7 4.0 %collective-permute-start = (bf16[2,128,256]{2,1,0:T(8,128)(2,1)S(1)}, bf16[2,128,256]{2,1,0:T(8,128)(2,1)S(1)}, u32[]{:S(2)}, u32[]{:S(2)}) collective-permute-start(bf16[2,128,256]{2,1,0:T(8,128)(2,1)S(1)} %get-tuple-element.25), channel_id=1, source_target_pairs={{0,8},{8,16},{16,24},{24,32},{32,40},{40,48},{48,56},{56,64},{64,7... | collective-permute-start | bytes 393224 | tf_op jit(solution)/shard_map/ppermute | solution.py:276
  5.7 0.0 copy-start.5
  5.7 3.2 %collective-permute-start.1 = (bf16[2,128,256]{2,1,0:T(8,128)(2,1)S(1)}, bf16[2,128,256]{2,1,0:T(8,128)(2,1)S(1)}, u32[]{:S(2)}, u32[]{:S(2)}) collective-permute-start(bf16[2,128,256]{2,1,0:T(8,128)(2,1)S(1)} %get-tuple-element.26), channel_id=1, source_target_pairs={{0,8},{8,16},{16,24},{24,32},{32,40},{40,48},{48,56},{56,64},{64,7... | collective-permute-start | bytes 393224 | tf_op jit(solution)/shard_map/ppermute | solution.py:277
  8.9 0.0 copy-done
  8.9 0.0 copy-done.1
  9.0 0.0 copy-done.5
  9.0 0.0 copy-start.2
  9.0 0.9 %copy-done.2 = bf16[1,384,256]{2,1,0:T(8,128)(2,1)S(1)} copy-done((bf16[1,384,256]{2,1,0:T(8,128)(2,1)S(1)}, bf16[1,384,256]{2,1,0:T(8,128)(2,1)}, u32[]{:S(2)}) %copy-start.2) | copy-done | bytes 196632
  9.9 0.0 copy-start.4
  9.9 0.9 %copy-done.4 = bf16[1,384,256]{2,1,0:T(8,128)(2,1)S(1)} copy-done((bf16[1,384,256]{2,1,0:T(8,128)(2,1)S(1)}, bf16[1,384,256]{2,1,0:T(8,128)(2,1)}, u32[]{:S(2)}) %copy-start.4) | copy-done | bytes 196632
  10.8 1.1 %own.1 = (bf16[128,256]{1,0:T(8,128)(2,1)S(1)}, f32[2,256,256]{2,1,0:T(8,128)S(1)}, f32[2,128,256]{2,1,0:T(8,128)S(1)}, f32[4,128]{1,0:T(4,128)S(1)}, f32[6,128,128]{2,1,0:T(8,128)S(1)}) custom-call(bf16[384,256]{1,0:T(8,128)(2,1)S(1)} %bitcast.15, bf16[384,256]{1,0:T(8,128)(2,1)S(1)} %bitcast.12, bf16[384,256]{1,0:T(8,128)(2,1)S(1)} %bitcast.24, ...), custom_call_target="tpu_custom_call" | custom-call | tf_op jit(solution)/shard_map/own/pallas_call | solution.py:250
  11.9 0.0 collective-permute-done.near_ref
  11.9 1.2 %near.1 = (bf16[128,256]{1,0:T(8,128)(2,1)S(1)}, f32[2,384,256]{2,1,0:T(8,128)S(1)}, f32[4,128]{1,0:T(4,128)S(1)}, f32[4,128,128]{2,1,0:T(8,128)S(1)}, f32[4,128,128]{2,1,0:T(8,128)S(1)}, /*index=5*/f32[8,128]{1,0:T(8,128)S(1)}) custom-call(bf16[384,256]{1,0:T(8,128)(2,1)S(1)} %bitcast.16, bf16[384,256]{1,0:T(8,128)(2,1)S(1)} %bitcast.13, ...), custom_call_target="tpu_custom_call" | custom-call | tf_op jit(solution)/shard_map/near/pallas_call | solution.py:250
  13.1 0.0 collective-permute-done.1.far_ref
  13.2 0.0 copy-start.3
  13.2 1.3 %far.1 = (f32[16,4,128]{2,1,0:T(4,128)}, bf16[2,384,128]{2,1,0:T(8,128)(2,1)S(1)}, bf16[2,384,128]{2,1,0:T(8,128)(2,1)S(1)}) custom-call(bf16[384,256]{1,0:T(8,128)(2,1)S(1)} %bitcast.17, bf16[384,256]{1,0:T(8,128)(2,1)S(1)} %bitcast.21, bf16[2,128,256]{2,1,0:T(8,128)(2,1)S(1)} %collective-permute-done.1.far_ref, ...), custom_call_target="tpu_custom_call" | custom-call | tf_op jit(solution)/shard_map/far/pallas_call | solution.py:250
  14.5 8.3 %all-to-all-start = ((f32[16,4,128]{2,1,0:T(4,128)}), f32[16,4,128]{2,1,0:T(4,128)S(1)}, u32[]{:S(2)}, u32[]{:S(2)}) async-start(f32[16,4,128]{2,1,0:T(4,128)} %get-tuple-element.45), calls=%async_computation | async-start | bytes 65536 | tf_op jit(solution)/shard_map/all_to_all | solution.py:262
  22.7 0.0 copy-done.3
  22.7 1.0 %first.1 = (bf16[384,256]{1,0:T(8,128)(2,1)}, bf16[2,256,256]{2,1,0:T(8,128)(2,1)S(1)}, bf16[2,128,256]{2,1,0:T(8,128)(2,1)S(1)}) custom-call(bf16[384,256]{1,0:T(8,128)(2,1)S(1)} %bitcast.18, bf16[384,256]{1,0:T(8,128)(2,1)S(1)} %bitcast.14, bf16[384,256]{1,0:T(8,128)(2,1)S(1)} %bitcast.22, bf16[2,128,256]{2,1,0:T(8,128)(2,1)S(1)} %collective-permute-done.near_ref, ...), custom_call_target="tpu_custom_call" | custom-call | tf_op jit(solution)/shard_map/first/pallas_call | solution.py:250
  23.7 1.3 %collective-permute-start.2 = (bf16[2,256,256]{2,1,0:T(8,128)(2,1)S(1)}, bf16[2,256,256]{2,1,0:T(8,128)(2,1)S(1)}, u32[]{:S(2)}, u32[]{:S(2)}) collective-permute-start(bf16[2,256,256]{2,1,0:T(8,128)(2,1)S(1)} %get-tuple-element.42), channel_id=1, source_target_pairs={{8,0},{16,8},{24,16},{32,24},{40,32},{48,40},{56,48},{64,56},{72,6... | collective-permute-start | bytes 786440 | tf_op jit(solution)/shard_map/ppermute | solution.py:322
  25.0 5.1 %all-to-all-done = f32[16,4,128]{2,1,0:T(4,128)S(1)} async-done(((f32[16,4,128]{2,1,0:T(4,128)}), f32[16,4,128]{2,1,0:T(4,128)S(1)}, u32[]{:S(2)}, u32[]{:S(2)}) %all-to-all-start) | async-done | bytes 32800 | tf_op jit(solution)/shard_map/all_to_all | solution.py:262
  30.1 0.7 %broadcast_in_dim.3 = f32[32,8,128]{2,1,0:T(8,128)} broadcast(f32[8,128]{1,0:T(8,128)S(1)} %bitcast_reduce_fusion), dimensions={1,2} | broadcast | bytes 135168 | tf_op jit(solution)/shard_map/broadcast_in_dim | solution.py:324
  30.8 12.9 %all-to-all-start.1 = ((f32[32,8,128]{2,1,0:T(8,128)}), f32[32,8,128]{2,1,0:T(8,128)S(1)}, u32[]{:S(2)}, u32[]{:S(2)}) async-start(f32[32,8,128]{2,1,0:T(8,128)} %broadcast_in_dim.3), calls=%async_computation.1 | async-start | bytes 262144 | tf_op jit(solution)/shard_map/all_to_all | solution.py:262
  43.7 0.0 collective-permute-done.2.back_ref
  43.7 0.8 %join.1 = (bf16[384,256]{1,0:T(8,128)(2,1)}, bf16[384,256]{1,0:T(8,128)(2,1)}) custom-call(f32[2,384,256]{2,1,0:T(8,128)S(1)} %get-tuple-element.30.part_ref, f32[2,128,256]{2,1,0:T(8,128)S(1)} %get-tuple-element.40.end_ref, bf16[2,128,256]{2,1,0:T(8,128)(2,1)S(1)} %get-tuple-element.41.done_ref, bf16[2,256,256]{2,1,0:T(8,128)(2,1)S(1)} %collective-permute-done.2.back_ref), custom_call_target="tpu_custom_call" | custom-call | tf_op jit(solution)/shard_map/join/pallas_call | solution.py:250
  44.5 8.6 %all-to-all-done.1 = f32[32,8,128]{2,1,0:T(8,128)S(1)} async-done(((f32[32,8,128]{2,1,0:T(8,128)}), f32[32,8,128]{2,1,0:T(8,128)S(1)}, u32[]{:S(2)}, u32[]{:S(2)}) %all-to-all-start.1) | async-done | bytes 131104 | tf_op jit(solution)/shard_map/all_to_all | solution.py:262
  53.0 0.7 %table.1 = f32[16,192]{1,0:T(8,128)} custom-call(f32[8,32,128]{2,1,0:T(8,128)S(1)} %bitcast.26), custom_call_target="tpu_custom_call" | custom-call | tf_op jit(solution)/shard_map/table/pallas_call | solution.py:250
  (1 shorter events, 0.0 us)
Async XLA Ops:
  0.6 8.3 %copy-start = (bf16[1,384,256]{2,1,0:T(8,128)(2,1)S(1)}, bf16[1,384,256]{2,1,0:T(8,128)(2,1)}, u32[]{:S(2)}) copy-start(bf16[1,384,256]{2,1,0:T(8,128)(2,1)} %param.6) | copy-start | bytes 589828
  0.6 8.3 %copy-start.1 = (bf16[1,384,256]{2,1,0:T(8,128)(2,1)S(1)}, bf16[1,384,256]{2,1,0:T(8,128)(2,1)}, u32[]{:S(2)}) copy-start(bf16[1,384,256]{2,1,0:T(8,128)(2,1)} %param.5) | copy-start | bytes 589828
  1.7 10.3 %collective-permute-start = (bf16[2,128,256]{2,1,0:T(8,128)(2,1)S(1)}, bf16[2,128,256]{2,1,0:T(8,128)(2,1)S(1)}, u32[]{:S(2)}, u32[]{:S(2)}) collective-permute-start(bf16[2,128,256]{2,1,0:T(8,128)(2,1)S(1)} %get-tuple-element.25), channel_id=1, source_target_pairs={{0,8},{8,16},{16,24},{24,32},{32,40},{40,48},{48,56},{56,64},{64,7... | collective-permute-start | bytes 393224 | tf_op jit(solution)/shard_map/ppermute | solution.py:276
  5.7 3.2 %copy-start.5 = (f32[2,192]{1,0:T(2,128)S(1)}, f32[2,192]{1,0:T(2,128)}, u32[]{:S(2)}) copy-start(f32[2,192]{1,0:T(2,128)} %rb_ref.1) | copy-start | bytes 4612
  5.7 7.4 %collective-permute-start.1 = (bf16[2,128,256]{2,1,0:T(8,128)(2,1)S(1)}, bf16[2,128,256]{2,1,0:T(8,128)(2,1)S(1)}, u32[]{:S(2)}, u32[]{:S(2)}) collective-permute-start(bf16[2,128,256]{2,1,0:T(8,128)(2,1)S(1)} %get-tuple-element.26), channel_id=1, source_target_pairs={{0,8},{8,16},{16,24},{24,32},{32,40},{40,48},{48,56},{56,64},{64,7... | collective-permute-start | bytes 393224 | tf_op jit(solution)/shard_map/ppermute | solution.py:277
  9.0 0.9 %copy-start.2 = (bf16[1,384,256]{2,1,0:T(8,128)(2,1)S(1)}, bf16[1,384,256]{2,1,0:T(8,128)(2,1)}, u32[]{:S(2)}) copy-start(bf16[1,384,256]{2,1,0:T(8,128)(2,1)} %param.9) | copy-start | bytes 589828
  9.9 0.9 %copy-start.4 = (bf16[1,384,256]{2,1,0:T(8,128)(2,1)S(1)}, bf16[1,384,256]{2,1,0:T(8,128)(2,1)}, u32[]{:S(2)}) copy-start(bf16[1,384,256]{2,1,0:T(8,128)(2,1)} %param.7) | copy-start | bytes 589828
  13.2 9.6 %copy-start.3 = (bf16[1,384,256]{2,1,0:T(8,128)(2,1)S(1)}, bf16[1,384,256]{2,1,0:T(8,128)(2,1)}, u32[]{:S(2)}) copy-start(bf16[1,384,256]{2,1,0:T(8,128)(2,1)} %param.9) | copy-start | bytes 589828
  14.5 15.7 %all-to-all-start = ((f32[16,4,128]{2,1,0:T(4,128)}), f32[16,4,128]{2,1,0:T(4,128)S(1)}, u32[]{:S(2)}, u32[]{:S(2)}) async-start(f32[16,4,128]{2,1,0:T(4,128)} %get-tuple-element.45), calls=%async_computation | async-start | bytes 65536 | tf_op jit(solution)/shard_map/all_to_all | solution.py:262
  23.7 20.0 %collective-permute-start.2 = (bf16[2,256,256]{2,1,0:T(8,128)(2,1)S(1)}, bf16[2,256,256]{2,1,0:T(8,128)(2,1)S(1)}, u32[]{:S(2)}, u32[]{:S(2)}) collective-permute-start(bf16[2,256,256]{2,1,0:T(8,128)(2,1)S(1)} %get-tuple-element.42), channel_id=1, source_target_pairs={{8,0},{16,8},{24,16},{32,24},{40,32},{48,40},{56,48},{64,56},{72,6... | collective-permute-start | bytes 786440 | tf_op jit(solution)/shard_map/ppermute | solution.py:322
  30.8 22.2 %all-to-all-start.1 = ((f32[32,8,128]{2,1,0:T(8,128)}), f32[32,8,128]{2,1,0:T(8,128)S(1)}, u32[]{:S(2)}, u32[]{:S(2)}) async-start(f32[32,8,128]{2,1,0:T(8,128)} %broadcast_in_dim.3), calls=%async_computation.1 | async-start | bytes 262144 | tf_op jit(solution)/shard_map/all_to_all | solution.py:262

commit v4 on v3

--- a/solution.py
+++ b/solution.py
@@ -1,4 +1,5 @@
 import functools
+import math
 
 import jax
 import jax.numpy as jnp
@@ -207,34 +208,39 @@
     pay_ref[...] = jnp.broadcast_to(total[None], pay_ref.shape)
 
 
-def first_body(
-    q_ref, k_ref, g_ref, near_ref, far_ref, part_ref, prob_ref, low_ref, dq1_ref, dq2_ref,
-    dq_ref, back_ref, done_ref,
+def back_body(q_ref, g_ref, part_ref, prob_ref, low_ref, back_ref):
+    for h in range(HEADS):
+        hs = head(h)
+        for i, (w, x) in enumerate(((low_ref, q_ref), (prob_ref, g_ref))):
+            out = dot(w[h, : 2 * BLK, :], x[:BLK, hs], 1, 0)
+            back_ref[i, :BLK, hs] = out[:BLK].astype(BF16)
+            back_ref[i, BLK:, hs] = (out[BLK:] + part_ref[i, :BLK, hs]).astype(BF16)
+
+
+def join_body(
+    q_ref, k_ref, g_ref, near_ref, far_ref, part_ref, end_ref, prob_ref, low_ref, dq1_ref, dq2_ref, back_ref,
+    dq_ref, dk_ref, dv_ref,
 ):
     dq_ref[BLK : 2 * BLK, :] = dq1_ref[...]
     dq_ref[2 * BLK :, :] = dq2_ref[...]
-    for h in range(HEADS):
-        hs = head(h)
-        low = low_ref[h]
-        keys = stack([far_ref[0, :, hs], near_ref[0, :, hs], k_ref[:BLK, hs]])
-        dq_ref[:BLK, hs] = dot(low, keys, 0, 0).astype(BF16)
-        outs = (dot(low, q_ref[:BLK, hs], 1, 0), dot(prob_ref[h], g_ref[:BLK, hs], 1, 0))
-        for i, out in enumerate(outs):
-            back_ref[i, :BLK, hs] = out[:BLK].astype(BF16)
-            back_ref[i, BLK:, hs] = (out[BLK : 2 * BLK] + part_ref[i, :BLK, hs]).astype(BF16)
-            done_ref[i, :, hs] = (out[2 * BLK :] + part_ref[i, BLK : 2 * BLK, hs]).astype(BF16)
-
-
-def join_body(part_ref, end_ref, done_ref, back_ref, dk_ref, dv_ref):
     for i, out in enumerate((dk_ref, dv_ref)):
-        out[:BLK, :] = done_ref[i]
         out[BLK : 2 * BLK, :] = (part_ref[i, 2 * BLK :, :] + back_ref[i, :BLK, :].astype(F32)).astype(BF16)
         out[2 * BLK :, :] = (end_ref[i] + back_ref[i, BLK:, :].astype(F32)).astype(BF16)
-
-
-def table_body(x_ref, o_ref, sum_ref):
+    for h in range(HEADS):
+        hs = head(h)
+        keys = stack([far_ref[0, :, hs], near_ref[0, :, hs], k_ref[:BLK, hs]])
+        dq_ref[:BLK, hs] = dot(low_ref[h], keys, 0, 0).astype(BF16)
+        for i, (out, w, x) in enumerate(((dk_ref, low_ref, q_ref), (dv_ref, prob_ref, g_ref))):
+            own = dot(w[h, 2 * BLK :, :], x[:BLK, hs], 1, 0)
+            out[:BLK, hs] = (own + part_ref[i, BLK : 2 * BLK, hs]).astype(BF16)
+
+
+def table_body(order, x_ref, o_ref, sum_ref):
     heads = o_ref.shape[0]
-    sum_ref[...] = jnp.sum(x_ref[...], axis=0)
+    total = jnp.sum(x_ref[...], axis=0)
+    span = total.shape[0] // len(order)
+    for i, at in enumerate(order):
+        sum_ref[at * span : (at + 1) * span, :] = total[i * span : (i + 1) * span]
     low = sum_ref[pl.ds(0, heads, stride=2), :]
     mid = sum_ref[pl.ds(1, heads, stride=2), :]
     lane = lax.broadcasted_iota(jnp.int32, low.shape, 1)
@@ -258,8 +264,19 @@
     )(*args)
 
 
-def exchange(x, axes):
-    return lax.all_to_all(x, axes, split_axis=0, concat_axis=0, tiled=True)
+def ordered(count, first):
+    return [(first + i) % count for i in range(count)]
+
+
+def exchange(x, size, outer, inner):
+    rest = [a for a in AXES if a not in (outer[0], inner[0])]
+    step = {a: math.prod(size[b] for b in AXES[AXES.index(a) + 1 :]) for a in AXES}
+    groups = [
+        [i * step[rest[0]] + j * step[rest[1]] + m * step[outer[0]] + n * step[inner[0]] for m in outer[1] for n in inner[1]]
+        for i in range(size[rest[0]])
+        for j in range(size[rest[1]])
+    ]
+    return lax.all_to_all(x, AXES, split_axis=0, concat_axis=0, axis_index_groups=groups, tiled=True)
 
 
 def local(queries, keys, values, rel_bias, out_grad):
@@ -302,6 +319,7 @@
         (q, k, v, g, near, table, mid, pay),
     )
     group = size["y"] * size["c"]
+    z_order, y_order, x_order = ordered(size["z"], 7), ordered(size["y"], 4), ordered(size["x"], 2)
     pay, prob, low = call(
         far_body,
         "far",
@@ -312,25 +330,24 @@
         ],
         (q, g, far, table, pay, expo, dp, stat),
     )
-    pay = exchange(pay, ("y", "c"))
-    dq, back, done = call(
-        first_body,
-        "first",
-        [((rows, width), BF16), ((2, 2 * BLK, width), BF16), (pair, BF16)],
-        (q, k, g, near, far, part, prob, low, dq1, dq2),
-    )
+    pay = exchange(pay, size, ("y", y_order), ("c", range(size["c"])))
+    (back,) = call(back_body, "back", [((2, 2 * BLK, width), BF16)], (q, g, part, prob, low))
     back = lax.ppermute(back, ("z", "y"), [(s + 1, s) for s in range(count - 1)])
     pay = pay.reshape(size["y"], size["c"] * 2 * HEADS, BLK).sum(axis=0)
     pay = jnp.broadcast_to(pay, (size["z"] * size["x"], *pay.shape))
-    pay = exchange(pay, ("z", "x"))
-    dk, dv = call(join_body, "join", [((rows, width), BF16)] * 2, (part, end, done, back), mib=6)
-    shape = (size["x"] * size["c"] * 2 * HEADS, BLK)
+    pay = exchange(pay, size, ("z", z_order), ("x", x_order))
+    dq, dk, dv = call(
+        join_body,
+        "join",
+        [((rows, width), BF16)] * 3,
+        (q, k, g, near, far, part, end, prob, low, dq1, dq2, back),
+    )
     (bias,) = call(
-        table_body,
+        functools.partial(table_body, x_order),
         "table",
-        [((shape[0] // 2, BUCKETS), F32)],
-        (pay.reshape(size["z"], *shape),),
-        scratch=[pltpu.VMEM(shape, F32)],
+        [((size["x"] * size["c"] * HEADS, BUCKETS), F32)],
+        (pay.reshape(size["z"], size["x"] * size["c"] * 2 * HEADS, BLK),),
+        scratch=[pltpu.VMEM((size["x"] * size["c"] * 2 * HEADS, BLK), F32)],
         mib=4,
     )
     return tuple(a.reshape(queries.shape) for a in (dq, dk, dv)) + (bias,)

time: 54.1 us -> 49.4 us (0.913)
  waiting for transfers between devices: 13.7 us -> 5.65 us
  starting transfers between devices: 29.7 us -> 33.2 us
    all_to_all x2, waiting for transfers between devices: 13.7 us -> 5.64 us  [exchange(): lax.all_to_all(x, AXES, split_axis=0, concat_axis=0, axis_index_groups=gr...]
    all_to_all x2, starting transfers between devices: 21.1 us -> 24.7 us  [exchange(): lax.all_to_all(x, AXES, split_axis=0, concat_axis=0, axis_index_groups=gr...]
  transfers between devices with their start and end apart: 5 -> 5, of which waited for: 2 -> 2; matrix products, arithmetic and copies ran while one was open for 1% -> 1% of each run, Pallas kernels for 8% -> 7%
where the time goes in v4:
time: 49.4 us; the launch traced here: 48.8 us
  starting transfers between devices  33.2 us (67%)
  Pallas kernels  6.63 us (13%)
  waiting for transfers between devices  5.65 us (11%)
  local copies, waits for them, and re-layouts  2.54 us (5%)
  between operations  0.77 us (2%)
    all_to_all x2, starting transfers between devices, exchange(): lax.all_to_all(x, AXES, split_axis=0, concat_axis=0, axis_index_groups=gr...  24.7 us
    pallas_call x7, Pallas kernels, call(): pl.pallas_call(body, out_shape=tuple((jax.ShapeDtypeStruct(*o) for o in o...  6.63 us
    all_to_all x2, waiting for transfers between devices, exchange(): lax.all_to_all(x, AXES, split_axis=0, concat_axis=0, axis_index_groups=gr...  5.64 us
    ppermute x1, starting transfers between devices, local(): near = lax.ppermute(near, ('z', 'y'), ahead)  4.03 us
    ppermute x1, starting transfers between devices, local(): far = lax.ppermute(far, ('z', 'y'), ahead)  3.2 us
    unnamed x12, local copies, waits for them, and re-layouts  1.87 us
    ppermute x1, starting transfers between devices, local(): lax.ppermute(back, ('z', 'y'), [(s + 1, s) for s in range(count - 1)])  1.29 us
  transfers between devices with their start and end apart: 5, of which 2 were waited for; matrix products, arithmetic and copies ran while one was open for 1% of the time, Pallas kernels for 7%

profile of v4, /device:TPU:1, one launch (start us, length us, event | category | flops | bytes accessed | tf_op | source)
XLA Modules:
  0.0 48.8 jit_solution(833149406293040380)
XLA Ops:
  0.6 0.0 copy-start
  0.6 0.0 copy-start.1
  0.7 1.0 %tails.1 = (bf16[2,128,256]{2,1,0:T(8,128)(2,1)S(1)}, bf16[2,128,256]{2,1,0:T(8,128)(2,1)S(1)}) custom-call(bf16[384,256]{1,0:T(8,128)(2,1)} %bitcast.21, bf16[384,256]{1,0:T(8,128)(2,1)} %bitcast.25), custom_call_target="tpu_custom_call" | custom-call | tf_op jit(solution)/shard_map/tails/pallas_call | solution.py:256
  1.7 4.0 %collective-permute-start = (bf16[2,128,256]{2,1,0:T(8,128)(2,1)S(1)}, bf16[2,128,256]{2,1,0:T(8,128)(2,1)S(1)}, u32[]{:S(2)}, u32[]{:S(2)}) collective-permute-start(bf16[2,128,256]{2,1,0:T(8,128)(2,1)S(1)} %get-tuple-element.23), channel_id=1, source_target_pairs={{0,8},{8,16},{16,24},{24,32},{32,40},{40,48},{48,56},{56,64},{64,7... | collective-permute-start | bytes 393224 | tf_op jit(solution)/shard_map/ppermute | solution.py:293
  5.7 0.0 copy-start.5
  5.7 3.2 %collective-permute-start.1 = (bf16[2,128,256]{2,1,0:T(8,128)(2,1)S(1)}, bf16[2,128,256]{2,1,0:T(8,128)(2,1)S(1)}, u32[]{:S(2)}, u32[]{:S(2)}) collective-permute-start(bf16[2,128,256]{2,1,0:T(8,128)(2,1)S(1)} %get-tuple-element.24), channel_id=1, source_target_pairs={{0,8},{8,16},{16,24},{24,32},{32,40},{40,48},{48,56},{56,64},{64,7... | collective-permute-start | bytes 393224 | tf_op jit(solution)/shard_map/ppermute | solution.py:294
  8.9 0.0 copy-done
  8.9 0.0 copy-done.1
  9.0 0.0 copy-done.5
  9.0 0.0 copy-start.2
  9.0 0.9 %copy-done.2 = bf16[1,384,256]{2,1,0:T(8,128)(2,1)S(1)} copy-done((bf16[1,384,256]{2,1,0:T(8,128)(2,1)S(1)}, bf16[1,384,256]{2,1,0:T(8,128)(2,1)}, u32[]{:S(2)}) %copy-start.2) | copy-done | bytes 196632
  9.9 0.0 copy-start.4
  9.9 0.9 %copy-done.4 = bf16[1,384,256]{2,1,0:T(8,128)(2,1)S(1)} copy-done((bf16[1,384,256]{2,1,0:T(8,128)(2,1)S(1)}, bf16[1,384,256]{2,1,0:T(8,128)(2,1)}, u32[]{:S(2)}) %copy-start.4) | copy-done | bytes 196632
  10.8 1.1 %own.1 = (bf16[128,256]{1,0:T(8,128)(2,1)S(1)}, f32[2,256,256]{2,1,0:T(8,128)S(1)}, f32[2,128,256]{2,1,0:T(8,128)S(1)}, f32[4,128]{1,0:T(4,128)S(1)}, f32[6,128,128]{2,1,0:T(8,128)S(1)}) custom-call(bf16[384,256]{1,0:T(8,128)(2,1)S(1)} %bitcast.11, bf16[384,256]{1,0:T(8,128)(2,1)S(1)} %bitcast.22, bf16[384,256]{1,0:T(8,128)(2,1)S(1)} %bitcast.26, ...), custom_call_target="tpu_custom_call" | custom-call | tf_op jit(solution)/shard_map/own/pallas_call | solution.py:256
  11.9 0.0 collective-permute-done.near_ref
  11.9 1.2 %near.1 = (bf16[128,256]{1,0:T(8,128)(2,1)S(1)}, f32[2,384,256]{2,1,0:T(8,128)S(1)}, f32[4,128]{1,0:T(4,128)S(1)}, f32[4,128,128]{2,1,0:T(8,128)S(1)}, f32[4,128,128]{2,1,0:T(8,128)S(1)}, /*index=5*/f32[8,128]{1,0:T(8,128)S(1)}) custom-call(bf16[384,256]{1,0:T(8,128)(2,1)S(1)} %bitcast.12, bf16[384,256]{1,0:T(8,128)(2,1)S(1)} %bitcast.23, ...), custom_call_target="tpu_custom_call" | custom-call | tf_op jit(solution)/shard_map/near/pallas_call | solution.py:256
  13.2 0.0 collective-permute-done.1.far_ref
  13.2 1.3 %far.1 = (f32[16,4,128]{2,1,0:T(4,128)}, bf16[2,384,128]{2,1,0:T(8,128)(2,1)S(1)}, bf16[2,384,128]{2,1,0:T(8,128)(2,1)S(1)}) custom-call(bf16[384,256]{1,0:T(8,128)(2,1)S(1)} %bitcast.13, bf16[384,256]{1,0:T(8,128)(2,1)S(1)} %bitcast.18, bf16[2,128,256]{2,1,0:T(8,128)(2,1)S(1)} %collective-permute-done.1.far_ref, ...), custom_call_target="tpu_custom_call" | custom-call | tf_op jit(solution)/shard_map/far/pallas_call | solution.py:256
  14.5 9.9 %all-to-all-start = ((f32[16,4,128]{2,1,0:T(4,128)}), f32[16,4,128]{2,1,0:T(4,128)S(1)}, u32[]{:S(2)}, u32[]{:S(2)}) async-start(f32[16,4,128]{2,1,0:T(4,128)} %get-tuple-element.41), calls=%async_computation | async-start | bytes 65536 | tf_op jit(solution)/shard_map/all_to_all | solution.py:279
  24.4 0.2 back.1
  24.6 1.3 %collective-permute-start.2 = (bf16[2,256,256]{2,1,0:T(8,128)(2,1)S(1)}, bf16[2,256,256]{2,1,0:T(8,128)(2,1)S(1)}, u32[]{:S(2)}, u32[]{:S(2)}) collective-permute-start(bf16[2,256,256]{2,1,0:T(8,128)(2,1)S(1)} %back.1), channel_id=1, source_target_pairs={{8,0},{16,8},{24,16},{32,24},{40,32},{48,40},{56,48},{64,56},{72,6... | collective-permute-start | bytes 786440 | tf_op jit(solution)/shard_map/ppermute | solution.py:335
  25.9 1.1 %all-to-all-done = f32[16,4,128]{2,1,0:T(4,128)S(1)} async-done(((f32[16,4,128]{2,1,0:T(4,128)}), f32[16,4,128]{2,1,0:T(4,128)S(1)}, u32[]{:S(2)}, u32[]{:S(2)}) %all-to-all-start) | async-done | bytes 32800 | tf_op jit(solution)/shard_map/all_to_all | solution.py:279
  27.0 0.0 copy-start.3
  27.0 0.7 %broadcast_in_dim.3 = f32[32,8,128]{2,1,0:T(8,128)} broadcast(f32[8,128]{1,0:T(8,128)S(1)} %bitcast_reduce_fusion), dimensions={1,2} | broadcast | bytes 135168 | tf_op jit(solution)/shard_map/broadcast_in_dim | solution.py:337
  27.7 14.8 %all-to-all-start.1 = ((f32[32,8,128]{2,1,0:T(8,128)}), f32[32,8,128]{2,1,0:T(8,128)S(1)}, u32[]{:S(2)}, u32[]{:S(2)}) async-start(f32[32,8,128]{2,1,0:T(8,128)} %broadcast_in_dim.3), calls=%async_computation.1 | async-start | bytes 262144 | tf_op jit(solution)/shard_map/all_to_all | solution.py:279
  42.4 0.0 collective-permute-done.2.back_ref
  42.4 0.0 copy-done.3
  42.4 1.1 %join.1 = (bf16[384,256]{1,0:T(8,128)(2,1)}, bf16[384,256]{1,0:T(8,128)(2,1)}, bf16[384,256]{1,0:T(8,128)(2,1)}) custom-call(bf16[384,256]{1,0:T(8,128)(2,1)S(1)} %bitcast.15, bf16[384,256]{1,0:T(8,128)(2,1)S(1)} %bitcast.24, bf16[384,256]{1,0:T(8,128)(2,1)S(1)} %bitcast.20, bf16[2,128,256]{2,1,0:T(8,128)(2,1)S(1)} %collective-permute-done.near_ref, ...), custom_call_target="tpu_custom_call" | custom-call | tf_op jit(solution)/shard_map/join/pallas_call | solution.py:256
  43.5 4.6 %all-to-all-done.1 = f32[32,8,128]{2,1,0:T(8,128)S(1)} async-done(((f32[32,8,128]{2,1,0:T(8,128)}), f32[32,8,128]{2,1,0:T(8,128)S(1)}, u32[]{:S(2)}, u32[]{:S(2)}) %all-to-all-start.1) | async-done | bytes 131104 | tf_op jit(solution)/shard_map/all_to_all | solution.py:279
  48.1 0.7 %table.1 = f32[16,192]{1,0:T(8,128)} custom-call(f32[8,32,128]{2,1,0:T(8,128)S(1)} %bitcast.28), custom_call_target="tpu_custom_call" | custom-call | tf_op jit(solution)/shard_map/table/pallas_call | solution.py:256
  (1 shorter events, 0.0 us)
Async XLA Ops:
  0.6 8.3 %copy-start = (bf16[1,384,256]{2,1,0:T(8,128)(2,1)S(1)}, bf16[1,384,256]{2,1,0:T(8,128)(2,1)}, u32[]{:S(2)}) copy-start(bf16[1,384,256]{2,1,0:T(8,128)(2,1)} %param.5) | copy-start | bytes 589828
  0.6 8.3 %copy-start.1 = (bf16[1,384,256]{2,1,0:T(8,128)(2,1)S(1)}, bf16[1,384,256]{2,1,0:T(8,128)(2,1)}, u32[]{:S(2)}) copy-start(bf16[1,384,256]{2,1,0:T(8,128)(2,1)} %param.9) | copy-start | bytes 589828
  1.7 10.2 %collective-permute-start = (bf16[2,128,256]{2,1,0:T(8,128)(2,1)S(1)}, bf16[2,128,256]{2,1,0:T(8,128)(2,1)S(1)}, u32[]{:S(2)}, u32[]{:S(2)}) collective-permute-start(bf16[2,128,256]{2,1,0:T(8,128)(2,1)S(1)} %get-tuple-element.23), channel_id=1, source_target_pairs={{0,8},{8,16},{16,24},{24,32},{32,40},{40,48},{48,56},{56,64},{64,7... | collective-permute-start | bytes 393224 | tf_op jit(solution)/shard_map/ppermute | solution.py:293
  5.7 3.2 %copy-start.5 = (f32[2,192]{1,0:T(2,128)S(1)}, f32[2,192]{1,0:T(2,128)}, u32[]{:S(2)}) copy-start(f32[2,192]{1,0:T(2,128)} %rb_ref.1) | copy-start | bytes 4612
  5.7 7.4 %collective-permute-start.1 = (bf16[2,128,256]{2,1,0:T(8,128)(2,1)S(1)}, bf16[2,128,256]{2,1,0:T(8,128)(2,1)S(1)}, u32[]{:S(2)}, u32[]{:S(2)}) collective-permute-start(bf16[2,128,256]{2,1,0:T(8,128)(2,1)S(1)} %get-tuple-element.24), channel_id=1, source_target_pairs={{0,8},{8,16},{16,24},{24,32},{32,40},{40,48},{48,56},{56,64},{64,7... | collective-permute-start | bytes 393224 | tf_op jit(solution)/shard_map/ppermute | solution.py:294
  9.0 0.9 %copy-start.2 = (bf16[1,384,256]{2,1,0:T(8,128)(2,1)S(1)}, bf16[1,384,256]{2,1,0:T(8,128)(2,1)}, u32[]{:S(2)}) copy-start(bf16[1,384,256]{2,1,0:T(8,128)(2,1)} %param.6) | copy-start | bytes 589828
  9.9 0.9 %copy-start.4 = (bf16[1,384,256]{2,1,0:T(8,128)(2,1)S(1)}, bf16[1,384,256]{2,1,0:T(8,128)(2,1)}, u32[]{:S(2)}) copy-start(bf16[1,384,256]{2,1,0:T(8,128)(2,1)} %param.7) | copy-start | bytes 589828
  14.5 12.5 %all-to-all-start = ((f32[16,4,128]{2,1,0:T(4,128)}), f32[16,4,128]{2,1,0:T(4,128)S(1)}, u32[]{:S(2)}, u32[]{:S(2)}) async-start(f32[16,4,128]{2,1,0:T(4,128)} %get-tuple-element.41), calls=%async_computation | async-start | bytes 65536 | tf_op jit(solution)/shard_map/all_to_all | solution.py:279
  24.6 17.8 %collective-permute-start.2 = (bf16[2,256,256]{2,1,0:T(8,128)(2,1)S(1)}, bf16[2,256,256]{2,1,0:T(8,128)(2,1)S(1)}, u32[]{:S(2)}, u32[]{:S(2)}) collective-permute-start(bf16[2,256,256]{2,1,0:T(8,128)(2,1)S(1)} %back.1), channel_id=1, source_target_pairs={{8,0},{16,8},{24,16},{32,24},{40,32},{48,40},{56,48},{64,56},{72,6... | collective-permute-start | bytes 786440 | tf_op jit(solution)/shard_map/ppermute | solution.py:335
  27.0 15.4 %copy-start.3 = (bf16[1,384,256]{2,1,0:T(8,128)(2,1)S(1)}, bf16[1,384,256]{2,1,0:T(8,128)(2,1)}, u32[]{:S(2)}) copy-start(bf16[1,384,256]{2,1,0:T(8,128)(2,1)} %param.6) | copy-start | bytes 589828
  27.7 20.4 %all-to-all-start.1 = ((f32[32,8,128]{2,1,0:T(8,128)}), f32[32,8,128]{2,1,0:T(8,128)S(1)}, u32[]{:S(2)}, u32[]{:S(2)}) async-start(f32[32,8,128]{2,1,0:T(8,128)} %broadcast_in_dim.3), calls=%async_computation.1 | async-start | bytes 262144 | tf_op jit(solution)/shard_map/all_to_all | solution.py:279

commit v5 on v4

--- a/solution.py
+++ b/solution.py
@@ -55,9 +55,10 @@
     for a in range(8, BLK, 8):
         acc = acc + pltpu.roll(x[a : a + 8], BLK - a, 1)
     row = lax.broadcasted_iota(jnp.int32, acc.shape, 0)
-    for bit in (1, 2, 4):
-        acc = jnp.where((row & bit) != 0, pltpu.roll(acc, BLK - bit, 1), acc)
-    return jnp.sum(acc, axis=0, keepdims=True)
+    out = acc
+    for b in range(1, 8):
+        out = jnp.where(row == b, pltpu.roll(acc, BLK - b, 1), out)
+    return jnp.sum(out, axis=0, keepdims=True)
 
 
 def skew_sum(d0, d1, d2):
@@ -85,6 +86,10 @@
     return functools.reduce(jnp.add, blocks).sum(axis=0, keepdims=True)
 
 
+def sum_rows(x):
+    return x.sum(axis=0, keepdims=True)
+
+
 def weights(scores, prob_grads):
     peak = peak_of(scores)
     expo = [jnp.exp2(s - peak) for s in scores]
@@ -108,27 +113,42 @@
     return jnp.where(first, NEG, 0.0).astype(F32)
 
 
-def tails_body(k_ref, v_ref, near_ref, far_ref, sem):
-    first = k_ref.shape[0] - 2 * BLK
-    copies = [
-        pltpu.make_async_copy(ref.at[pl.ds(first + at, BLK)], out.at[i], sem.at[2 * i + j])
-        for i, ref in enumerate((k_ref, v_ref))
-        for j, (out, at) in enumerate(((near_ref, BLK), (far_ref, 0)))
-    ]
+def start_all(copies):
     for copy in copies:
         copy.start()
+    return copies
+
+
+def wait_all(copies):
     for copy in copies:
         copy.wait()
 
 
-def own_body(q_ref, k_ref, v_ref, g_ref, rb_ref, dq_ref, mid_ref, end_ref, pay_ref, tab_ref, rb_pad):
+def tails_body(k_ref, v_ref, near_ref, far_ref, sem):
+    first = k_ref.shape[0] - near_ref.shape[1] - far_ref.shape[1]
+    copies = [
+        pltpu.make_async_copy(ref.at[pl.ds(first + at, out.shape[1])], out.at[i], sem.at[2 * i + j])
+        for i, ref in enumerate((k_ref, v_ref))
+        for j, (out, at) in enumerate(((near_ref, far_ref.shape[1]), (far_ref, 0)))
+    ]
+    wait_all(start_all(copies))
+
+
+def own_body(
+    q_hbm, k_hbm, v_hbm, g_hbm, rb_ref,
+    q_ref, k_ref, v_ref, g_ref, dq_ref, mid_ref, end_ref, pay_ref, tab_ref, rb_pad, sem,
+):
+    loads = ((k_hbm, k_ref), (q_hbm, q_ref), (v_hbm, v_ref), (g_hbm, g_ref))
+    loads = start_all([pltpu.make_async_copy(x, y, sem.at[i]) for i, (x, y) in enumerate(loads)])
     rb_pad[...] = jnp.zeros_like(rb_pad)
     rb_pad[0:HEADS, 0:BUCKETS] = rb_ref[...]
     for h in range(HEADS):
-        hs = head(h)
-        table = bias_blocks(rb_pad[h : h + 1, :])
-        for m in range(3):
-            tab_ref[3 * h + m] = table[m]
+        for m, block in enumerate(bias_blocks(rb_pad[h : h + 1, :])):
+            tab_ref[3 * h + m] = block
+    wait_all(loads)
+    for h in range(HEADS):
+        hs = head(h)
+        table = [tab_ref[3 * h + m] for m in range(3)]
         k = k_ref[:, hs]
         q = q_ref[2 * BLK :, hs]
         g = g_ref[2 * BLK :, hs]
@@ -153,31 +173,32 @@
     for h in range(HEADS):
         hs = head(h)
         table = [tab_ref[3 * h + m] for m in range(3)]
-        veiled = [table[0] + hidden, table[1] + hidden]
         k = stack([near_ref[0, :, hs], k_ref[: 2 * BLK, hs]])
         v = stack([near_ref[1, :, hs], v_ref[: 2 * BLK, hs]])
         q = q_ref[: 2 * BLK, hs]
         g = g_ref[: 2 * BLK, hs]
         raw = dot(k, q, 1, 1)
         dps = dot(v, g, 1, 1)
-        scores = [s * (SCALE * LOG2E) + t for s, t in zip(cut(raw[:, BLK:]), [veiled[0]] + table[1:])]
-        dp = cut(dps[:, BLK:])
+        scores = [s * (SCALE * LOG2E) + t for s, t in zip(cut(raw[SEG:, BLK:]), [table[0] + hidden] + table[1:])]
+        dp = cut(dps[SEG:, BLK:])
         expo, _, total, mixed = weights(scores, dp)
         inv = 1.0 / total
         prob, low, grad = softmax_grad(expo, dp, [inv] * 3, mixed * inv)
         low = stack(low)
-        dq_ref[:, hs] = dot(low, k, 0, 0).astype(BF16)
+        dq_ref[:, hs] = dot(low, k[SEG:], 0, 0).astype(BF16)
         for i, out in enumerate((dot(low, q[BLK:], 1, 0), dot(stack(prob), g[BLK:], 1, 0))):
             part_ref[i, :BLK, hs] = out[:BLK]
             part_ref[i, BLK:, hs] = out[BLK:] + mid_in[i, :, hs]
         pay_ref[2 * h : 2 * h + 2, :] = skew_sum(*grad) + pay_in[2 * h : 2 * h + 2, :]
-        scores = [s * (SCALE * LOG2E) + t for s, t in zip(cut(raw[: 2 * BLK, :BLK]), [veiled[1], table[2]])]
-        dp = cut(dps[: 2 * BLK, :BLK])
-        expo, peak, total, mixed = weights(scores, dp)
-        for i in range(2):
-            expo_ref[2 * h + i] = expo[i]
-            dp_ref[2 * h + i] = dp[i]
-        for i, x in enumerate((peak, total, mixed)):
+        shift = stack([table[0][SEG:] + hidden, table[1] + hidden, table[2]])
+        rows = shift.shape[0]
+        score = raw[:rows, :BLK] * (SCALE * LOG2E) + shift
+        dp = dps[:rows, :BLK]
+        peak = score.max(axis=0, keepdims=True)
+        expo = jnp.exp2(score - peak)
+        expo_ref[h] = expo
+        dp_ref[h] = dp
+        for i, x in enumerate((peak, sum_rows(expo), sum_rows(expo * dp))):
             stat_ref[3 * h + i : 3 * h + i + 1, :] = x
 
 
@@ -188,22 +209,19 @@
     pay = []
     for h in range(HEADS):
         hs = head(h)
-        score = dot(far_ref[0, :, hs], q_ref[:BLK, hs], 1, 1) * (SCALE * LOG2E) + (tab_ref[3 * h] + hidden)
+        score = dot(far_ref[0, :, hs], q_ref[:BLK, hs], 1, 1) * (SCALE * LOG2E) + (tab_ref[3 * h, :SEG, :] + hidden)
         dp = dot(far_ref[1, :, hs], g_ref[:BLK, hs], 1, 1)
         peak, total, mixed = (stat_ref[3 * h + i : 3 * h + i + 1, :] for i in range(3))
         top = jnp.maximum(peak, score.max(axis=0, keepdims=True))
         expo = jnp.exp2(score - top)
         fade = jnp.exp2(peak - top)
-        inv = 1.0 / (total * fade + sum_of([expo]))
-        delta = (mixed * fade + sum_of([expo * dp])) * inv
-        fade = fade * inv
-        expos = [expo, expo_ref[2 * h], expo_ref[2 * h + 1]]
-        dps = [dp, dp_ref[2 * h], dp_ref[2 * h + 1]]
-        prob, low, grad = softmax_grad(expos, dps, [inv, fade, fade], delta)
-        pay.append(skew_sum(*grad))
-        for m in range(3):
-            prob_ref[h, m * BLK : (m + 1) * BLK, :] = prob[m]
-            low_ref[h, m * BLK : (m + 1) * BLK, :] = low[m]
+        inv = 1.0 / (total * fade + sum_rows(expo))
+        delta = (mixed * fade + sum_rows(expo * dp)) * inv
+        prob = stack([expo * inv, expo_ref[h] * (fade * inv)])
+        grad = prob * (stack([dp, dp_ref[h]]) - delta)
+        prob_ref[h] = prob.astype(BF16)
+        low_ref[h] = (grad * SCALE).astype(BF16)
+        pay.append(skew_sum(*cut(grad)))
     total = jnp.concatenate(pay, axis=0) + pay_in[...]
     pay_ref[...] = jnp.broadcast_to(total[None], pay_ref.shape)
 
@@ -285,17 +303,24 @@
     size = {a: lax.axis_size(a) for a in AXES}
     count = size["z"] * size["y"]
     pair = (2, BLK, width)
-    kept = tuple(pltpu.with_memory_space_constraint(a, pltpu.HBM) for a in (k, v))
+    q, k, v, g = (pltpu.with_memory_space_constraint(a, pltpu.HBM) for a in (q, k, v, g))
     near, far = call(
-        tails_body, "tails", [(pair, BF16)] * 2, kept, [HBM] * 2, [pltpu.SemaphoreType.DMA((4,))], 4
+        tails_body,
+        "tails",
+        [((2, LEFT * SEG - SEG, width), BF16), ((2, SEG, width), BF16)],
+        (k, v),
+        [HBM] * 2,
+        [pltpu.SemaphoreType.DMA((4,))],
+        4,
     )
     ahead = [(s, s + 1) for s in range(count - 1)]
     near = lax.ppermute(near, ("z", "y"), ahead)
     far = lax.ppermute(far, ("z", "y"), ahead)
-    dq2, mid, end, pay, table = call(
+    q, k, v, g, dq2, mid, end, pay, table = call(
         own_body,
         "own",
-        [
+        [((rows, width), BF16)] * 4
+        + [
             ((BLK, width), BF16),
             ((2, 2 * BLK, width), F32),
             (pair, F32),
@@ -303,8 +328,10 @@
             ((3 * HEADS, BLK, BLK), F32),
         ],
         (q, k, v, g, rel_bias),
-        scratch=[pltpu.VMEM((8, 2 * BLK), F32)],
-    )
+        [HBM] * 4 + [VMEM],
+        [pltpu.VMEM((8, 2 * BLK), F32), pltpu.SemaphoreType.DMA((4,))],
+    )
+    seen = (HEADS, 2 * BLK + SEG, BLK)
     dq1, part, pay, expo, dp, stat = call(
         near_body,
         "near",
@@ -312,14 +339,14 @@
             ((BLK, width), BF16),
             ((2, 3 * BLK, width), F32),
             ((2 * HEADS, BLK), F32),
-            ((2 * HEADS, BLK, BLK), F32),
-            ((2 * HEADS, BLK, BLK), F32),
+            (seen, F32),
+            (seen, F32),
             ((8, BLK), F32),
         ],
         (q, k, v, g, near, table, mid, pay),
     )
     group = size["y"] * size["c"]
-    z_order, y_order, x_order = ordered(size["z"], 7), ordered(size["y"], 4), ordered(size["x"], 2)
+    z_order, y_order, x_order = [5,0,1,7,2,6,3,4], ordered(size["y"], 4), ordered(size["x"], 2)
     pay, prob, low = call(
         far_body,
         "far",

time: 49.4 us -> 48.5 us (0.982)
  local copies, waits for them, and re-layouts: 2.54 us -> 0.66 us
  starting transfers between devices: 33.2 us -> 35 us
  waiting for transfers between devices: 5.65 us -> 3.86 us
  Pallas kernels: 6.63 us -> 7.58 us
    unnamed x12 -> x2, local copies, waits for them, and re-layouts: 1.87 us -> 0.01 us
    all_to_all x2, starting transfers between devices: 24.7 us -> 26.5 us  [exchange(): lax.all_to_all(x, AXES, split_axis=0, concat_axis=0, axis_index_groups=gr...]
    all_to_all x2, waiting for transfers between devices: 5.64 us -> 3.85 us  [exchange(): lax.all_to_all(x, AXES, split_axis=0, concat_axis=0, axis_index_groups=gr...]
    pallas_call x7, Pallas kernels: 6.63 us -> 7.58 us  [call(): pl.pallas_call(body, out_shape=tuple((jax.ShapeDtypeStruct(*o) for o in o...]
  transfers between devices with their start and end apart: 5 -> 5, of which waited for: 2 -> 2; matrix products, arithmetic and copies ran while one was open for 1% -> 1% of each run, Pallas kernels for 7% -> 10%
where the time goes in v5:
time: 48.5 us; the launch traced here: 47.8 us
  starting transfers between devices  35 us (72%)
  Pallas kernels  7.58 us (16%)
  waiting for transfers between devices  3.86 us (8%)
  between operations  0.74 us (2%)
  local copies, waits for them, and re-layouts  0.66 us (1%)
    all_to_all x2, starting transfers between devices, exchange(): lax.all_to_all(x, AXES, split_axis=0, concat_axis=0, axis_index_groups=gr...  26.5 us
    pallas_call x7, Pallas kernels, call(): pl.pallas_call(body, out_shape=tuple((jax.ShapeDtypeStruct(*o) for o in o...  7.58 us
    ppermute x1, starting transfers between devices, local(): near = lax.ppermute(near, ('z', 'y'), ahead)  4.03 us
    all_to_all x2, waiting for transfers between devices, exchange(): lax.all_to_all(x, AXES, split_axis=0, concat_axis=0, axis_index_groups=gr...  3.85 us
    ppermute x1, starting transfers between devices, local(): far = lax.ppermute(far, ('z', 'y'), ahead)  3.2 us
    ppermute x1, starting transfers between devices, local(): lax.ppermute(back, ('z', 'y'), [(s + 1, s) for s in range(count - 1)])  1.29 us
  transfers between devices with their start and end apart: 5, of which 2 were waited for; matrix products, arithmetic and copies ran while one was open for 1% of the time, Pallas kernels for 10%

profile of v5, /device:TPU:1, one launch (start us, length us, event | category | flops | bytes accessed | tf_op | source)
XLA Modules:
  0.0 47.8 jit_solution(1423160327714919612)
XLA Ops:
  0.6 1.0 %tails.1 = (bf16[2,192,256]{2,1,0:T(8,128)(2,1)S(1)}, bf16[2,64,256]{2,1,0:T(8,128)(2,1)S(1)}) custom-call(bf16[384,256]{1,0:T(8,128)(2,1)} %bitcast.12, bf16[384,256]{1,0:T(8,128)(2,1)} %bitcast.14), custom_call_target="tpu_custom_call" | custom-call | tf_op jit(solution)/shard_map/tails/pallas_call | solution.py:274
  1.6 4.0 %collective-permute-start = (bf16[2,192,256]{2,1,0:T(8,128)(2,1)S(1)}, bf16[2,192,256]{2,1,0:T(8,128)(2,1)S(1)}, u32[]{:S(2)}, u32[]{:S(2)}) collective-permute-start(bf16[2,192,256]{2,1,0:T(8,128)(2,1)S(1)} %get-tuple-element.30), channel_id=1, source_target_pairs={{0,8},{8,16},{16,24},{24,32},{32,40},{40,48},{48,56},{56,64},{64,7... | collective-permute-start | bytes 589832 | tf_op jit(solution)/shard_map/ppermute | solution.py:317
  5.7 0.0 copy-start
  5.7 3.2 %collective-permute-start.1 = (bf16[2,64,256]{2,1,0:T(8,128)(2,1)S(1)}, bf16[2,64,256]{2,1,0:T(8,128)(2,1)S(1)}, u32[]{:S(2)}, u32[]{:S(2)}) collective-permute-start(bf16[2,64,256]{2,1,0:T(8,128)(2,1)S(1)} %get-tuple-element.31), channel_id=1, source_target_pairs={{0,8},{8,16},{16,24},{24,32},{32,40},{40,48},{48,56},{56,64},{64,7... | collective-permute-start | bytes 196616 | tf_op jit(solution)/shard_map/ppermute | solution.py:318
  8.9 0.0 copy-done
  8.9 2.3 %own.1 = (bf16[384,256]{1,0:T(8,128)(2,1)S(1)}, bf16[384,256]{1,0:T(8,128)(2,1)S(1)}, bf16[384,256]{1,0:T(8,128)(2,1)S(1)}, bf16[384,256]{1,0:T(8,128)(2,1)S(1)}...) custom-call(bf16[384,256]{1,0:T(8,128)(2,1)} %bitcast.16, ...), custom_call_target="tpu_custom_call" | custom-call | tf_op jit(solution)/shard_map/own/pallas_call | solution.py:274
  11.2 0.0 collective-permute-done.near_ref
  11.2 1.1 %near.1 = (bf16[128,256]{1,0:T(8,128)(2,1)S(1)}, f32[2,384,256]{2,1,0:T(8,128)S(1)}, f32[4,128]{1,0:T(4,128)S(1)}, f32[2,320,128]{2,1,0:T(8,128)S(1)}, f32[2,320,128]{2,1,0:T(8,128)S(1)}, /*index=5*/f32[8,128]{1,0:T(8,128)S(1)}) custom-call(bf16[384,256]{1,0:T(8,128)(2,1)S(1)} %get-tuple-element.27.q_ref, bf16[384,256]{1,0:T(8,128)(2,1)S(1)} %get-tuple-element.28.k_ref, ...), custom_call_target="tpu_custom_call" | custom-call | tf_op jit(solution)/shard_map/near/pallas_call | solution.py:274
  12.4 0.0 collective-permute-done.1.far_ref
  12.4 1.1 %far.1 = (f32[16,4,128]{2,1,0:T(4,128)}, bf16[2,384,128]{2,1,0:T(8,128)(2,1)S(1)}, bf16[2,384,128]{2,1,0:T(8,128)(2,1)S(1)}) custom-call(bf16[384,256]{1,0:T(8,128)(2,1)S(1)} %get-tuple-element.27.q_ref, bf16[384,256]{1,0:T(8,128)(2,1)S(1)} %get-tuple-element.29.g_ref, bf16[2,64,256]{2,1,0:T(8,128)(2,1)S(1)} %collective-permute-done.1.far_ref, ...), custom_call_target="tpu_custom_call" | custom-call | tf_op jit(solution)/shard_map/far/pallas_call | solution.py:274
  13.5 11.1 %all-to-all-start = ((f32[16,4,128]{2,1,0:T(4,128)}), f32[16,4,128]{2,1,0:T(4,128)S(1)}, u32[]{:S(2)}, u32[]{:S(2)}) async-start(f32[16,4,128]{2,1,0:T(4,128)} %get-tuple-element.49), calls=%async_computation | async-start | bytes 65536 | tf_op jit(solution)/shard_map/all_to_all | solution.py:297
  24.6 0.2 back.1
  24.9 1.3 %collective-permute-start.2 = (bf16[2,256,256]{2,1,0:T(8,128)(2,1)S(1)}, bf16[2,256,256]{2,1,0:T(8,128)(2,1)S(1)}, u32[]{:S(2)}, u32[]{:S(2)}) collective-permute-start(bf16[2,256,256]{2,1,0:T(8,128)(2,1)S(1)} %back.1), channel_id=1, source_target_pairs={{8,0},{16,8},{24,16},{32,24},{40,32},{48,40},{56,48},{64,56},{72,6... | collective-permute-start | bytes 786440 | tf_op jit(solution)/shard_map/ppermute | solution.py:362
  26.2 1.1 %all-to-all-done = f32[16,4,128]{2,1,0:T(4,128)S(1)} async-done(((f32[16,4,128]{2,1,0:T(4,128)}), f32[16,4,128]{2,1,0:T(4,128)S(1)}, u32[]{:S(2)}, u32[]{:S(2)}) %all-to-all-start) | async-done | bytes 32800 | tf_op jit(solution)/shard_map/all_to_all | solution.py:297
  27.2 0.7 %broadcast_in_dim.3 = f32[32,8,128]{2,1,0:T(8,128)} broadcast(f32[8,128]{1,0:T(8,128)S(1)} %bitcast_reduce_fusion), dimensions={1,2} | broadcast | bytes 135168 | tf_op jit(solution)/shard_map/broadcast_in_dim | solution.py:364
  27.9 15.4 %all-to-all-start.1 = ((f32[32,8,128]{2,1,0:T(8,128)}), f32[32,8,128]{2,1,0:T(8,128)S(1)}, u32[]{:S(2)}, u32[]{:S(2)}) async-start(f32[32,8,128]{2,1,0:T(8,128)} %broadcast_in_dim.3), calls=%async_computation.1 | async-start | bytes 262144 | tf_op jit(solution)/shard_map/all_to_all | solution.py:297
  43.3 0.0 collective-permute-done.2.back_ref
  43.3 1.1 %join.1 = (bf16[384,256]{1,0:T(8,128)(2,1)}, bf16[384,256]{1,0:T(8,128)(2,1)}, bf16[384,256]{1,0:T(8,128)(2,1)}) custom-call(bf16[384,256]{1,0:T(8,128)(2,1)S(1)} %get-tuple-element.27.q_ref, bf16[384,256]{1,0:T(8,128)(2,1)S(1)} %get-tuple-element.28.k_ref, bf16[384,256]{1,0:T(8,128)(2,1)S(1)} %get-tuple-element.29.g_ref, ...), custom_call_target="tpu_custom_call" | custom-call | tf_op jit(solution)/shard_map/join/pallas_call | solution.py:274
  44.4 2.8 %all-to-all-done.1 = f32[32,8,128]{2,1,0:T(8,128)S(1)} async-done(((f32[32,8,128]{2,1,0:T(8,128)}), f32[32,8,128]{2,1,0:T(8,128)S(1)}, u32[]{:S(2)}, u32[]{:S(2)}) %all-to-all-start.1) | async-done | bytes 131104 | tf_op jit(solution)/shard_map/all_to_all | solution.py:297
  47.1 0.7 %table.1 = f32[16,192]{1,0:T(8,128)} custom-call(f32[8,32,128]{2,1,0:T(8,128)S(1)} %bitcast.11), custom_call_target="tpu_custom_call" | custom-call | tf_op jit(solution)/shard_map/table/pallas_call | solution.py:274
  (1 shorter events, 0.0 us)
Async XLA Ops:
  1.6 9.6 %collective-permute-start = (bf16[2,192,256]{2,1,0:T(8,128)(2,1)S(1)}, bf16[2,192,256]{2,1,0:T(8,128)(2,1)S(1)}, u32[]{:S(2)}, u32[]{:S(2)}) collective-permute-start(bf16[2,192,256]{2,1,0:T(8,128)(2,1)S(1)} %get-tuple-element.30), channel_id=1, source_target_pairs={{0,8},{8,16},{16,24},{24,32},{32,40},{40,48},{48,56},{56,64},{64,7... | collective-permute-start | bytes 589832 | tf_op jit(solution)/shard_map/ppermute | solution.py:317
  5.7 3.2 %copy-start = (f32[2,192]{1,0:T(2,128)S(1)}, f32[2,192]{1,0:T(2,128)}, u32[]{:S(2)}) copy-start(f32[2,192]{1,0:T(2,128)} %rb_ref.1) | copy-start | bytes 4612
  5.7 6.7 %collective-permute-start.1 = (bf16[2,64,256]{2,1,0:T(8,128)(2,1)S(1)}, bf16[2,64,256]{2,1,0:T(8,128)(2,1)S(1)}, u32[]{:S(2)}, u32[]{:S(2)}) collective-permute-start(bf16[2,64,256]{2,1,0:T(8,128)(2,1)S(1)} %get-tuple-element.31), channel_id=1, source_target_pairs={{0,8},{8,16},{16,24},{24,32},{32,40},{40,48},{48,56},{56,64},{64,7... | collective-permute-start | bytes 196616 | tf_op jit(solution)/shard_map/ppermute | solution.py:318
  13.5 13.7 %all-to-all-start = ((f32[16,4,128]{2,1,0:T(4,128)}), f32[16,4,128]{2,1,0:T(4,128)S(1)}, u32[]{:S(2)}, u32[]{:S(2)}) async-start(f32[16,4,128]{2,1,0:T(4,128)} %get-tuple-element.49), calls=%async_computation | async-start | bytes 65536 | tf_op jit(solution)/shard_map/all_to_all | solution.py:297
  24.9 18.4 %collective-permute-start.2 = (bf16[2,256,256]{2,1,0:T(8,128)(2,1)S(1)}, bf16[2,256,256]{2,1,0:T(8,128)(2,1)S(1)}, u32[]{:S(2)}, u32[]{:S(2)}) collective-permute-start(bf16[2,256,256]{2,1,0:T(8,128)(2,1)S(1)} %back.1), channel_id=1, source_target_pairs={{8,0},{16,8},{24,16},{32,24},{40,32},{48,40},{56,48},{64,56},{72,6... | collective-permute-start | bytes 786440 | tf_op jit(solution)/shard_map/ppermute | solution.py:362
  27.9 19.3 %all-to-all-start.1 = ((f32[32,8,128]{2,1,0:T(8,128)}), f32[32,8,128]{2,1,0:T(8,128)S(1)}, u32[]{:S(2)}, u32[]{:S(2)}) async-start(f32[32,8,128]{2,1,0:T(8,128)} %broadcast_in_dim.3), calls=%async_computation.1 | async-start | bytes 262144 | tf_op jit(solution)/shard_map/all_to_all | solution.py:297

commit v6 on v5

--- a/solution.py
+++ b/solution.py
@@ -23,6 +23,7 @@
 VMEM = pl.BlockSpec(memory_space=pltpu.VMEM)
 HBM = pl.BlockSpec(memory_space=pltpu.HBM)
 AXES = ("z", "y", "x", "c")
+ORDERS = {"z": (5, 3, 2, 1, 0, 4, 7, 6), "y": (4, 5, 3, 6, 2, 7, 1, 0), "x": (2, 1, 3, 0), "c": (1, 0)}
 
 
 def dot(a, b, ca, cb):
@@ -203,7 +204,8 @@
 
 
 def far_body(
-    q_ref, g_ref, far_ref, tab_ref, pay_in, expo_ref, dp_ref, stat_ref, pay_ref, prob_ref, low_ref
+    q_ref, g_ref, far_ref, tab_ref, pay_in, expo_ref, dp_ref, stat_ref, part_ref,
+    pay_hbm, prob_ref, low_ref, back_ref, pay_ref, sem,
 ):
     hidden = hidden_keys()
     pay = []
@@ -224,15 +226,15 @@
         pay.append(skew_sum(*cut(grad)))
     total = jnp.concatenate(pay, axis=0) + pay_in[...]
     pay_ref[...] = jnp.broadcast_to(total[None], pay_ref.shape)
-
-
-def back_body(q_ref, g_ref, part_ref, prob_ref, low_ref, back_ref):
+    copy = pltpu.make_async_copy(pay_ref, pay_hbm, sem)
+    copy.start()
     for h in range(HEADS):
         hs = head(h)
         for i, (w, x) in enumerate(((low_ref, q_ref), (prob_ref, g_ref))):
             out = dot(w[h, : 2 * BLK, :], x[:BLK, hs], 1, 0)
             back_ref[i, :BLK, hs] = out[:BLK].astype(BF16)
             back_ref[i, BLK:, hs] = (out[BLK:] + part_ref[i, :BLK, hs]).astype(BF16)
+    copy.wait()
 
 
 def join_body(
@@ -253,12 +255,15 @@
             out[:BLK, hs] = (own + part_ref[i, BLK : 2 * BLK, hs]).astype(BF16)
 
 
-def table_body(order, x_ref, o_ref, sum_ref):
+def table_body(x_order, c_order, x_ref, o_ref, sum_ref):
     heads = o_ref.shape[0]
     total = jnp.sum(x_ref[...], axis=0)
-    span = total.shape[0] // len(order)
-    for i, at in enumerate(order):
-        sum_ref[at * span : (at + 1) * span, :] = total[i * span : (i + 1) * span]
+    cores = len(c_order)
+    span = total.shape[0] // (len(x_order) * cores)
+    for i, x in enumerate(x_order):
+        for j, c in enumerate(c_order):
+            at, to = (i * cores + j) * span, (x * cores + c) * span
+            sum_ref[to : to + span, :] = total[at : at + span]
     low = sum_ref[pl.ds(0, heads, stride=2), :]
     mid = sum_ref[pl.ds(1, heads, stride=2), :]
     lane = lax.broadcasted_iota(jnp.int32, low.shape, 1)
@@ -270,20 +275,20 @@
     o_ref[:, BLK:] = last[:, : BUCKETS - BLK]
 
 
-def call(body, name, outs, args, spaces=None, scratch=(), mib=8):
+def call(body, name, outs, args, spaces=None, scratch=(), mib=8, outputs=None):
     return pl.pallas_call(
         body,
         out_shape=tuple(jax.ShapeDtypeStruct(*o) for o in outs),
         in_specs=spaces or [VMEM] * len(args),
-        out_specs=(VMEM,) * len(outs),
+        out_specs=outputs or (VMEM,) * len(outs),
         scratch_shapes=scratch,
         compiler_params=pltpu.CompilerParams(vmem_limit_bytes=mib << 20),
         name=name,
     )(*args)
 
 
-def ordered(count, first):
-    return [(first + i) % count for i in range(count)]
+def late_first(count, order):
+    return [i for i in order if i < count] + [i for i in range(count) if i not in order]
 
 
 def exchange(x, size, outer, inner):
@@ -346,19 +351,21 @@
         (q, k, v, g, near, table, mid, pay),
     )
     group = size["y"] * size["c"]
-    z_order, y_order, x_order = [5,0,1,7,2,6,3,4], ordered(size["y"], 4), ordered(size["x"], 2)
-    pay, prob, low = call(
+    z_order, y_order, x_order, c_order = (late_first(size[a], ORDERS[a]) for a in AXES)
+    pay, prob, low, back = call(
         far_body,
         "far",
         [
             ((group, 2 * HEADS, BLK), F32),
             ((HEADS, 3 * BLK, BLK), BF16),
             ((HEADS, 3 * BLK, BLK), BF16),
+            ((2, 2 * BLK, width), BF16),
         ],
-        (q, g, far, table, pay, expo, dp, stat),
-    )
-    pay = exchange(pay, size, ("y", y_order), ("c", range(size["c"])))
-    (back,) = call(back_body, "back", [((2, 2 * BLK, width), BF16)], (q, g, part, prob, low))
+        (q, g, far, table, pay, expo, dp, stat, part),
+        scratch=[pltpu.VMEM((group, 2 * HEADS, BLK), F32), pltpu.SemaphoreType.DMA],
+        outputs=(HBM, VMEM, VMEM, VMEM),
+    )
+    pay = exchange(pay, size, ("y", y_order), ("c", c_order))
     back = lax.ppermute(back, ("z", "y"), [(s + 1, s) for s in range(count - 1)])
     pay = pay.reshape(size["y"], size["c"] * 2 * HEADS, BLK).sum(axis=0)
     pay = jnp.broadcast_to(pay, (size["z"] * size["x"], *pay.shape))
@@ -370,7 +377,7 @@
         (q, k, g, near, far, part, end, prob, low, dq1, dq2, back),
     )
     (bias,) = call(
-        functools.partial(table_body, x_order),
+        functools.partial(table_body, x_order, c_order),
         "table",
         [((size["x"] * size["c"] * HEADS, BUCKETS), F32)],
         (pay.reshape(size["z"], size["x"] * size["c"] * 2 * HEADS, BLK),),

time: 48.5 us -> 47.9 us (0.988)
  starting transfers between devices: 35 us -> 33.2 us
  waiting for transfers between devices: 3.86 us -> 5.53 us
    all_to_all x2, starting transfers between devices: 26.5 us -> 24.7 us  [exchange(): lax.all_to_all(x, AXES, split_axis=0, concat_axis=0, axis_index_groups=gr...]
    all_to_all x2, waiting for transfers between devices: 3.85 us -> 5.52 us  [exchange(): lax.all_to_all(x, AXES, split_axis=0, concat_axis=0, axis_index_groups=gr...]
    pallas_call x7 -> x6, Pallas kernels: 7.58 us -> 7.4 us  [call(): pl.pallas_call(body, out_shape=tuple((jax.ShapeDtypeStruct(*o) for o in o...]
where the time goes in v6:
time: 47.9 us; the launch traced here: 47.5 us
  starting transfers between devices  33.2 us (69%)
  Pallas kernels  7.4 us (15%)
  waiting for transfers between devices  5.53 us (12%)
  between operations  0.74 us (2%)
  local copies, waits for them, and re-layouts  0.66 us (1%)
    all_to_all x2, starting transfers between devices, exchange(): lax.all_to_all(x, AXES, split_axis=0, concat_axis=0, axis_index_groups=gr...  24.7 us
    pallas_call x6, Pallas kernels, call(): pl.pallas_call(body, out_shape=tuple((jax.ShapeDtypeStruct(*o) for o in o...  7.4 us
    all_to_all x2, waiting for transfers between devices, exchange(): lax.all_to_all(x, AXES, split_axis=0, concat_axis=0, axis_index_groups=gr...  5.52 us
    ppermute x1, starting transfers between devices, local(): near = lax.ppermute(near, ('z', 'y'), ahead)  4.03 us
    ppermute x1, starting transfers between devices, local(): far = lax.ppermute(far, ('z', 'y'), ahead)  3.2 us
    ppermute x1, starting transfers between devices, local(): lax.ppermute(back, ('z', 'y'), [(s + 1, s) for s in range(count - 1)])  1.28 us
  transfers between devices with their start and end apart: 5, of which 2 were waited for; matrix products, arithmetic and copies ran while one was open for 1% of the time, Pallas kernels for 10%

profile of v6, /device:TPU:1, one launch (start us, length us, event | category | flops | bytes accessed | tf_op | source)
XLA Modules:
  0.0 47.5 jit_solution(5363724750147974322)
XLA Ops:
  0.6 1.0 %tails.1 = (bf16[2,192,256]{2,1,0:T(8,128)(2,1)S(1)}, bf16[2,64,256]{2,1,0:T(8,128)(2,1)S(1)}) custom-call(bf16[384,256]{1,0:T(8,128)(2,1)} %bitcast.12, bf16[384,256]{1,0:T(8,128)(2,1)} %bitcast.14), custom_call_target="tpu_custom_call" | custom-call | tf_op jit(solution)/shard_map/tails/pallas_call | solution.py:279
  1.6 4.0 %collective-permute-start = (bf16[2,192,256]{2,1,0:T(8,128)(2,1)S(1)}, bf16[2,192,256]{2,1,0:T(8,128)(2,1)S(1)}, u32[]{:S(2)}, u32[]{:S(2)}) collective-permute-start(bf16[2,192,256]{2,1,0:T(8,128)(2,1)S(1)} %get-tuple-element.31), channel_id=1, source_target_pairs={{0,8},{8,16},{16,24},{24,32},{32,40},{40,48},{48,56},{56,64},{64,7... | collective-permute-start | bytes 589832 | tf_op jit(solution)/shard_map/ppermute | solution.py:322
  5.7 0.0 copy-start
  5.7 3.2 %collective-permute-start.1 = (bf16[2,64,256]{2,1,0:T(8,128)(2,1)S(1)}, bf16[2,64,256]{2,1,0:T(8,128)(2,1)S(1)}, u32[]{:S(2)}, u32[]{:S(2)}) collective-permute-start(bf16[2,64,256]{2,1,0:T(8,128)(2,1)S(1)} %get-tuple-element.32), channel_id=1, source_target_pairs={{0,8},{8,16},{16,24},{24,32},{32,40},{40,48},{48,56},{56,64},{64,7... | collective-permute-start | bytes 196616 | tf_op jit(solution)/shard_map/ppermute | solution.py:323
  8.9 0.0 copy-done
  8.9 2.3 %own.1 = (bf16[384,256]{1,0:T(8,128)(2,1)S(1)}, bf16[384,256]{1,0:T(8,128)(2,1)S(1)}, bf16[384,256]{1,0:T(8,128)(2,1)S(1)}, bf16[384,256]{1,0:T(8,128)(2,1)S(1)}...) custom-call(bf16[384,256]{1,0:T(8,128)(2,1)} %bitcast.16, ...), custom_call_target="tpu_custom_call" | custom-call | tf_op jit(solution)/shard_map/own/pallas_call | solution.py:279
  11.2 0.0 collective-permute-done.near_ref
  11.2 1.1 %near.1 = (bf16[128,256]{1,0:T(8,128)(2,1)S(1)}, f32[2,384,256]{2,1,0:T(8,128)S(1)}, f32[4,128]{1,0:T(4,128)S(1)}, f32[2,320,128]{2,1,0:T(8,128)S(1)}, f32[2,320,128]{2,1,0:T(8,128)S(1)}, /*index=5*/f32[8,128]{1,0:T(8,128)S(1)}) custom-call(bf16[384,256]{1,0:T(8,128)(2,1)S(1)} %get-tuple-element.28.q_ref, bf16[384,256]{1,0:T(8,128)(2,1)S(1)} %get-tuple-element.29.k_ref, ...), custom_call_target="tpu_custom_call" | custom-call | tf_op jit(solution)/shard_map/near/pallas_call | solution.py:279
  12.4 0.0 collective-permute-done.1.far_ref
  12.4 1.2 %far.1 = (f32[16,4,128]{2,1,0:T(4,128)}, bf16[2,384,128]{2,1,0:T(8,128)(2,1)S(1)}, bf16[2,384,128]{2,1,0:T(8,128)(2,1)S(1)}, bf16[2,256,256]{2,1,0:T(8,128)(2,1)S(1)}) custom-call(bf16[384,256]{1,0:T(8,128)(2,1)S(1)} %get-tuple-element.28.q_ref, bf16[384,256]{1,0:T(8,128)(2,1)S(1)} %get-tuple-element.30.g_ref, ...), custom_call_target="tpu_custom_call" | custom-call | tf_op jit(solution)/shard_map/far/pallas_call | solution.py:279
  13.6 9.3 %all-to-all-start = ((f32[16,4,128]{2,1,0:T(4,128)}), f32[16,4,128]{2,1,0:T(4,128)S(1)}, u32[]{:S(2)}, u32[]{:S(2)}) async-start(f32[16,4,128]{2,1,0:T(4,128)} %get-tuple-element.51), calls=%async_computation | async-start | bytes 65536 | tf_op jit(solution)/shard_map/all_to_all | solution.py:302
  22.9 1.3 %collective-permute-start.2 = (bf16[2,256,256]{2,1,0:T(8,128)(2,1)S(1)}, bf16[2,256,256]{2,1,0:T(8,128)(2,1)S(1)}, u32[]{:S(2)}, u32[]{:S(2)}) collective-permute-start(bf16[2,256,256]{2,1,0:T(8,128)(2,1)S(1)} %get-tuple-element.47), channel_id=1, source_target_pairs={{8,0},{16,8},{24,16},{32,24},{40,32},{48,40},{56,48},{64,56},{72,6... | collective-permute-start | bytes 786440 | tf_op jit(solution)/shard_map/ppermute | solution.py:369
  24.1 2.3 %all-to-all-done = f32[16,4,128]{2,1,0:T(4,128)S(1)} async-done(((f32[16,4,128]{2,1,0:T(4,128)}), f32[16,4,128]{2,1,0:T(4,128)S(1)}, u32[]{:S(2)}, u32[]{:S(2)}) %all-to-all-start) | async-done | bytes 32800 | tf_op jit(solution)/shard_map/all_to_all | solution.py:302
  26.5 0.7 %broadcast_in_dim.3 = f32[32,8,128]{2,1,0:T(8,128)} broadcast(f32[8,128]{1,0:T(8,128)S(1)} %bitcast_reduce_fusion), dimensions={1,2} | broadcast | bytes 135168 | tf_op jit(solution)/shard_map/broadcast_in_dim | solution.py:371
  27.1 15.4 %all-to-all-start.1 = ((f32[32,8,128]{2,1,0:T(8,128)}), f32[32,8,128]{2,1,0:T(8,128)S(1)}, u32[]{:S(2)}, u32[]{:S(2)}) async-start(f32[32,8,128]{2,1,0:T(8,128)} %broadcast_in_dim.3), calls=%async_computation.1 | async-start | bytes 262144 | tf_op jit(solution)/shard_map/all_to_all | solution.py:302
  42.5 0.0 collective-permute-done.2.back_ref
  42.5 1.1 %join.1 = (bf16[384,256]{1,0:T(8,128)(2,1)}, bf16[384,256]{1,0:T(8,128)(2,1)}, bf16[384,256]{1,0:T(8,128)(2,1)}) custom-call(bf16[384,256]{1,0:T(8,128)(2,1)S(1)} %get-tuple-element.28.q_ref, bf16[384,256]{1,0:T(8,128)(2,1)S(1)} %get-tuple-element.29.k_ref, bf16[384,256]{1,0:T(8,128)(2,1)S(1)} %get-tuple-element.30.g_ref, ...), custom_call_target="tpu_custom_call" | custom-call | tf_op jit(solution)/shard_map/join/pallas_call | solution.py:279
  43.6 3.2 %all-to-all-done.1 = f32[32,8,128]{2,1,0:T(8,128)S(1)} async-done(((f32[32,8,128]{2,1,0:T(8,128)}), f32[32,8,128]{2,1,0:T(8,128)S(1)}, u32[]{:S(2)}, u32[]{:S(2)}) %all-to-all-start.1) | async-done | bytes 131104 | tf_op jit(solution)/shard_map/all_to_all | solution.py:302
  46.8 0.7 %table.1 = f32[16,192]{1,0:T(8,128)} custom-call(f32[8,32,128]{2,1,0:T(8,128)S(1)} %bitcast.11), custom_call_target="tpu_custom_call" | custom-call | tf_op jit(solution)/shard_map/table/pallas_call | solution.py:279
  (1 shorter events, 0.0 us)
Async XLA Ops:
  1.6 9.6 %collective-permute-start = (bf16[2,192,256]{2,1,0:T(8,128)(2,1)S(1)}, bf16[2,192,256]{2,1,0:T(8,128)(2,1)S(1)}, u32[]{:S(2)}, u32[]{:S(2)}) collective-permute-start(bf16[2,192,256]{2,1,0:T(8,128)(2,1)S(1)} %get-tuple-element.31), channel_id=1, source_target_pairs={{0,8},{8,16},{16,24},{24,32},{32,40},{40,48},{48,56},{56,64},{64,7... | collective-permute-start | bytes 589832 | tf_op jit(solution)/shard_map/ppermute | solution.py:322
  5.7 3.2 %copy-start = (f32[2,192]{1,0:T(2,128)S(1)}, f32[2,192]{1,0:T(2,128)}, u32[]{:S(2)}) copy-start(f32[2,192]{1,0:T(2,128)} %rb_ref.1) | copy-start | bytes 4612
  5.7 6.7 %collective-permute-start.1 = (bf16[2,64,256]{2,1,0:T(8,128)(2,1)S(1)}, bf16[2,64,256]{2,1,0:T(8,128)(2,1)S(1)}, u32[]{:S(2)}, u32[]{:S(2)}) collective-permute-start(bf16[2,64,256]{2,1,0:T(8,128)(2,1)S(1)} %get-tuple-element.32), channel_id=1, source_target_pairs={{0,8},{8,16},{16,24},{24,32},{32,40},{40,48},{48,56},{56,64},{64,7... | collective-permute-start | bytes 196616 | tf_op jit(solution)/shard_map/ppermute | solution.py:323
  13.6 12.9 %all-to-all-start = ((f32[16,4,128]{2,1,0:T(4,128)}), f32[16,4,128]{2,1,0:T(4,128)S(1)}, u32[]{:S(2)}, u32[]{:S(2)}) async-start(f32[16,4,128]{2,1,0:T(4,128)} %get-tuple-element.51), calls=%async_computation | async-start | bytes 65536 | tf_op jit(solution)/shard_map/all_to_all | solution.py:302
  22.9 19.6 %collective-permute-start.2 = (bf16[2,256,256]{2,1,0:T(8,128)(2,1)S(1)}, bf16[2,256,256]{2,1,0:T(8,128)(2,1)S(1)}, u32[]{:S(2)}, u32[]{:S(2)}) collective-permute-start(bf16[2,256,256]{2,1,0:T(8,128)(2,1)S(1)} %get-tuple-element.47), channel_id=1, source_target_pairs={{8,0},{16,8},{24,16},{32,24},{40,32},{48,40},{56,48},{64,56},{72,6... | collective-permute-start | bytes 786440 | tf_op jit(solution)/shard_map/ppermute | solution.py:369
  27.1 19.7 %all-to-all-start.1 = ((f32[32,8,128]{2,1,0:T(8,128)}), f32[32,8,128]{2,1,0:T(8,128)S(1)}, u32[]{:S(2)}, u32[]{:S(2)}) async-start(f32[32,8,128]{2,1,0:T(8,128)} %broadcast_in_dim.3), calls=%async_computation.1 | async-start | bytes 262144 | tf_op jit(solution)/shard_map/all_to_all | solution.py:302

commit v7 on v6

--- a/solution.py
+++ b/solution.py
@@ -15,6 +15,8 @@
 BUCKETS = 192
 HEADS = 2
 BLK = 128
+FAR = 96
+LEAD = BLK - FAR
 SCALE = HEAD_DIM**-0.5
 LOG2E = 1.4426950408889634
 NEG = -1e30
@@ -167,31 +169,26 @@
 
 
 def near_body(
-    q_ref, k_ref, v_ref, g_ref, near_ref, tab_ref, mid_in, pay_in,
-    dq_ref, part_ref, pay_ref, expo_ref, dp_ref, stat_ref,
+    q_ref, k_ref, v_ref, g_ref, near_ref, tab_ref, pay_in,
+    prob_ref, low_ref, pay_ref, expo_ref, dp_ref, stat_ref,
 ):
     hidden = hidden_keys()
     for h in range(HEADS):
         hs = head(h)
         table = [tab_ref[3 * h + m] for m in range(3)]
-        k = stack([near_ref[0, :, hs], k_ref[: 2 * BLK, hs]])
-        v = stack([near_ref[1, :, hs], v_ref[: 2 * BLK, hs]])
         q = q_ref[: 2 * BLK, hs]
         g = g_ref[: 2 * BLK, hs]
-        raw = dot(k, q, 1, 1)
-        dps = dot(v, g, 1, 1)
-        scores = [s * (SCALE * LOG2E) + t for s, t in zip(cut(raw[SEG:, BLK:]), [table[0] + hidden] + table[1:])]
-        dp = cut(dps[SEG:, BLK:])
+        raw = dot(stack([near_ref[0, :, hs], k_ref[: 2 * BLK, hs]]), q, 1, 1)
+        dps = dot(stack([near_ref[1, :, hs], v_ref[: 2 * BLK, hs]]), g, 1, 1)
+        scores = [s * (SCALE * LOG2E) + t for s, t in zip(cut(raw[LEAD:, BLK:]), [table[0] + hidden] + table[1:])]
+        dp = cut(dps[LEAD:, BLK:])
         expo, _, total, mixed = weights(scores, dp)
         inv = 1.0 / total
         prob, low, grad = softmax_grad(expo, dp, [inv] * 3, mixed * inv)
-        low = stack(low)
-        dq_ref[:, hs] = dot(low, k[SEG:], 0, 0).astype(BF16)
-        for i, out in enumerate((dot(low, q[BLK:], 1, 0), dot(stack(prob), g[BLK:], 1, 0))):
-            part_ref[i, :BLK, hs] = out[:BLK]
-            part_ref[i, BLK:, hs] = out[BLK:] + mid_in[i, :, hs]
+        prob_ref[h] = stack(prob)
+        low_ref[h] = stack(low)
         pay_ref[2 * h : 2 * h + 2, :] = skew_sum(*grad) + pay_in[2 * h : 2 * h + 2, :]
-        shift = stack([table[0][SEG:] + hidden, table[1] + hidden, table[2]])
+        shift = stack([table[0][FAR:] + hidden, table[1] + hidden, table[2]])
         rows = shift.shape[0]
         score = raw[:rows, :BLK] * (SCALE * LOG2E) + shift
         dp = dps[:rows, :BLK]
@@ -204,14 +201,14 @@
 
 
 def far_body(
-    q_ref, g_ref, far_ref, tab_ref, pay_in, expo_ref, dp_ref, stat_ref, part_ref,
+    q_ref, g_ref, far_ref, tab_ref, pay_in, expo_ref, dp_ref, stat_ref, prob1_ref, low1_ref,
     pay_hbm, prob_ref, low_ref, back_ref, pay_ref, sem,
 ):
     hidden = hidden_keys()
     pay = []
     for h in range(HEADS):
         hs = head(h)
-        score = dot(far_ref[0, :, hs], q_ref[:BLK, hs], 1, 1) * (SCALE * LOG2E) + (tab_ref[3 * h, :SEG, :] + hidden)
+        score = dot(far_ref[0, :, hs], q_ref[:BLK, hs], 1, 1) * (SCALE * LOG2E) + (tab_ref[3 * h, :FAR, :] + hidden)
         dp = dot(far_ref[1, :, hs], g_ref[:BLK, hs], 1, 1)
         peak, total, mixed = (stat_ref[3 * h + i : 3 * h + i + 1, :] for i in range(3))
         top = jnp.maximum(peak, score.max(axis=0, keepdims=True))
@@ -230,29 +227,33 @@
     copy.start()
     for h in range(HEADS):
         hs = head(h)
-        for i, (w, x) in enumerate(((low_ref, q_ref), (prob_ref, g_ref))):
-            out = dot(w[h, : 2 * BLK, :], x[:BLK, hs], 1, 0)
-            back_ref[i, :BLK, hs] = out[:BLK].astype(BF16)
-            back_ref[i, BLK:, hs] = (out[BLK:] + part_ref[i, :BLK, hs]).astype(BF16)
+        pairs = ((low_ref, low1_ref, q_ref), (prob_ref, prob1_ref, g_ref))
+        for i, (w0, w1, x) in enumerate(pairs):
+            both = jnp.concatenate([w0[h, BLK : 2 * BLK, :], w1[h, :BLK, :]], axis=1)
+            back_ref[i, :BLK, hs] = dot(w0[h, :BLK, :], x[:BLK, hs], 1, 0).astype(BF16)
+            back_ref[i, BLK:, hs] = dot(both, x[: 2 * BLK, hs], 1, 0).astype(BF16)
     copy.wait()
 
 
 def join_body(
-    q_ref, k_ref, g_ref, near_ref, far_ref, part_ref, end_ref, prob_ref, low_ref, dq1_ref, dq2_ref, back_ref,
+    q_ref, k_ref, g_ref, near_ref, far_ref, mid_ref, end_ref,
+    prob_ref, low_ref, prob1_ref, low1_ref, dq2_ref, back_ref,
     dq_ref, dk_ref, dv_ref,
 ):
-    dq_ref[BLK : 2 * BLK, :] = dq1_ref[...]
     dq_ref[2 * BLK :, :] = dq2_ref[...]
-    for i, out in enumerate((dk_ref, dv_ref)):
-        out[BLK : 2 * BLK, :] = (part_ref[i, 2 * BLK :, :] + back_ref[i, :BLK, :].astype(F32)).astype(BF16)
-        out[2 * BLK :, :] = (end_ref[i] + back_ref[i, BLK:, :].astype(F32)).astype(BF16)
-    for h in range(HEADS):
-        hs = head(h)
-        keys = stack([far_ref[0, :, hs], near_ref[0, :, hs], k_ref[:BLK, hs]])
-        dq_ref[:BLK, hs] = dot(low_ref[h], keys, 0, 0).astype(BF16)
-        for i, (out, w, x) in enumerate(((dk_ref, low_ref, q_ref), (dv_ref, prob_ref, g_ref))):
-            own = dot(w[h, 2 * BLK :, :], x[:BLK, hs], 1, 0)
-            out[:BLK, hs] = (own + part_ref[i, BLK : 2 * BLK, hs]).astype(BF16)
+    for h in range(HEADS):
+        hs = head(h)
+        keys = stack([far_ref[0, :, hs], near_ref[0, :, hs], k_ref[: 2 * BLK, hs]])
+        dq_ref[:BLK, hs] = dot(low_ref[h], keys[: 3 * BLK], 0, 0).astype(BF16)
+        dq_ref[BLK : 2 * BLK, hs] = dot(low1_ref[h], keys[BLK:], 0, 0).astype(BF16)
+        pairs = ((dk_ref, low_ref, low1_ref, q_ref), (dv_ref, prob_ref, prob1_ref, g_ref))
+        for i, (out, w0, w1, x) in enumerate(pairs):
+            both = jnp.concatenate([w0[h, 2 * BLK :, :], w1[h, BLK : 2 * BLK, :]], axis=1)
+            first = dot(both, x[: 2 * BLK, hs], 1, 0) + mid_ref[i, :BLK, hs]
+            second = dot(w1[h, 2 * BLK :, :], x[BLK : 2 * BLK, hs], 1, 0) + mid_ref[i, BLK:, hs]
+            out[:BLK, hs] = first.astype(BF16)
+            out[BLK : 2 * BLK, hs] = (second + back_ref[i, :BLK, hs].astype(F32)).astype(BF16)
+            out[2 * BLK :, hs] = (end_ref[i, :, hs] + back_ref[i, BLK:, hs].astype(F32)).astype(BF16)
 
 
 def table_body(x_order, c_order, x_ref, o_ref, sum_ref):
@@ -312,7 +313,7 @@
     near, far = call(
         tails_body,
         "tails",
-        [((2, LEFT * SEG - SEG, width), BF16), ((2, SEG, width), BF16)],
+        [((2, LEFT * SEG - FAR, width), BF16), ((2, FAR, width), BF16)],
         (k, v),
         [HBM] * 2,
         [pltpu.SemaphoreType.DMA((4,))],
@@ -336,19 +337,13 @@
         [HBM] * 4 + [VMEM],
         [pltpu.VMEM((8, 2 * BLK), F32), pltpu.SemaphoreType.DMA((4,))],
     )
-    seen = (HEADS, 2 * BLK + SEG, BLK)
-    dq1, part, pay, expo, dp, stat = call(
+    seen = (HEADS, 2 * BLK + LEAD, BLK)
+    kept = ((HEADS, 3 * BLK, BLK), BF16)
+    prob1, low1, pay, expo, dp, stat = call(
         near_body,
         "near",
-        [
-            ((BLK, width), BF16),
-            ((2, 3 * BLK, width), F32),
-            ((2 * HEADS, BLK), F32),
-            (seen, F32),
-            (seen, F32),
-            ((8, BLK), F32),
-        ],
-        (q, k, v, g, near, table, mid, pay),
+        [kept, kept, ((2 * HEADS, BLK), F32), (seen, F32), (seen, F32), ((8, BLK), F32)],
+        (q, k, v, g, near, table, pay),
     )
     group = size["y"] * size["c"]
     z_order, y_order, x_order, c_order = (late_first(size[a], ORDERS[a]) for a in AXES)
@@ -357,11 +352,11 @@
         "far",
         [
             ((group, 2 * HEADS, BLK), F32),
-            ((HEADS, 3 * BLK, BLK), BF16),
-            ((HEADS, 3 * BLK, BLK), BF16),
+            kept,
+            kept,
             ((2, 2 * BLK, width), BF16),
         ],
-        (q, g, far, table, pay, expo, dp, stat, part),
+        (q, g, far, table, pay, expo, dp, stat, prob1, low1),
         scratch=[pltpu.VMEM((group, 2 * HEADS, BLK), F32), pltpu.SemaphoreType.DMA],
         outputs=(HBM, VMEM, VMEM, VMEM),
     )
@@ -374,7 +369,7 @@
         join_body,
         "join",
         [((rows, width), BF16)] * 3,
-        (q, k, g, near, far, part, end, prob, low, dq1, dq2, back),
+        (q, k, g, near, far, mid, end, prob, low, prob1, low1, dq2, back),
     )
     (bias,) = call(
         functools.partial(table_body, x_order, c_order),

time: 47.9 us -> 47.5 us (level)
  waiting for transfers between devices: 5.53 us -> 4.99 us
    all_to_all x2, waiting for transfers between devices: 5.52 us -> 4.98 us  [exchange(): lax.all_to_all(x, AXES, split_axis=0, concat_axis=0, axis_index_groups=gr...]
  transfers between devices with their start and end apart: 5 -> 5, of which waited for: 2 -> 2; matrix products, arithmetic and copies ran while one was open for 1% -> 1% of each run, Pallas kernels for 10% -> 9%
where the time goes in v7:
time: 47.5 us; the launch traced here: 47.1 us
  starting transfers between devices  33.5 us (71%)
  Pallas kernels  7.17 us (15%)
  waiting for transfers between devices  4.99 us (11%)
  between operations  0.74 us (2%)
  local copies, waits for them, and re-layouts  0.66 us (1%)
    all_to_all x2, starting transfers between devices, exchange(): lax.all_to_all(x, AXES, split_axis=0, concat_axis=0, axis_index_groups=gr...  25 us
    pallas_call x6, Pallas kernels, call(): pl.pallas_call(body, out_shape=tuple((jax.ShapeDtypeStruct(*o) for o in o...  7.17 us
    all_to_all x2, waiting for transfers between devices, exchange(): lax.all_to_all(x, AXES, split_axis=0, concat_axis=0, axis_index_groups=gr...  4.98 us
    ppermute x1, starting transfers between devices, local(): near = lax.ppermute(near, ('z', 'y'), ahead)  4.03 us
    ppermute x1, starting transfers between devices, local(): far = lax.ppermute(far, ('z', 'y'), ahead)  3.2 us
    ppermute x1, starting transfers between devices, local(): lax.ppermute(back, ('z', 'y'), [(s + 1, s) for s in range(count - 1)])  1.28 us
  transfers between devices with their start and end apart: 5, of which 2 were waited for; matrix products, arithmetic and copies ran while one was open for 1% of the time, Pallas kernels for 9%

profile of v7, /device:TPU:1, one launch (start us, length us, event | category | flops | bytes accessed | tf_op | source)
XLA Modules:
  0.0 47.1 jit_solution(12252243323496131016)
XLA Ops:
  0.6 1.0 %tails.1 = (bf16[2,160,256]{2,1,0:T(8,128)(2,1)S(1)}, bf16[2,96,256]{2,1,0:T(8,128)(2,1)S(1)}) custom-call(bf16[384,256]{1,0:T(8,128)(2,1)} %bitcast.12, bf16[384,256]{1,0:T(8,128)(2,1)} %bitcast.14), custom_call_target="tpu_custom_call" | custom-call | tf_op jit(solution)/shard_map/tails/pallas_call | solution.py:280
  1.6 4.0 %collective-permute-start = (bf16[2,160,256]{2,1,0:T(8,128)(2,1)S(1)}, bf16[2,160,256]{2,1,0:T(8,128)(2,1)S(1)}, u32[]{:S(2)}, u32[]{:S(2)}) collective-permute-start(bf16[2,160,256]{2,1,0:T(8,128)(2,1)S(1)} %get-tuple-element.31), channel_id=1, source_target_pairs={{0,8},{8,16},{16,24},{24,32},{32,40},{40,48},{48,56},{56,64},{64,7... | collective-permute-start | bytes 491528 | tf_op jit(solution)/shard_map/ppermute | solution.py:323
  5.7 0.0 copy-start
  5.7 3.2 %collective-permute-start.1 = (bf16[2,96,256]{2,1,0:T(8,128)(2,1)S(1)}, bf16[2,96,256]{2,1,0:T(8,128)(2,1)S(1)}, u32[]{:S(2)}, u32[]{:S(2)}) collective-permute-start(bf16[2,96,256]{2,1,0:T(8,128)(2,1)S(1)} %get-tuple-element.32), channel_id=1, source_target_pairs={{0,8},{8,16},{16,24},{24,32},{32,40},{40,48},{48,56},{56,64},{64,7... | collective-permute-start | bytes 294920 | tf_op jit(solution)/shard_map/ppermute | solution.py:324
  8.9 0.0 copy-done
  8.9 2.3 %own.1 = (bf16[384,256]{1,0:T(8,128)(2,1)S(1)}, bf16[384,256]{1,0:T(8,128)(2,1)S(1)}, bf16[384,256]{1,0:T(8,128)(2,1)S(1)}, bf16[384,256]{1,0:T(8,128)(2,1)S(1)}...) custom-call(bf16[384,256]{1,0:T(8,128)(2,1)} %bitcast.16, ...), custom_call_target="tpu_custom_call" | custom-call | tf_op jit(solution)/shard_map/own/pallas_call | solution.py:280
  11.2 0.0 collective-permute-done.near_ref
  11.2 0.8 %near.1 = (bf16[2,384,128]{2,1,0:T(8,128)(2,1)S(1)}, bf16[2,384,128]{2,1,0:T(8,128)(2,1)S(1)}, f32[4,128]{1,0:T(4,128)S(1)}, f32[2,288,128]{2,1,0:T(8,128)S(1)},...) custom-call(bf16[384,256]{1,0:T(8,128)(2,1)S(1)} %get-tuple-element.28.q_ref, ...), custom_call_target="tpu_custom_call" | custom-call | tf_op jit(solution)/shard_map/near/pallas_call | solution.py:280
  12.0 0.0 collective-permute-done.1.far_ref
  12.0 1.2 %far.1 = (f32[16,4,128]{2,1,0:T(4,128)}, bf16[2,384,128]{2,1,0:T(8,128)(2,1)S(1)}, bf16[2,384,128]{2,1,0:T(8,128)(2,1)S(1)}, bf16[2,256,256]{2,1,0:T(8,128)(2,1)S(1)}) custom-call(bf16[384,256]{1,0:T(8,128)(2,1)S(1)} %get-tuple-element.28.q_ref, bf16[384,256]{1,0:T(8,128)(2,1)S(1)} %get-tuple-element.30.g_ref, ...), custom_call_target="tpu_custom_call" | custom-call | tf_op jit(solution)/shard_map/far/pallas_call | solution.py:280
  13.2 9.7 %all-to-all-start = ((f32[16,4,128]{2,1,0:T(4,128)}), f32[16,4,128]{2,1,0:T(4,128)S(1)}, u32[]{:S(2)}, u32[]{:S(2)}) async-start(f32[16,4,128]{2,1,0:T(4,128)} %get-tuple-element.51), calls=%async_computation | async-start | bytes 65536 | tf_op jit(solution)/shard_map/all_to_all | solution.py:303
  22.9 1.3 %collective-permute-start.2 = (bf16[2,256,256]{2,1,0:T(8,128)(2,1)S(1)}, bf16[2,256,256]{2,1,0:T(8,128)(2,1)S(1)}, u32[]{:S(2)}, u32[]{:S(2)}) collective-permute-start(bf16[2,256,256]{2,1,0:T(8,128)(2,1)S(1)} %get-tuple-element.47), channel_id=1, source_target_pairs={{8,0},{16,8},{24,16},{32,24},{40,32},{48,40},{56,48},{64,56},{72,6... | collective-permute-start | bytes 786440 | tf_op jit(solution)/shard_map/ppermute | solution.py:364
  24.2 1.9 %all-to-all-done = f32[16,4,128]{2,1,0:T(4,128)S(1)} async-done(((f32[16,4,128]{2,1,0:T(4,128)}), f32[16,4,128]{2,1,0:T(4,128)S(1)}, u32[]{:S(2)}, u32[]{:S(2)}) %all-to-all-start) | async-done | bytes 32800 | tf_op jit(solution)/shard_map/all_to_all | solution.py:303
  26.1 0.7 %broadcast_in_dim.3 = f32[32,8,128]{2,1,0:T(8,128)} broadcast(f32[8,128]{1,0:T(8,128)S(1)} %bitcast_reduce_fusion), dimensions={1,2} | broadcast | bytes 135168 | tf_op jit(solution)/shard_map/broadcast_in_dim | solution.py:366
  26.7 15.4 %all-to-all-start.1 = ((f32[32,8,128]{2,1,0:T(8,128)}), f32[32,8,128]{2,1,0:T(8,128)S(1)}, u32[]{:S(2)}, u32[]{:S(2)}) async-start(f32[32,8,128]{2,1,0:T(8,128)} %broadcast_in_dim.3), calls=%async_computation.1 | async-start | bytes 262144 | tf_op jit(solution)/shard_map/all_to_all | solution.py:303
  42.1 0.0 collective-permute-done.2.back_ref
  42.1 1.2 %join.1 = (bf16[384,256]{1,0:T(8,128)(2,1)}, bf16[384,256]{1,0:T(8,128)(2,1)}, bf16[384,256]{1,0:T(8,128)(2,1)}) custom-call(bf16[384,256]{1,0:T(8,128)(2,1)S(1)} %get-tuple-element.28.q_ref, bf16[384,256]{1,0:T(8,128)(2,1)S(1)} %get-tuple-element.29.k_ref, bf16[384,256]{1,0:T(8,128)(2,1)S(1)} %get-tuple-element.30.g_ref, ...), custom_call_target="tpu_custom_call" | custom-call | tf_op jit(solution)/shard_map/join/pallas_call | solution.py:280
  43.3 3.1 %all-to-all-done.1 = f32[32,8,128]{2,1,0:T(8,128)S(1)} async-done(((f32[32,8,128]{2,1,0:T(8,128)}), f32[32,8,128]{2,1,0:T(8,128)S(1)}, u32[]{:S(2)}, u32[]{:S(2)}) %all-to-all-start.1) | async-done | bytes 131104 | tf_op jit(solution)/shard_map/all_to_all | solution.py:303
  46.4 0.7 %table.1 = f32[16,192]{1,0:T(8,128)} custom-call(f32[8,32,128]{2,1,0:T(8,128)S(1)} %bitcast.11), custom_call_target="tpu_custom_call" | custom-call | tf_op jit(solution)/shard_map/table/pallas_call | solution.py:280
  (1 shorter events, 0.0 us)
Async XLA Ops:
  1.6 9.6 %collective-permute-start = (bf16[2,160,256]{2,1,0:T(8,128)(2,1)S(1)}, bf16[2,160,256]{2,1,0:T(8,128)(2,1)S(1)}, u32[]{:S(2)}, u32[]{:S(2)}) collective-permute-start(bf16[2,160,256]{2,1,0:T(8,128)(2,1)S(1)} %get-tuple-element.31), channel_id=1, source_target_pairs={{0,8},{8,16},{16,24},{24,32},{32,40},{40,48},{48,56},{56,64},{64,7... | collective-permute-start | bytes 491528 | tf_op jit(solution)/shard_map/ppermute | solution.py:323
  5.7 3.2 %copy-start = (f32[2,192]{1,0:T(2,128)S(1)}, f32[2,192]{1,0:T(2,128)}, u32[]{:S(2)}) copy-start(f32[2,192]{1,0:T(2,128)} %rb_ref.1) | copy-start | bytes 4612
  5.7 6.3 %collective-permute-start.1 = (bf16[2,96,256]{2,1,0:T(8,128)(2,1)S(1)}, bf16[2,96,256]{2,1,0:T(8,128)(2,1)S(1)}, u32[]{:S(2)}, u32[]{:S(2)}) collective-permute-start(bf16[2,96,256]{2,1,0:T(8,128)(2,1)S(1)} %get-tuple-element.32), channel_id=1, source_target_pairs={{0,8},{8,16},{16,24},{24,32},{32,40},{40,48},{48,56},{56,64},{64,7... | collective-permute-start | bytes 294920 | tf_op jit(solution)/shard_map/ppermute | solution.py:324
  13.2 12.8 %all-to-all-start = ((f32[16,4,128]{2,1,0:T(4,128)}), f32[16,4,128]{2,1,0:T(4,128)S(1)}, u32[]{:S(2)}, u32[]{:S(2)}) async-start(f32[16,4,128]{2,1,0:T(4,128)} %get-tuple-element.51), calls=%async_computation | async-start | bytes 65536 | tf_op jit(solution)/shard_map/all_to_all | solution.py:303
  22.9 19.2 %collective-permute-start.2 = (bf16[2,256,256]{2,1,0:T(8,128)(2,1)S(1)}, bf16[2,256,256]{2,1,0:T(8,128)(2,1)S(1)}, u32[]{:S(2)}, u32[]{:S(2)}) collective-permute-start(bf16[2,256,256]{2,1,0:T(8,128)(2,1)S(1)} %get-tuple-element.47), channel_id=1, source_target_pairs={{8,0},{16,8},{24,16},{32,24},{40,32},{48,40},{56,48},{64,56},{72,6... | collective-permute-start | bytes 786440 | tf_op jit(solution)/shard_map/ppermute | solution.py:364
  26.7 19.7 %all-to-all-start.1 = ((f32[32,8,128]{2,1,0:T(8,128)}), f32[32,8,128]{2,1,0:T(8,128)S(1)}, u32[]{:S(2)}, u32[]{:S(2)}) async-start(f32[32,8,128]{2,1,0:T(8,128)} %broadcast_in_dim.3), calls=%async_computation.1 | async-start | bytes 262144 | tf_op jit(solution)/shard_map/all_to_all | solution.py:303

commit v8 on v7

--- a/solution.py
+++ b/solution.py
@@ -129,11 +129,13 @@
 
 def tails_body(k_ref, v_ref, near_ref, far_ref, sem):
     first = k_ref.shape[0] - near_ref.shape[1] - far_ref.shape[1]
-    copies = [
-        pltpu.make_async_copy(ref.at[pl.ds(first + at, out.shape[1])], out.at[i], sem.at[2 * i + j])
-        for i, ref in enumerate((k_ref, v_ref))
-        for j, (out, at) in enumerate(((near_ref, far_ref.shape[1]), (far_ref, 0)))
-    ]
+    copies = []
+    for out, at in ((near_ref, first + far_ref.shape[1]), (far_ref, first)):
+        half = out.shape[1] // 2
+        for i, ref in enumerate((k_ref, v_ref)):
+            for part in (0, half):
+                rows = (ref.at[pl.ds(at + part, half)], out.at[i, pl.ds(part, half)])
+                copies.append(pltpu.make_async_copy(*rows, sem.at[len(copies)]))
     wait_all(start_all(copies))
 
 
@@ -225,13 +227,17 @@
     pay_ref[...] = jnp.broadcast_to(total[None], pay_ref.shape)
     copy = pltpu.make_async_copy(pay_ref, pay_hbm, sem)
     copy.start()
-    for h in range(HEADS):
-        hs = head(h)
+
+    def halo(h, carry):
+        hs = pl.ds(pl.multiple_of(h * HEAD_DIM, HEAD_DIM), HEAD_DIM)
         pairs = ((low_ref, low1_ref, q_ref), (prob_ref, prob1_ref, g_ref))
         for i, (w0, w1, x) in enumerate(pairs):
             both = jnp.concatenate([w0[h, BLK : 2 * BLK, :], w1[h, :BLK, :]], axis=1)
             back_ref[i, :BLK, hs] = dot(w0[h, :BLK, :], x[:BLK, hs], 1, 0).astype(BF16)
             back_ref[i, BLK:, hs] = dot(both, x[: 2 * BLK, hs], 1, 0).astype(BF16)
+        return carry
+
+    lax.fori_loop(0, HEADS, halo, 0)
     copy.wait()
 
 
@@ -316,7 +322,7 @@
         [((2, LEFT * SEG - FAR, width), BF16), ((2, FAR, width), BF16)],
         (k, v),
         [HBM] * 2,
-        [pltpu.SemaphoreType.DMA((4,))],
+        [pltpu.SemaphoreType.DMA((8,))],
         4,
     )
     ahead = [(s, s + 1) for s in range(count - 1)]

time: 47.5 us -> 47.4 us (level)
  no operation moved by 1% of the time
where the time goes in v8:
time: 47.4 us; the launch traced here: 47 us
  starting transfers between devices  33.5 us (71%)
  Pallas kernels  7.07 us (15%)
  waiting for transfers between devices  4.99 us (11%)
  between operations  0.74 us (2%)
  local copies, waits for them, and re-layouts  0.66 us (1%)
    all_to_all x2, starting transfers between devices, exchange(): lax.all_to_all(x, AXES, split_axis=0, concat_axis=0, axis_index_groups=gr...  25 us
    pallas_call x6, Pallas kernels, call(): pl.pallas_call(body, out_shape=tuple((jax.ShapeDtypeStruct(*o) for o in o...  7.07 us
    all_to_all x2, waiting for transfers between devices, exchange(): lax.all_to_all(x, AXES, split_axis=0, concat_axis=0, axis_index_groups=gr...  4.98 us
    ppermute x1, starting transfers between devices, local(): near = lax.ppermute(near, ('z', 'y'), ahead)  4.03 us
    ppermute x1, starting transfers between devices, local(): far = lax.ppermute(far, ('z', 'y'), ahead)  3.2 us
    ppermute x1, starting transfers between devices, local(): lax.ppermute(back, ('z', 'y'), [(s + 1, s) for s in range(count - 1)])  1.28 us
  transfers between devices with their start and end apart: 5, of which 2 were waited for; matrix products, arithmetic and copies ran while one was open for 1% of the time, Pallas kernels for 9%

profile of v8, /device:TPU:1, one launch (start us, length us, event | category | flops | bytes accessed | tf_op | source)
XLA Modules:
  0.0 47.0 jit_solution(7161593520876927200)
XLA Ops:
  0.6 0.9 %tails.1 = (bf16[2,160,256]{2,1,0:T(8,128)(2,1)S(1)}, bf16[2,96,256]{2,1,0:T(8,128)(2,1)S(1)}) custom-call(bf16[384,256]{1,0:T(8,128)(2,1)} %bitcast.12, bf16[384,256]{1,0:T(8,128)(2,1)} %bitcast.14), custom_call_target="tpu_custom_call" | custom-call | tf_op jit(solution)/shard_map/tails/pallas_call | solution.py:286
  1.6 4.0 %collective-permute-start = (bf16[2,160,256]{2,1,0:T(8,128)(2,1)S(1)}, bf16[2,160,256]{2,1,0:T(8,128)(2,1)S(1)}, u32[]{:S(2)}, u32[]{:S(2)}) collective-permute-start(bf16[2,160,256]{2,1,0:T(8,128)(2,1)S(1)} %get-tuple-element.31), channel_id=1, source_target_pairs={{0,8},{8,16},{16,24},{24,32},{32,40},{40,48},{48,56},{56,64},{64,7... | collective-permute-start | bytes 491528 | tf_op jit(solution)/shard_map/ppermute | solution.py:329
  5.6 0.0 copy-start
  5.6 3.2 %collective-permute-start.1 = (bf16[2,96,256]{2,1,0:T(8,128)(2,1)S(1)}, bf16[2,96,256]{2,1,0:T(8,128)(2,1)S(1)}, u32[]{:S(2)}, u32[]{:S(2)}) collective-permute-start(bf16[2,96,256]{2,1,0:T(8,128)(2,1)S(1)} %get-tuple-element.32), channel_id=1, source_target_pairs={{0,8},{8,16},{16,24},{24,32},{32,40},{40,48},{48,56},{56,64},{64,7... | collective-permute-start | bytes 294920 | tf_op jit(solution)/shard_map/ppermute | solution.py:330
  8.8 0.0 copy-done
  8.8 2.3 %own.1 = (bf16[384,256]{1,0:T(8,128)(2,1)S(1)}, bf16[384,256]{1,0:T(8,128)(2,1)S(1)}, bf16[384,256]{1,0:T(8,128)(2,1)S(1)}, bf16[384,256]{1,0:T(8,128)(2,1)S(1)}...) custom-call(bf16[384,256]{1,0:T(8,128)(2,1)} %bitcast.16, ...), custom_call_target="tpu_custom_call" | custom-call | tf_op jit(solution)/shard_map/own/pallas_call | solution.py:286
  11.2 0.0 collective-permute-done.near_ref
  11.2 0.8 %near.1 = (bf16[2,384,128]{2,1,0:T(8,128)(2,1)S(1)}, bf16[2,384,128]{2,1,0:T(8,128)(2,1)S(1)}, f32[4,128]{1,0:T(4,128)S(1)}, f32[2,288,128]{2,1,0:T(8,128)S(1)},...) custom-call(bf16[384,256]{1,0:T(8,128)(2,1)S(1)} %get-tuple-element.28.q_ref, ...), custom_call_target="tpu_custom_call" | custom-call | tf_op jit(solution)/shard_map/near/pallas_call | solution.py:286
  12.0 0.0 collective-permute-done.1.far_ref
  12.0 1.2 %far.1 = (f32[16,4,128]{2,1,0:T(4,128)}, bf16[2,384,128]{2,1,0:T(8,128)(2,1)S(1)}, bf16[2,384,128]{2,1,0:T(8,128)(2,1)S(1)}, bf16[2,256,256]{2,1,0:T(8,128)(2,1)S(1)}) custom-call(bf16[384,256]{1,0:T(8,128)(2,1)S(1)} %get-tuple-element.28.q_ref, bf16[384,256]{1,0:T(8,128)(2,1)S(1)} %get-tuple-element.30.g_ref, ...), custom_call_target="tpu_custom_call" | custom-call | tf_op jit(solution)/shard_map/far/pallas_call | solution.py:286
  13.1 9.7 %all-to-all-start = ((f32[16,4,128]{2,1,0:T(4,128)}), f32[16,4,128]{2,1,0:T(4,128)S(1)}, u32[]{:S(2)}, u32[]{:S(2)}) async-start(f32[16,4,128]{2,1,0:T(4,128)} %get-tuple-element.51), calls=%async_computation | async-start | bytes 65536 | tf_op jit(solution)/shard_map/all_to_all | solution.py:309
  22.8 1.3 %collective-permute-start.2 = (bf16[2,256,256]{2,1,0:T(8,128)(2,1)S(1)}, bf16[2,256,256]{2,1,0:T(8,128)(2,1)S(1)}, u32[]{:S(2)}, u32[]{:S(2)}) collective-permute-start(bf16[2,256,256]{2,1,0:T(8,128)(2,1)S(1)} %get-tuple-element.47), channel_id=1, source_target_pairs={{8,0},{16,8},{24,16},{32,24},{40,32},{48,40},{56,48},{64,56},{72,6... | collective-permute-start | bytes 786440 | tf_op jit(solution)/shard_map/ppermute | solution.py:370
  24.1 1.9 %all-to-all-done = f32[16,4,128]{2,1,0:T(4,128)S(1)} async-done(((f32[16,4,128]{2,1,0:T(4,128)}), f32[16,4,128]{2,1,0:T(4,128)S(1)}, u32[]{:S(2)}, u32[]{:S(2)}) %all-to-all-start) | async-done | bytes 32800 | tf_op jit(solution)/shard_map/all_to_all | solution.py:309
  26.0 0.7 %broadcast_in_dim.3 = f32[32,8,128]{2,1,0:T(8,128)} broadcast(f32[8,128]{1,0:T(8,128)S(1)} %bitcast_reduce_fusion), dimensions={1,2} | broadcast | bytes 135168 | tf_op jit(solution)/shard_map/broadcast_in_dim | solution.py:372
  26.6 15.4 %all-to-all-start.1 = ((f32[32,8,128]{2,1,0:T(8,128)}), f32[32,8,128]{2,1,0:T(8,128)S(1)}, u32[]{:S(2)}, u32[]{:S(2)}) async-start(f32[32,8,128]{2,1,0:T(8,128)} %broadcast_in_dim.3), calls=%async_computation.1 | async-start | bytes 262144 | tf_op jit(solution)/shard_map/all_to_all | solution.py:309
  42.0 0.0 collective-permute-done.2.back_ref
  42.0 1.2 %join.1 = (bf16[384,256]{1,0:T(8,128)(2,1)}, bf16[384,256]{1,0:T(8,128)(2,1)}, bf16[384,256]{1,0:T(8,128)(2,1)}) custom-call(bf16[384,256]{1,0:T(8,128)(2,1)S(1)} %get-tuple-element.28.q_ref, bf16[384,256]{1,0:T(8,128)(2,1)S(1)} %get-tuple-element.29.k_ref, bf16[384,256]{1,0:T(8,128)(2,1)S(1)} %get-tuple-element.30.g_ref, ...), custom_call_target="tpu_custom_call" | custom-call | tf_op jit(solution)/shard_map/join/pallas_call | solution.py:286
  43.2 3.1 %all-to-all-done.1 = f32[32,8,128]{2,1,0:T(8,128)S(1)} async-done(((f32[32,8,128]{2,1,0:T(8,128)}), f32[32,8,128]{2,1,0:T(8,128)S(1)}, u32[]{:S(2)}, u32[]{:S(2)}) %all-to-all-start.1) | async-done | bytes 131104 | tf_op jit(solution)/shard_map/all_to_all | solution.py:309
  46.3 0.7 %table.1 = f32[16,192]{1,0:T(8,128)} custom-call(f32[8,32,128]{2,1,0:T(8,128)S(1)} %bitcast.11), custom_call_target="tpu_custom_call" | custom-call | tf_op jit(solution)/shard_map/table/pallas_call | solution.py:286
  (1 shorter events, 0.0 us)
Async XLA Ops:
  1.6 9.6 %collective-permute-start = (bf16[2,160,256]{2,1,0:T(8,128)(2,1)S(1)}, bf16[2,160,256]{2,1,0:T(8,128)(2,1)S(1)}, u32[]{:S(2)}, u32[]{:S(2)}) collective-permute-start(bf16[2,160,256]{2,1,0:T(8,128)(2,1)S(1)} %get-tuple-element.31), channel_id=1, source_target_pairs={{0,8},{8,16},{16,24},{24,32},{32,40},{40,48},{48,56},{56,64},{64,7... | collective-permute-start | bytes 491528 | tf_op jit(solution)/shard_map/ppermute | solution.py:329
  5.6 3.2 %copy-start = (f32[2,192]{1,0:T(2,128)S(1)}, f32[2,192]{1,0:T(2,128)}, u32[]{:S(2)}) copy-start(f32[2,192]{1,0:T(2,128)} %rb_ref.1) | copy-start | bytes 4612
  5.6 6.3 %collective-permute-start.1 = (bf16[2,96,256]{2,1,0:T(8,128)(2,1)S(1)}, bf16[2,96,256]{2,1,0:T(8,128)(2,1)S(1)}, u32[]{:S(2)}, u32[]{:S(2)}) collective-permute-start(bf16[2,96,256]{2,1,0:T(8,128)(2,1)S(1)} %get-tuple-element.32), channel_id=1, source_target_pairs={{0,8},{8,16},{16,24},{24,32},{32,40},{40,48},{48,56},{56,64},{64,7... | collective-permute-start | bytes 294920 | tf_op jit(solution)/shard_map/ppermute | solution.py:330
  13.1 12.8 %all-to-all-start = ((f32[16,4,128]{2,1,0:T(4,128)}), f32[16,4,128]{2,1,0:T(4,128)S(1)}, u32[]{:S(2)}, u32[]{:S(2)}) async-start(f32[16,4,128]{2,1,0:T(4,128)} %get-tuple-element.51), calls=%async_computation | async-start | bytes 65536 | tf_op jit(solution)/shard_map/all_to_all | solution.py:309
  22.8 19.2 %collective-permute-start.2 = (bf16[2,256,256]{2,1,0:T(8,128)(2,1)S(1)}, bf16[2,256,256]{2,1,0:T(8,128)(2,1)S(1)}, u32[]{:S(2)}, u32[]{:S(2)}) collective-permute-start(bf16[2,256,256]{2,1,0:T(8,128)(2,1)S(1)} %get-tuple-element.47), channel_id=1, source_target_pairs={{8,0},{16,8},{24,16},{32,24},{40,32},{48,40},{56,48},{64,56},{72,6... | collective-permute-start | bytes 786440 | tf_op jit(solution)/shard_map/ppermute | solution.py:370
  26.6 19.7 %all-to-all-start.1 = ((f32[32,8,128]{2,1,0:T(8,128)}), f32[32,8,128]{2,1,0:T(8,128)S(1)}, u32[]{:S(2)}, u32[]{:S(2)}) async-start(f32[32,8,128]{2,1,0:T(8,128)} %broadcast_in_dim.3), calls=%async_computation.1 | async-start | bytes 262144 | tf_op jit(solution)/shard_map/all_to_all | solution.py:309

commit v9 on v8

--- a/solution.py
+++ b/solution.py
@@ -53,15 +53,17 @@
     return t0, t1, t2
 
 
+def tree_sum(parts):
+    while len(parts) > 1:
+        parts = [sum(parts[i : i + 2][1:], parts[i]) for i in range(0, len(parts), 2)]
+    return parts[0]
+
+
 def along_diagonals(x):
-    acc = x[:8]
-    for a in range(8, BLK, 8):
-        acc = acc + pltpu.roll(x[a : a + 8], BLK - a, 1)
+    acc = tree_sum([pltpu.roll(x[a : a + 8], BLK - a, 1) if a else x[:8] for a in range(0, BLK, 8)])
     row = lax.broadcasted_iota(jnp.int32, acc.shape, 0)
-    out = acc
-    for b in range(1, 8):
-        out = jnp.where(row == b, pltpu.roll(acc, BLK - b, 1), out)
-    return jnp.sum(out, axis=0, keepdims=True)
+    parts = [jnp.where(row == b, pltpu.roll(acc, BLK - b, 1) if b else acc, 0.0) for b in range(8)]
+    return jnp.sum(tree_sum(parts), axis=0, keepdims=True)
 
 
 def skew_sum(d0, d1, d2):

time: 47.4 us -> 47.4 us (level)
  no operation moved by 1% of the time
where the time goes in v9:
time: 47.4 us; the launch traced here: 47 us
  starting transfers between devices  33.5 us (71%)
  Pallas kernels  7.11 us (15%)
  waiting for transfers between devices  4.98 us (11%)
  between operations  0.73 us (2%)
  local copies, waits for them, and re-layouts  0.66 us (1%)
    all_to_all x2, starting transfers between devices, exchange(): lax.all_to_all(x, AXES, split_axis=0, concat_axis=0, axis_index_groups=gr...  25 us
    pallas_call x6, Pallas kernels, call(): pl.pallas_call(body, out_shape=tuple((jax.ShapeDtypeStruct(*o) for o in o...  7.11 us
    all_to_all x2, waiting for transfers between devices, exchange(): lax.all_to_all(x, AXES, split_axis=0, concat_axis=0, axis_index_groups=gr...  4.97 us
    ppermute x1, starting transfers between devices, local(): near = lax.ppermute(near, ('z', 'y'), ahead)  4.03 us
    ppermute x1, starting transfers between devices, local(): far = lax.ppermute(far, ('z', 'y'), ahead)  3.2 us
    ppermute x1, starting transfers between devices, local(): lax.ppermute(back, ('z', 'y'), [(s + 1, s) for s in range(count - 1)])  1.28 us
  transfers between devices with their start and end apart: 5, of which 2 were waited for; matrix products, arithmetic and copies ran while one was open for 1% of the time, Pallas kernels for 9%

profile of v9, /device:TPU:1, one launch (start us, length us, event | category | flops | bytes accessed | tf_op | source)
XLA Modules:
  0.0 47.0 jit_solution(282226228389455795)
XLA Ops:
  0.6 0.9 %tails.1 = (bf16[2,160,256]{2,1,0:T(8,128)(2,1)S(1)}, bf16[2,96,256]{2,1,0:T(8,128)(2,1)S(1)}) custom-call(bf16[384,256]{1,0:T(8,128)(2,1)} %bitcast.12, bf16[384,256]{1,0:T(8,128)(2,1)} %bitcast.14), custom_call_target="tpu_custom_call" | custom-call | tf_op jit(solution)/shard_map/tails/pallas_call | solution.py:288
  1.6 4.0 %collective-permute-start = (bf16[2,160,256]{2,1,0:T(8,128)(2,1)S(1)}, bf16[2,160,256]{2,1,0:T(8,128)(2,1)S(1)}, u32[]{:S(2)}, u32[]{:S(2)}) collective-permute-start(bf16[2,160,256]{2,1,0:T(8,128)(2,1)S(1)} %get-tuple-element.31), channel_id=1, source_target_pairs={{0,8},{8,16},{16,24},{24,32},{32,40},{40,48},{48,56},{56,64},{64,7... | collective-permute-start | bytes 491528 | tf_op jit(solution)/shard_map/ppermute | solution.py:331
  5.6 0.0 copy-start
  5.6 3.2 %collective-permute-start.1 = (bf16[2,96,256]{2,1,0:T(8,128)(2,1)S(1)}, bf16[2,96,256]{2,1,0:T(8,128)(2,1)S(1)}, u32[]{:S(2)}, u32[]{:S(2)}) collective-permute-start(bf16[2,96,256]{2,1,0:T(8,128)(2,1)S(1)} %get-tuple-element.32), channel_id=1, source_target_pairs={{0,8},{8,16},{16,24},{24,32},{32,40},{40,48},{48,56},{56,64},{64,7... | collective-permute-start | bytes 294920 | tf_op jit(solution)/shard_map/ppermute | solution.py:332
  8.8 0.0 copy-done
  8.8 2.4 %own.1 = (bf16[384,256]{1,0:T(8,128)(2,1)S(1)}, bf16[384,256]{1,0:T(8,128)(2,1)S(1)}, bf16[384,256]{1,0:T(8,128)(2,1)S(1)}, bf16[384,256]{1,0:T(8,128)(2,1)S(1)}...) custom-call(bf16[384,256]{1,0:T(8,128)(2,1)} %bitcast.16, ...), custom_call_target="tpu_custom_call" | custom-call | tf_op jit(solution)/shard_map/own/pallas_call | solution.py:288
  11.2 0.0 collective-permute-done.near_ref
  11.2 0.8 %near.1 = (bf16[2,384,128]{2,1,0:T(8,128)(2,1)S(1)}, bf16[2,384,128]{2,1,0:T(8,128)(2,1)S(1)}, f32[4,128]{1,0:T(4,128)S(1)}, f32[2,288,128]{2,1,0:T(8,128)S(1)},...) custom-call(bf16[384,256]{1,0:T(8,128)(2,1)S(1)} %get-tuple-element.28.q_ref, ...), custom_call_target="tpu_custom_call" | custom-call | tf_op jit(solution)/shard_map/near/pallas_call | solution.py:288
  12.0 0.0 collective-permute-done.1.far_ref
  12.0 1.1 %far.1 = (f32[16,4,128]{2,1,0:T(4,128)}, bf16[2,384,128]{2,1,0:T(8,128)(2,1)S(1)}, bf16[2,384,128]{2,1,0:T(8,128)(2,1)S(1)}, bf16[2,256,256]{2,1,0:T(8,128)(2,1)S(1)}) custom-call(bf16[384,256]{1,0:T(8,128)(2,1)S(1)} %get-tuple-element.28.q_ref, bf16[384,256]{1,0:T(8,128)(2,1)S(1)} %get-tuple-element.30.g_ref, ...), custom_call_target="tpu_custom_call" | custom-call | tf_op jit(solution)/shard_map/far/pallas_call | solution.py:288
  13.2 9.6 %all-to-all-start = ((f32[16,4,128]{2,1,0:T(4,128)}), f32[16,4,128]{2,1,0:T(4,128)S(1)}, u32[]{:S(2)}, u32[]{:S(2)}) async-start(f32[16,4,128]{2,1,0:T(4,128)} %get-tuple-element.51), calls=%async_computation | async-start | bytes 65536 | tf_op jit(solution)/shard_map/all_to_all | solution.py:311
  22.8 1.3 %collective-permute-start.2 = (bf16[2,256,256]{2,1,0:T(8,128)(2,1)S(1)}, bf16[2,256,256]{2,1,0:T(8,128)(2,1)S(1)}, u32[]{:S(2)}, u32[]{:S(2)}) collective-permute-start(bf16[2,256,256]{2,1,0:T(8,128)(2,1)S(1)} %get-tuple-element.47), channel_id=1, source_target_pairs={{8,0},{16,8},{24,16},{32,24},{40,32},{48,40},{56,48},{64,56},{72,6... | collective-permute-start | bytes 786440 | tf_op jit(solution)/shard_map/ppermute | solution.py:372
  24.1 1.9 %all-to-all-done = f32[16,4,128]{2,1,0:T(4,128)S(1)} async-done(((f32[16,4,128]{2,1,0:T(4,128)}), f32[16,4,128]{2,1,0:T(4,128)S(1)}, u32[]{:S(2)}, u32[]{:S(2)}) %all-to-all-start) | async-done | bytes 32800 | tf_op jit(solution)/shard_map/all_to_all | solution.py:311
  25.9 0.7 %broadcast_in_dim.3 = f32[32,8,128]{2,1,0:T(8,128)} broadcast(f32[8,128]{1,0:T(8,128)S(1)} %bitcast_reduce_fusion), dimensions={1,2} | broadcast | bytes 135168 | tf_op jit(solution)/shard_map/broadcast_in_dim | solution.py:374
  26.6 15.4 %all-to-all-start.1 = ((f32[32,8,128]{2,1,0:T(8,128)}), f32[32,8,128]{2,1,0:T(8,128)S(1)}, u32[]{:S(2)}, u32[]{:S(2)}) async-start(f32[32,8,128]{2,1,0:T(8,128)} %broadcast_in_dim.3), calls=%async_computation.1 | async-start | bytes 262144 | tf_op jit(solution)/shard_map/all_to_all | solution.py:311
  42.0 0.0 collective-permute-done.2.back_ref
  42.0 1.2 %join.1 = (bf16[384,256]{1,0:T(8,128)(2,1)}, bf16[384,256]{1,0:T(8,128)(2,1)}, bf16[384,256]{1,0:T(8,128)(2,1)}) custom-call(bf16[384,256]{1,0:T(8,128)(2,1)S(1)} %get-tuple-element.28.q_ref, bf16[384,256]{1,0:T(8,128)(2,1)S(1)} %get-tuple-element.29.k_ref, bf16[384,256]{1,0:T(8,128)(2,1)S(1)} %get-tuple-element.30.g_ref, ...), custom_call_target="tpu_custom_call" | custom-call | tf_op jit(solution)/shard_map/join/pallas_call | solution.py:288
  43.2 3.1 %all-to-all-done.1 = f32[32,8,128]{2,1,0:T(8,128)S(1)} async-done(((f32[32,8,128]{2,1,0:T(8,128)}), f32[32,8,128]{2,1,0:T(8,128)S(1)}, u32[]{:S(2)}, u32[]{:S(2)}) %all-to-all-start.1) | async-done | bytes 131104 | tf_op jit(solution)/shard_map/all_to_all | solution.py:311
  46.3 0.7 %table.1 = f32[16,192]{1,0:T(8,128)} custom-call(f32[8,32,128]{2,1,0:T(8,128)S(1)} %bitcast.11), custom_call_target="tpu_custom_call" | custom-call | tf_op jit(solution)/shard_map/table/pallas_call | solution.py:288
  (1 shorter events, 0.0 us)
Async XLA Ops:
  1.6 9.7 %collective-permute-start = (bf16[2,160,256]{2,1,0:T(8,128)(2,1)S(1)}, bf16[2,160,256]{2,1,0:T(8,128)(2,1)S(1)}, u32[]{:S(2)}, u32[]{:S(2)}) collective-permute-start(bf16[2,160,256]{2,1,0:T(8,128)(2,1)S(1)} %get-tuple-element.31), channel_id=1, source_target_pairs={{0,8},{8,16},{16,24},{24,32},{32,40},{40,48},{48,56},{56,64},{64,7... | collective-permute-start | bytes 491528 | tf_op jit(solution)/shard_map/ppermute | solution.py:331
  5.6 3.2 %copy-start = (f32[2,192]{1,0:T(2,128)S(1)}, f32[2,192]{1,0:T(2,128)}, u32[]{:S(2)}) copy-start(f32[2,192]{1,0:T(2,128)} %rb_ref.1) | copy-start | bytes 4612
  5.6 6.4 %collective-permute-start.1 = (bf16[2,96,256]{2,1,0:T(8,128)(2,1)S(1)}, bf16[2,96,256]{2,1,0:T(8,128)(2,1)S(1)}, u32[]{:S(2)}, u32[]{:S(2)}) collective-permute-start(bf16[2,96,256]{2,1,0:T(8,128)(2,1)S(1)} %get-tuple-element.32), channel_id=1, source_target_pairs={{0,8},{8,16},{16,24},{24,32},{32,40},{40,48},{48,56},{56,64},{64,7... | collective-permute-start | bytes 294920 | tf_op jit(solution)/shard_map/ppermute | solution.py:332
  13.2 12.8 %all-to-all-start = ((f32[16,4,128]{2,1,0:T(4,128)}), f32[16,4,128]{2,1,0:T(4,128)S(1)}, u32[]{:S(2)}, u32[]{:S(2)}) async-start(f32[16,4,128]{2,1,0:T(4,128)} %get-tuple-element.51), calls=%async_computation | async-start | bytes 65536 | tf_op jit(solution)/shard_map/all_to_all | solution.py:311
  22.8 19.2 %collective-permute-start.2 = (bf16[2,256,256]{2,1,0:T(8,128)(2,1)S(1)}, bf16[2,256,256]{2,1,0:T(8,128)(2,1)S(1)}, u32[]{:S(2)}, u32[]{:S(2)}) collective-permute-start(bf16[2,256,256]{2,1,0:T(8,128)(2,1)S(1)} %get-tuple-element.47), channel_id=1, source_target_pairs={{8,0},{16,8},{24,16},{32,24},{40,32},{48,40},{56,48},{64,56},{72,6... | collective-permute-start | bytes 786440 | tf_op jit(solution)/shard_map/ppermute | solution.py:372
  26.6 19.7 %all-to-all-start.1 = ((f32[32,8,128]{2,1,0:T(8,128)}), f32[32,8,128]{2,1,0:T(8,128)S(1)}, u32[]{:S(2)}, u32[]{:S(2)}) async-start(f32[32,8,128]{2,1,0:T(8,128)} %broadcast_in_dim.3), calls=%async_computation.1 | async-start | bytes 262144 | tf_op jit(solution)/shard_map/all_to_all | solution.py:311

commit v10 on v8

--- a/solution.py
+++ b/solution.py
@@ -15,7 +15,7 @@
 BUCKETS = 192
 HEADS = 2
 BLK = 128
-FAR = 96
+FAR = 112
 LEAD = BLK - FAR
 SCALE = HEAD_DIM**-0.5
 LOG2E = 1.4426950408889634

time: 47.4 us -> 47.4 us (level)
  no operation moved by 1% of the time
where the time goes in v10:
time: 47.4 us; the launch traced here: 47 us
  starting transfers between devices  33.8 us (71%)
  Pallas kernels  7.1 us (15%)
  waiting for transfers between devices  4.68 us (10%)
  between operations  0.74 us (2%)
  local copies, waits for them, and re-layouts  0.66 us (1%)
    all_to_all x2, starting transfers between devices, exchange(): lax.all_to_all(x, AXES, split_axis=0, concat_axis=0, axis_index_groups=gr...  25.3 us
    pallas_call x6, Pallas kernels, call(): pl.pallas_call(body, out_shape=tuple((jax.ShapeDtypeStruct(*o) for o in o...  7.1 us
    all_to_all x2, waiting for transfers between devices, exchange(): lax.all_to_all(x, AXES, split_axis=0, concat_axis=0, axis_index_groups=gr...  4.67 us
    ppermute x1, starting transfers between devices, local(): near = lax.ppermute(near, ('z', 'y'), ahead)  4.03 us
    ppermute x1, starting transfers between devices, local(): far = lax.ppermute(far, ('z', 'y'), ahead)  3.2 us
    ppermute x1, starting transfers between devices, local(): lax.ppermute(back, ('z', 'y'), [(s + 1, s) for s in range(count - 1)])  1.28 us
  transfers between devices with their start and end apart: 5, of which 2 were waited for; matrix products, arithmetic and copies ran while one was open for 1% of the time, Pallas kernels for 9%

profile of v10, /device:TPU:1, one launch (start us, length us, event | category | flops | bytes accessed | tf_op | source)
XLA Modules:
  0.0 47.0 jit_solution(5831629083898659536)
XLA Ops:
  0.6 0.9 %tails.1 = (bf16[2,144,256]{2,1,0:T(8,128)(2,1)S(1)}, bf16[2,112,256]{2,1,0:T(8,128)(2,1)S(1)}) custom-call(bf16[384,256]{1,0:T(8,128)(2,1)} %bitcast.12, bf16[384,256]{1,0:T(8,128)(2,1)} %bitcast.14), custom_call_target="tpu_custom_call" | custom-call | tf_op jit(solution)/shard_map/tails/pallas_call | solution.py:286
  1.6 4.0 %collective-permute-start = (bf16[2,144,256]{2,1,0:T(8,128)(2,1)S(1)}, bf16[2,144,256]{2,1,0:T(8,128)(2,1)S(1)}, u32[]{:S(2)}, u32[]{:S(2)}) collective-permute-start(bf16[2,144,256]{2,1,0:T(8,128)(2,1)S(1)} %get-tuple-element.31), channel_id=1, source_target_pairs={{0,8},{8,16},{16,24},{24,32},{32,40},{40,48},{48,56},{56,64},{64,7... | collective-permute-start | bytes 442376 | tf_op jit(solution)/shard_map/ppermute | solution.py:329
  5.6 0.0 copy-start
  5.6 3.2 %collective-permute-start.1 = (bf16[2,112,256]{2,1,0:T(8,128)(2,1)S(1)}, bf16[2,112,256]{2,1,0:T(8,128)(2,1)S(1)}, u32[]{:S(2)}, u32[]{:S(2)}) collective-permute-start(bf16[2,112,256]{2,1,0:T(8,128)(2,1)S(1)} %get-tuple-element.32), channel_id=1, source_target_pairs={{0,8},{8,16},{16,24},{24,32},{32,40},{40,48},{48,56},{56,64},{64,7... | collective-permute-start | bytes 344072 | tf_op jit(solution)/shard_map/ppermute | solution.py:330
  8.8 0.0 copy-done
  8.8 2.3 %own.1 = (bf16[384,256]{1,0:T(8,128)(2,1)S(1)}, bf16[384,256]{1,0:T(8,128)(2,1)S(1)}, bf16[384,256]{1,0:T(8,128)(2,1)S(1)}, bf16[384,256]{1,0:T(8,128)(2,1)S(1)}...) custom-call(bf16[384,256]{1,0:T(8,128)(2,1)} %bitcast.16, ...), custom_call_target="tpu_custom_call" | custom-call | tf_op jit(solution)/shard_map/own/pallas_call | solution.py:286
  11.2 0.0 collective-permute-done.near_ref
  11.2 0.8 %near.1 = (bf16[2,384,128]{2,1,0:T(8,128)(2,1)S(1)}, bf16[2,384,128]{2,1,0:T(8,128)(2,1)S(1)}, f32[4,128]{1,0:T(4,128)S(1)}, f32[2,272,128]{2,1,0:T(8,128)S(1)},...) custom-call(bf16[384,256]{1,0:T(8,128)(2,1)S(1)} %get-tuple-element.28.q_ref, ...), custom_call_target="tpu_custom_call" | custom-call | tf_op jit(solution)/shard_map/near/pallas_call | solution.py:286
  12.0 0.0 collective-permute-done.1.far_ref
  12.0 1.2 %far.1 = (f32[16,4,128]{2,1,0:T(4,128)}, bf16[2,384,128]{2,1,0:T(8,128)(2,1)S(1)}, bf16[2,384,128]{2,1,0:T(8,128)(2,1)S(1)}, bf16[2,256,256]{2,1,0:T(8,128)(2,1)S(1)}) custom-call(bf16[384,256]{1,0:T(8,128)(2,1)S(1)} %get-tuple-element.28.q_ref, bf16[384,256]{1,0:T(8,128)(2,1)S(1)} %get-tuple-element.30.g_ref, ...), custom_call_target="tpu_custom_call" | custom-call | tf_op jit(solution)/shard_map/far/pallas_call | solution.py:286
  13.2 9.9 %all-to-all-start = ((f32[16,4,128]{2,1,0:T(4,128)}), f32[16,4,128]{2,1,0:T(4,128)S(1)}, u32[]{:S(2)}, u32[]{:S(2)}) async-start(f32[16,4,128]{2,1,0:T(4,128)} %get-tuple-element.51), calls=%async_computation | async-start | bytes 65536 | tf_op jit(solution)/shard_map/all_to_all | solution.py:309
  23.1 1.3 %collective-permute-start.2 = (bf16[2,256,256]{2,1,0:T(8,128)(2,1)S(1)}, bf16[2,256,256]{2,1,0:T(8,128)(2,1)S(1)}, u32[]{:S(2)}, u32[]{:S(2)}) collective-permute-start(bf16[2,256,256]{2,1,0:T(8,128)(2,1)S(1)} %get-tuple-element.47), channel_id=1, source_target_pairs={{8,0},{16,8},{24,16},{32,24},{40,32},{48,40},{56,48},{64,56},{72,6... | collective-permute-start | bytes 786440 | tf_op jit(solution)/shard_map/ppermute | solution.py:370
  24.4 1.6 %all-to-all-done = f32[16,4,128]{2,1,0:T(4,128)S(1)} async-done(((f32[16,4,128]{2,1,0:T(4,128)}), f32[16,4,128]{2,1,0:T(4,128)S(1)}, u32[]{:S(2)}, u32[]{:S(2)}) %all-to-all-start) | async-done | bytes 32800 | tf_op jit(solution)/shard_map/all_to_all | solution.py:309
  26.0 0.7 %broadcast_in_dim.3 = f32[32,8,128]{2,1,0:T(8,128)} broadcast(f32[8,128]{1,0:T(8,128)S(1)} %bitcast_reduce_fusion), dimensions={1,2} | broadcast | bytes 135168 | tf_op jit(solution)/shard_map/broadcast_in_dim | solution.py:372
  26.6 15.4 %all-to-all-start.1 = ((f32[32,8,128]{2,1,0:T(8,128)}), f32[32,8,128]{2,1,0:T(8,128)S(1)}, u32[]{:S(2)}, u32[]{:S(2)}) async-start(f32[32,8,128]{2,1,0:T(8,128)} %broadcast_in_dim.3), calls=%async_computation.1 | async-start | bytes 262144 | tf_op jit(solution)/shard_map/all_to_all | solution.py:309
  42.0 0.0 collective-permute-done.2.back_ref
  42.0 1.2 %join.1 = (bf16[384,256]{1,0:T(8,128)(2,1)}, bf16[384,256]{1,0:T(8,128)(2,1)}, bf16[384,256]{1,0:T(8,128)(2,1)}) custom-call(bf16[384,256]{1,0:T(8,128)(2,1)S(1)} %get-tuple-element.28.q_ref, bf16[384,256]{1,0:T(8,128)(2,1)S(1)} %get-tuple-element.29.k_ref, bf16[384,256]{1,0:T(8,128)(2,1)S(1)} %get-tuple-element.30.g_ref, ...), custom_call_target="tpu_custom_call" | custom-call | tf_op jit(solution)/shard_map/join/pallas_call | solution.py:286
  43.2 3.1 %all-to-all-done.1 = f32[32,8,128]{2,1,0:T(8,128)S(1)} async-done(((f32[32,8,128]{2,1,0:T(8,128)}), f32[32,8,128]{2,1,0:T(8,128)S(1)}, u32[]{:S(2)}, u32[]{:S(2)}) %all-to-all-start.1) | async-done | bytes 131104 | tf_op jit(solution)/shard_map/all_to_all | solution.py:309
  46.3 0.7 %table.1 = f32[16,192]{1,0:T(8,128)} custom-call(f32[8,32,128]{2,1,0:T(8,128)S(1)} %bitcast.11), custom_call_target="tpu_custom_call" | custom-call | tf_op jit(solution)/shard_map/table/pallas_call | solution.py:286
  (1 shorter events, 0.0 us)
Async XLA Ops:
  1.6 9.6 %collective-permute-start = (bf16[2,144,256]{2,1,0:T(8,128)(2,1)S(1)}, bf16[2,144,256]{2,1,0:T(8,128)(2,1)S(1)}, u32[]{:S(2)}, u32[]{:S(2)}) collective-permute-start(bf16[2,144,256]{2,1,0:T(8,128)(2,1)S(1)} %get-tuple-element.31), channel_id=1, source_target_pairs={{0,8},{8,16},{16,24},{24,32},{32,40},{40,48},{48,56},{56,64},{64,7... | collective-permute-start | bytes 442376 | tf_op jit(solution)/shard_map/ppermute | solution.py:329
  5.6 3.2 %copy-start = (f32[2,192]{1,0:T(2,128)S(1)}, f32[2,192]{1,0:T(2,128)}, u32[]{:S(2)}) copy-start(f32[2,192]{1,0:T(2,128)} %rb_ref.1) | copy-start | bytes 4612
  5.6 6.3 %collective-permute-start.1 = (bf16[2,112,256]{2,1,0:T(8,128)(2,1)S(1)}, bf16[2,112,256]{2,1,0:T(8,128)(2,1)S(1)}, u32[]{:S(2)}, u32[]{:S(2)}) collective-permute-start(bf16[2,112,256]{2,1,0:T(8,128)(2,1)S(1)} %get-tuple-element.32), channel_id=1, source_target_pairs={{0,8},{8,16},{16,24},{24,32},{32,40},{40,48},{48,56},{56,64},{64,7... | collective-permute-start | bytes 344072 | tf_op jit(solution)/shard_map/ppermute | solution.py:330
  13.2 12.8 %all-to-all-start = ((f32[16,4,128]{2,1,0:T(4,128)}), f32[16,4,128]{2,1,0:T(4,128)S(1)}, u32[]{:S(2)}, u32[]{:S(2)}) async-start(f32[16,4,128]{2,1,0:T(4,128)} %get-tuple-element.51), calls=%async_computation | async-start | bytes 65536 | tf_op jit(solution)/shard_map/all_to_all | solution.py:309
  23.1 18.9 %collective-permute-start.2 = (bf16[2,256,256]{2,1,0:T(8,128)(2,1)S(1)}, bf16[2,256,256]{2,1,0:T(8,128)(2,1)S(1)}, u32[]{:S(2)}, u32[]{:S(2)}) collective-permute-start(bf16[2,256,256]{2,1,0:T(8,128)(2,1)S(1)} %get-tuple-element.47), channel_id=1, source_target_pairs={{8,0},{16,8},{24,16},{32,24},{40,32},{48,40},{56,48},{64,56},{72,6... | collective-permute-start | bytes 786440 | tf_op jit(solution)/shard_map/ppermute | solution.py:370
  26.6 19.7 %all-to-all-start.1 = ((f32[32,8,128]{2,1,0:T(8,128)}), f32[32,8,128]{2,1,0:T(8,128)S(1)}, u32[]{:S(2)}, u32[]{:S(2)}) async-start(f32[32,8,128]{2,1,0:T(8,128)} %broadcast_in_dim.3), calls=%async_computation.1 | async-start | bytes 262144 | tf_op jit(solution)/shard_map/all_to_all | solution.py:309
